TPU v7x, 256 devices: a whole 4x4x8 slice. The times are simulated.
256 devices in a mesh: kv: 16 (over y, x), tp: 16 (over z, core).
Axes of the slice: x: 4, y: 4, z: 8, core: 2. Of those that a mesh axis runs over, the one named last changes fastest.
Arguments:
- tokens: bfloat16 [256, 4096], P('kv', 'tp'), may hold values from -6 to 6
- attn_gain: float32 [4096], replicated, may hold values from 0.1 to 1.9
- w_query: bfloat16 [4096, 2048], P(None, 'tp'), may hold values from -0.09375 to 0.09375
- w_key: bfloat16 [4096, 2048], P(None, 'tp'), may hold values from -0.09375 to 0.09375
- w_value: bfloat16 [4096, 2048], P(None, 'tp'), may hold values from -0.09375 to 0.09375
- w_outgate: bfloat16 [4096, 2048], P(None, 'tp'), may hold values from -0.09375 to 0.09375
- w_rates: bfloat16 [2, 4096, 16], P(None, None, 'tp'), may hold values from -0.09375 to 0.09375
- head_rate: float32 [16], P('tp'), may hold values from 0.02 to 2
- head_gain: float32 [2048], P('tp'), may hold values from 0.1 to 1.9
- w_out: bfloat16 [2048, 4096], P('tp'), may hold values from -0.125 to 0.125
- state: float32 [256, 16, 128, 128], P('kv', 'tp'), may hold values from -2.4 to 2.4
- mlp_gain: float32 [4096], replicated, may hold values from 0.1 to 1.9
- w_gate: bfloat16 [4096, 11264], P(None, ('kv', 'tp')), may hold values from -0.09375 to 0.09375
- w_up: bfloat16 [4096, 11264], P(None, ('kv', 'tp')), may hold values from -0.09375 to 0.09375
- w_down: bfloat16 [4096, 11264], P(None, ('kv', 'tp')), may hold values from -0.25 to 0.25
Outputs:
- result: bfloat16 [256, 4096], P('kv', 'tp')
- new_state: float32 [256, 16, 128, 128], P('kv', 'tp')
All inputs are finite; a program needn't handle non-finite values.
Results may differ from a plain program's by a relative error of at most 0.014.
Values may be sent and summed in bfloat16 or wider, within the bound.
No kernel may reach another device: no remote copies, remote signals or barrier semaphores. Data moves between devices by JAX's collectives and lax.ppermute only.
A program may use at most 64 MiB of HBM per device.

v0:
```python
import jax
import jax.numpy as jnp
from jax import lax
from jax.sharding import PartitionSpec as P

EPS = 1e-06


def copy_for_each(value, axis):
    size = lax.axis_size(axis)
    return lax.all_to_all(
        jnp.broadcast_to(value[None], (size, *value.shape)), axis, 0, 0, tiled=True
    )


def in_order(tiles, dim):
    lengths = list(tiles.shape[1:])
    lengths[dim] *= tiles.shape[0]
    return jnp.moveaxis(tiles, 0, dim).reshape(lengths)


def gather_directly(value, axis, dim):
    tiles = copy_for_each(value, axis)
    return in_order(tiles, dim)


def cut_along(value, dim, size):
    lengths = value.shape
    tiles = value.reshape(*lengths[:dim], size, lengths[dim] // size, *lengths[dim + 1 :])
    return jnp.moveaxis(tiles, dim, 0)


def sent_and_summed(value, axis, dim):
    size = lax.axis_size(axis)
    tiles = lax.all_to_all(cut_along(value, dim, size), axis, 0, 0, tiled=True)
    return jnp.sum(tiles.astype(jnp.float32), axis=0)


def sent_and_summed_2(value, axis, dim):
    tiles = cut_along(value, dim, lax.axis_size(axis))
    arrived = lax.all_to_all(tiles, axis, split_axis=0, concat_axis=0, tiled=True)
    return arrived.sum(axis=0)


def row_norm(values, gain):
    floats = values.astype(jnp.float32)
    scaled = floats * lax.rsqrt(jnp.mean(floats * floats, axis=-1, keepdims=True) + EPS)
    return (scaled * gain).astype(jnp.bfloat16)


def hidden_units(normed_mlp, gate_part, up_part):
    gate_pre = jnp.dot(normed_mlp, gate_part, preferred_element_type=jnp.float32)
    up_pre = jnp.dot(normed_mlp, up_part, preferred_element_type=jnp.float32)
    return (jax.nn.silu(gate_pre) * up_pre).astype(jnp.bfloat16)


def down_product(hidden, down_part):
    return lax.dot_general(
        hidden, down_part, (((1,), (1,)), ((), ())), preferred_element_type=jnp.float32
    )


def body(
    tokens,
    attn_gain,
    w_query,
    w_key,
    w_value,
    w_outgate,
    w_rates,
    head_rate,
    head_gain,
    w_out,
    state,
    mlp_gain,
    w_gate,
    w_up,
    w_down,
):
    count = tokens.shape[0]
    local_heads = head_rate.shape[0]
    size = w_query.shape[1] // local_heads
    whole_rows = gather_directly(tokens, "tp", 1)
    normed = row_norm(whole_rows, attn_gain)
    query = jnp.dot(normed, w_query, preferred_element_type=jnp.float32).reshape(
        count, local_heads, size
    )
    key = jnp.dot(normed, w_key, preferred_element_type=jnp.float32).reshape(
        count, local_heads, size
    )
    value = jnp.dot(normed, w_value, preferred_element_type=jnp.float32).reshape(
        count, local_heads, size
    )
    gate_in = jnp.dot(normed, w_outgate, preferred_element_type=jnp.float32).reshape(
        count, local_heads, size
    )
    rates = jnp.einsum("bd,sdh->sbh", normed, w_rates, preferred_element_type=jnp.float32)
    unit_query = (
        query * lax.rsqrt(jnp.sum(query * query, axis=-1, keepdims=True) + EPS) * size ** (-0.5)
    )
    unit_key = key * lax.rsqrt(jnp.sum(key * key, axis=-1, keepdims=True) + EPS)
    strength = jax.nn.sigmoid(rates[0])
    fade = jnp.exp(-head_rate * jax.nn.softplus(rates[1]))
    carried = state * fade[:, :, None, None]
    fresh = strength[:, :, None] * (value - jnp.einsum("bhi,bhiv->bhv", unit_key, carried))
    new_state = carried + unit_key[:, :, :, None] * fresh[:, :, None, :]
    readout = jnp.einsum("bhi,bhiv->bhv", unit_query, new_state)
    normed_out = readout * lax.rsqrt(jnp.mean(readout * readout, axis=-1, keepdims=True) + EPS)
    mixed = (normed_out * head_gain.reshape(local_heads, size) * jax.nn.silu(gate_in)).astype(
        jnp.bfloat16
    )
    partial_value = jnp.dot(
        mixed.reshape(count, local_heads * size), w_out, preferred_element_type=jnp.float32
    )
    projected = sent_and_summed(partial_value.astype(jnp.bfloat16), "tp", 1)
    residual = (tokens.astype(jnp.float32) + projected).astype(jnp.bfloat16)
    full_residual = gather_directly(residual, "tp", 1)
    normed_mlp = row_norm(full_residual, mlp_gain)
    shared_rows = gather_directly(normed_mlp, "kv", 0)
    hidden = hidden_units(shared_rows, w_gate, w_up)
    owned = lax.all_to_all(hidden, "kv", split_axis=0, concat_axis=1, tiled=True)
    folded = down_product(owned, lax.all_gather(w_down, "kv", axis=1, tiled=True))
    down = sent_and_summed_2(folded, "tp", 1)
    result = (residual.astype(jnp.float32) + down).astype(jnp.bfloat16)
    return (result, new_state)


def solution(mesh):
    return jax.shard_map(
        body,
        mesh=mesh,
        in_specs=(
            P("kv", "tp"),
            P(),
            P(None, "tp"),
            P(None, "tp"),
            P(None, "tp"),
            P(None, "tp"),
            P(None, None, "tp"),
            P("tp"),
            P("tp"),
            P("tp", None),
            P("kv", "tp", None, None),
            P(),
            P(None, ("kv", "tp")),
            P(None, ("kv", "tp")),
            P(None, ("kv", "tp")),
        ),
        out_specs=(P("kv", "tp"), P("kv", "tp", None, None)),
        check_vma=False,
    )
```

profile of v0, /device:TPU:1, one launch (start us, length us, event | category | flops | bytes accessed | tf_op | source)
XLA Modules:
  0.0 156.5 jit_solution(1678312154421125208)
XLA Ops:
  7.2 0.7 all-gather.3.cloned.1.call-update
  7.9 1.4 broadcast_in_dim.6
  9.3 10.0 %all-to-all-start = ((bf16[16,16,256]{2,1,0:T(8,128)(2,1)}), bf16[16,16,256]{2,1,0:T(8,128)(2,1)S(1)}, u32[]{:S(2)}, u32[]{:S(2)}) async-start(bf16[16,16,256]{2,1,0:T(8,128)(2,1)} %broadcast_in_dim.6), calls=%async_computation | async-start | bytes 262144 | tf_op jit(solution)/shard_map/all_to_all | solution.py:11
  19.9 0.7 mul.205
  20.6 7.5 %all-to-all-done = bf16[16,16,256]{2,1,0:T(8,128)(2,1)S(1)} async-done(((bf16[16,16,256]{2,1,0:T(8,128)(2,1)}), bf16[16,16,256]{2,1,0:T(8,128)(2,1)S(1)}, u32[]{:S(2)}, u32[]{:S(2)}) %all-to-all-start) | async-done | bytes 131104 | tf_op jit(solution)/shard_map/all_to_all | solution.py:11
  28.6 0.4 multiply_reduce_fusion.1
  29.0 0.4 copy-done.3
  29.4 0.4 multiply_reduce_fusion.2
  30.1 0.3 fusion.10
  30.4 0.3 fusion.7
  30.7 0.5 fusion.33
  31.4 0.5 convolution_convert_fusion
  31.9 11.6 %all_to_all.44 = bf16[16,16,256]{2,1,0:T(8,128)(2,1)S(1)} all-to-all(bf16[16,16,256]{2,1,0:T(8,128)(2,1)S(1)} %bitcast.108), channel_id=1, replica_groups=mesh['kv'=16,'tp'=16] {'tp'}, dimensions={0} | all-to-all | bytes 262144 | tf_op jit(solution)/shard_map/all_to_all | solution.py:35
  43.5 11.6 %all_to_all.45 = bf16[16,16,256]{2,1,0:T(8,128)(2,1)S(1)} all-to-all(bf16[16,16,256]{2,1,0:T(8,128)(2,1)S(1)} %broadcast_in_dim.7), channel_id=1, replica_groups=mesh['kv'=16,'tp'=16] {'tp'}, dimensions={0} | all-to-all | bytes 262144 | tf_op jit(solution)/shard_map/all_to_all | solution.py:11
  55.6 49.6 %all_to_all.46 = bf16[16,16,4096]{2,1,0:T(8,128)(2,1)S(1)} all-to-all(bf16[16,16,4096]{2,1,0:T(8,128)(2,1)S(1)} %broadcast_in_dim.8), channel_id=1, replica_groups=mesh['kv'=16,'tp'=16] {'kv'}, dimensions={0} | all-to-all | bytes 4194304 | tf_op jit(solution)/shard_map/all_to_all | solution.py:11
  105.2 0.7 fusion.36
  106.2 0.7 fusion.6
  107.3 9.0 %all_to_all.47 = bf16[16,2,352]{2,1,0:T(2,128)(2,1)S(1)} all-to-all(bf16[16,2,352]{2,1,0:T(2,128)(2,1)S(1)} %reshape.265), channel_id=1, replica_groups=mesh['kv'=16,'tp'=16] {'kv'}, dimensions={0} | all-to-all | bytes 45056 | tf_op jit(solution)/shard_map/all_to_all | solution.py:121
  116.5 8.0 %reshape.258 = bf16[704,4096]{1,0:T(8,128)(2,1)} reshape(bf16[16,44,4096]{2,1,0:T(8,128)(2,1)} %all-gather.3.cloned.1.call-done) | data formatting | bytes 11534336
  124.6 4.2 %fusion.3 = f32[16,16,256]{2,1,0:T(8,128)} fusion(bf16[16,704,1]{1,0,2:T(8,128)(2,1)S(1)} %reshape.263, bf16[88,16,8,256]{3,2,1,0:T(8,128)(2,1)} %bitcast.102), kind=kOutput, calls=%fused_computation.4 | convolution fusion | flops 92274688 | bytes 6051840 | tf_op jit(solution)/shard_map/dot_general | solution.py:58
  128.8 8.7 %all-to-all-start.5 = ((f32[16,16,256]{2,1,0:T(8,128)}), f32[16,16,256]{2,1,0:T(8,128)S(1)}, u32[]{:S(2)}, u32[]{:S(2)}) async-start(f32[16,16,256]{2,1,0:T(8,128)} %fusion.3), calls=%async_computation.5 | async-start | bytes 524288 | tf_op jit(solution)/shard_map/all_to_all | solution.py:41
  137.5 1.3 multiply_add_fusion
  138.8 10.3 %all-to-all-done.5 = f32[16,16,256]{2,1,0:T(8,128)S(1)} async-done(((f32[16,16,256]{2,1,0:T(8,128)}), f32[16,16,256]{2,1,0:T(8,128)S(1)}, u32[]{:S(2)}, u32[]{:S(2)}) %all-to-all-start.5) | async-done | bytes 262176 | tf_op jit(solution)/shard_map/all_to_all | solution.py:41
  149.1 0.6 add_convert_fusion
  (59 shorter events, 2.4 us)
Async XLA Ops:
  7.2 24.2 %copy-start = (bf16[128,4096]{1,0:T(8,128)(2,1)S(1)}, bf16[128,4096]{1,0:T(8,128)(2,1)}, u32[]{:S(2)}) copy-start(bf16[128,4096]{1,0:T(8,128)(2,1)} %param.24) | copy-start | bytes 3145732
  7.2 21.3 %copy-start.8 = (f32[4096]{0:T(1024)S(1)}, f32[4096]{0:T(1024)}, u32[]{:S(2)}) copy-start(f32[4096]{0:T(1024)} %param.16) | copy-start | bytes 49156
  7.2 21.4 %copy-start.2 = (bf16[4096,128]{1,0:T(8,128)(2,1)S(1)}, bf16[4096,128]{1,0:T(8,128)(2,1)}, u32[]{:S(2)}) copy-start(bf16[4096,128]{1,0:T(8,128)(2,1)} %param.18) | copy-start | bytes 3145732
  7.2 109.3 %all-gather.3.cloned.1.call-start = ((), (), s32[]{:S(2)}) async-start(), calls=%async_computation.6 | async-start | bytes 6684672 | tf_op jit(solution)/shard_map/all_gather | solution.py:122
  9.3 18.9 %all-to-all-start = ((bf16[16,16,256]{2,1,0:T(8,128)(2,1)}), bf16[16,16,256]{2,1,0:T(8,128)(2,1)S(1)}, u32[]{:S(2)}, u32[]{:S(2)}) async-start(bf16[16,16,256]{2,1,0:T(8,128)(2,1)} %broadcast_in_dim.6), calls=%async_computation | async-start | bytes 262144 | tf_op jit(solution)/shard_map/all_to_all | solution.py:11
  28.2 1.2 copy-start.3
  28.3 1.4 copy-start.12
  28.4 1.7 %copy-start.1 = (f32[16,1,128,128]{3,2,1,0:T(8,128)S(1)}, f32[16,1,128,128]{3,2,1,0:T(8,128)}, u32[]{:S(2)}) copy-start(f32[16,1,128,128]{3,2,1,0:T(8,128)} %param.25) | copy-start | bytes 3145732
  28.5 1.9 %copy-start.4 = (bf16[4096,128]{1,0:T(8,128)(2,1)S(1)}, bf16[4096,128]{1,0:T(8,128)(2,1)}, u32[]{:S(2)}) copy-start(bf16[4096,128]{1,0:T(8,128)(2,1)} %param.19) | copy-start | bytes 3145732
  29.4 2.0 %copy-start.5 = (bf16[4096,128]{1,0:T(8,128)(2,1)S(1)}, bf16[4096,128]{1,0:T(8,128)(2,1)}, u32[]{:S(2)}) copy-start(bf16[4096,128]{1,0:T(8,128)(2,1)} %param.20) | copy-start | bytes 3145732
  29.4 2.0 %copy-start.11 = (f32[128]{0:T(128)S(1)}, f32[128]{0:T(128)}, u32[]{:S(2)}) copy-start(f32[128]{0:T(128)} %param.23) | copy-start | bytes 1540
  30.7 12.8 %copy-start.9 = (bf16[16,256]{1,0:T(8,128)(2,1)S(1)}, bf16[16,256]{1,0:T(8,128)(2,1)}, u32[]{:S(2)}) copy-start(bf16[16,256]{1,0:T(8,128)(2,1)} %param.15) | copy-start | bytes 24580
  31.4 23.9 %copy-start.10 = (f32[4096]{0:T(1024)S(1)}, f32[4096]{0:T(1024)}, u32[]{:S(2)}) copy-start(f32[4096]{0:T(1024)} %param.26) | copy-start | bytes 49156
  55.6 49.6 %copy-start.6 = (bf16[4096,44]{0,1:T(8,128)(2,1)S(1)}, bf16[4096,44]{0,1:T(8,128)(2,1)}, u32[]{:S(2)}) copy-start(bf16[4096,44]{0,1:T(8,128)(2,1)} %param.27) | copy-start | bytes 1081348
  105.2 1.0 copy-start.7
  128.8 20.3 %all-to-all-start.5 = ((f32[16,16,256]{2,1,0:T(8,128)}), f32[16,16,256]{2,1,0:T(8,128)S(1)}, u32[]{:S(2)}, u32[]{:S(2)}) async-start(f32[16,16,256]{2,1,0:T(8,128)} %fusion.3), calls=%async_computation.5 | async-start | bytes 524288 | tf_op jit(solution)/shard_map/all_to_all | solution.py:41
Sparse Core Ops, SparseCore 0:
  10.4 91.6 all-gather.2
where the time goes:
time: 157 us
  blocking collectives  81.7 us (52%)
  starting transfers between devices  18.7 us (12%)
  waiting for transfers between devices  18.5 us (12%)
  between operations  15 us (10%)
  local copies, waits for them, and re-layouts  11.6 us (7%)
  matrix products  8.08 us (5%)
  other arithmetic  2.96 us (2%)
    all_to_all x2, blocking collectives, copy_for_each(): lax.all_to_all(jnp.broadcast_to(value[None], (size, *value.shape)), axis,...  61.2 us
    all_to_all x1, blocking collectives, sent_and_summed(): tiles = lax.all_to_all(cut_along(value, dim, size), axis, 0, 0, tiled=True)  11.6 us
    all_to_all x1, waiting for transfers between devices, sent_and_summed_2(): lax.all_to_all(tiles, axis, split_axis=0, concat_axis=0, tiled=True)  10.3 us
    all_to_all x1, starting transfers between devices, copy_for_each(): lax.all_to_all(jnp.broadcast_to(value[None], (size, *value.shape)), axis,...  9.97 us
    all_to_all x1, blocking collectives, body(): lax.all_to_all(hidden, 'kv', split_axis=0, concat_axis=1, tiled=True)  8.99 us
    unnamed x29, local copies, waits for them, and re-layouts  8.94 us
    all_to_all x1, starting transfers between devices, sent_and_summed_2(): lax.all_to_all(tiles, axis, split_axis=0, concat_axis=0, tiled=True)  8.69 us
    all_to_all x1, waiting for transfers between devices, copy_for_each(): lax.all_to_all(jnp.broadcast_to(value[None], (size, *value.shape)), axis,...  7.51 us
  transfers between devices with their start and end apart: 3, of which 2 were waited for; matrix products, arithmetic and copies ran while one was open for 6% of the time, Pallas kernels for 0%

commit v1 on v0

v1 whole, which is shorter than its diff:
```python
import jax
import jax.numpy as jnp
from jax import lax
from jax.sharding import PartitionSpec as P

EPS = 1e-06
UNITS = 48


def y_ring(shift, side):
    return [
        (side * y + x, side * ((y + shift) % side) + x) for y in range(side) for x in range(side)
    ]


def plane_groups(side, tp):
    return [[(side * y + x) * tp + t for x in range(side) for t in range(tp)] for y in range(side)]


def body(
    tokens,
    attn_gain,
    w_query,
    w_key,
    w_value,
    w_outgate,
    w_rates,
    head_rate,
    head_gain,
    w_out,
    state,
    mlp_gain,
    w_gate,
    w_up,
    w_down,
):
    f32, bf16 = jnp.float32, jnp.bfloat16
    count, part = tokens.shape
    tp = lax.axis_size("tp")
    side = 4
    width = part * tp
    size = w_query.shape[1]
    units = w_gate.shape[1]

    own = jnp.stack([w_gate.T, w_up.T, w_down.T])
    own = jnp.pad(own, ((0, 0), (0, UNITS - units), (0, 0)))
    above = lax.ppermute(own, "kv", y_ring(1, side))
    below = lax.ppermute(own, "kv", y_ring(-1, side))

    tiles = lax.all_to_all(
        jnp.broadcast_to(tokens[None], (tp, count, part)), "tp", 0, 0, tiled=True
    )
    rows = jnp.moveaxis(tiles, 0, 1).reshape(count, width).astype(f32)
    scale = lax.rsqrt(jnp.mean(rows * rows, axis=-1, keepdims=True) + EPS)
    normed = (rows * scale * attn_gain).astype(bf16)
    query = jnp.dot(normed, w_query, preferred_element_type=f32)
    key = jnp.dot(normed, w_key, preferred_element_type=f32)
    value = jnp.dot(normed, w_value, preferred_element_type=f32)
    gate_in = jnp.dot(normed, w_outgate, preferred_element_type=f32)
    rates = jnp.einsum("bd,sdh->sbh", normed, w_rates, preferred_element_type=f32)
    unit_query = query * lax.rsqrt(jnp.sum(query * query, -1, keepdims=True) + EPS) * size**-0.5
    unit_key = key * lax.rsqrt(jnp.sum(key * key, -1, keepdims=True) + EPS)
    strength = jax.nn.sigmoid(rates[0])
    fade = jnp.exp(-head_rate * jax.nn.softplus(rates[1]))
    carried = state[:, 0] * fade[:, :, None]
    fresh = strength * (value - jnp.einsum("bi,biv->bv", unit_key, carried))
    new_state = carried + unit_key[:, :, None] * fresh[:, None, :]
    readout = jnp.einsum("bi,biv->bv", unit_query, new_state)
    normed_out = readout * lax.rsqrt(jnp.mean(readout * readout, -1, keepdims=True) + EPS)
    mixed = (normed_out * head_gain * jax.nn.silu(gate_in)).astype(bf16)
    partial = jnp.dot(mixed, w_out, preferred_element_type=f32).astype(bf16)
    tiles = jnp.moveaxis(partial.reshape(count, tp, part), 1, 0)
    tiles = lax.all_to_all(tiles, "tp", 0, 0, tiled=True)
    residual = (tokens.astype(f32) + jnp.sum(tiles.astype(f32), axis=0)).astype(bf16)

    residual, above, below = lax.optimization_barrier((residual, above, below))
    half = UNITS // 2
    far_low = lax.ppermute(above[:, :half], "kv", y_ring(1, side))
    far_high = lax.ppermute(below[:, half:], "kv", y_ring(-1, side))

    groups = plane_groups(side, tp)
    peers = side * tp
    tiles = lax.all_to_all(
        jnp.broadcast_to(residual[None], (peers, count, part)),
        ("kv", "tp"),
        0,
        0,
        tiled=True,
        axis_index_groups=groups,
    )
    rows = jnp.transpose(tiles.reshape(side, tp, count, part), (0, 2, 1, 3))
    rows = rows.reshape(side * count, width).astype(f32)
    scale = lax.rsqrt(jnp.mean(rows * rows, axis=-1, keepdims=True) + EPS)
    normed_mlp = (rows * scale * mlp_gain).astype(bf16)
    normed_mlp, far_low, far_high = lax.optimization_barrier((normed_mlp, far_low, far_high))
    weights = jnp.concatenate([own, above, below, far_low, far_high], axis=1)
    nt = (((1,), (1,)), ((), ()))
    gate_pre = lax.dot_general(normed_mlp, weights[0], nt, preferred_element_type=f32)
    up_pre = lax.dot_general(normed_mlp, weights[1], nt, preferred_element_type=f32)
    hidden = (jax.nn.silu(gate_pre) * up_pre).astype(bf16)
    partial = jnp.dot(hidden, weights[2], preferred_element_type=f32).astype(bf16)
    tiles = jnp.transpose(partial.reshape(side, count, tp, part), (0, 2, 1, 3))
    tiles = lax.all_to_all(
        tiles.reshape(peers, count, part),
        ("kv", "tp"),
        0,
        0,
        tiled=True,
        axis_index_groups=groups,
    )
    down = jnp.sum(tiles.astype(f32), axis=0)
    result = (residual.astype(f32) + down).astype(bf16)
    return (result, new_state[:, None])


def solution(mesh):
    return jax.shard_map(
        body,
        mesh=mesh,
        in_specs=(
            P("kv", "tp"),
            P(),
            P(None, "tp"),
            P(None, "tp"),
            P(None, "tp"),
            P(None, "tp"),
            P(None, None, "tp"),
            P("tp"),
            P("tp"),
            P("tp", None),
            P("kv", "tp", None, None),
            P(),
            P(None, ("kv", "tp")),
            P(None, ("kv", "tp")),
            P(None, ("kv", "tp")),
        ),
        out_specs=(P("kv", "tp"), P("kv", "tp", None, None)),
        check_vma=False,
    )
```

time: 157 us -> 115 us (0.73)
  blocking collectives: 81.7 us -> 14.5 us
  starting transfers between devices: 18.7 us -> 35.8 us
  between operations: 15 us -> 1.55 us
  waiting for transfers between devices: 18.5 us -> 25.1 us
  local copies, waits for them, and re-layouts: 11.6 us -> 17.5 us
  other arithmetic: 2.96 us -> 8.72 us
  matrix products: 8.08 us -> 10.9 us
    all_to_all x4 -> x1, blocking collectives: 81.7 us -> 14.5 us  [body(): tiles = lax.all_to_all(tiles, 'tp', 0, 0, tiled=True)]
    all_to_all x2 -> x3, starting transfers between devices: 18.7 us -> 30.4 us  [the longest x1 10.7 us: body(): lax.all_to_all(jnp.broadcast_to(residual[None], (peers, count, part)), ('...]
    all_to_all x2 -> x3, waiting for transfers between devices: 17.8 us -> 24.9 us  [the longest x1 15.9 us: body(): lax.all_to_all(tiles.reshape(peers, count, part), ('kv', 'tp'), 0, 0, til...]
    ppermute x0 -> x4, starting transfers between devices: none -> 5.41 us  [the longest x1 1.61 us: body(): far_high = lax.ppermute(below[:, half:], 'kv', y_ring(-1, side))]
    slice x0 -> x2, local copies, waits for them, and re-layouts: none -> 4.01 us  [the longest x1 2.02 us: body(): far_low = lax.ppermute(above[:, :half], 'kv', y_ring(1, side))]
    another operation x0 -> x1, other arithmetic: none -> 2.98 us  [body(): own = jnp.stack([w_gate.T, w_up.T, w_down.T])]
    dot_general x10 -> x9, matrix products: 8.08 us -> 10.9 us  [the longest x1 3.19 us: body(): jnp.dot(hidden, weights[2], preferred_element_type=f32).astype(bf16)]
    convert_element_type x4 -> x5, other arithmetic: 0.81 us -> 2.93 us  [the longest x1 1.39 us: body(): normed_mlp = (rows * scale * mlp_gain).astype(bf16)]
  transfers between devices with their start and end apart: 3 -> 7, of which waited for: 2 -> 4; matrix products, arithmetic and copies ran while one was open for 6% -> 21% of each run, Pallas kernels for 0% -> 0%
where the time goes in v1:
time: 115 us; the launch traced here: 114 us
  starting transfers between devices  35.8 us (31%)
  waiting for transfers between devices  25.1 us (22%)
  local copies, waits for them, and re-layouts  17.5 us (15%)
  blocking collectives  14.5 us (13%)
  matrix products  10.9 us (9%)
  other arithmetic  8.72 us (8%)
  between operations  1.55 us (1%)
    all_to_all x1, waiting for transfers between devices, body(): lax.all_to_all(tiles.reshape(peers, count, part), ('kv', 'tp'), 0, 0, til...  15.9 us
    all_to_all x1, blocking collectives, body(): tiles = lax.all_to_all(tiles, 'tp', 0, 0, tiled=True)  14.5 us
    all_to_all x1, starting transfers between devices, body(): lax.all_to_all(jnp.broadcast_to(residual[None], (peers, count, part)), ('...  10.7 us
    all_to_all x1, starting transfers between devices, body(): lax.all_to_all(jnp.broadcast_to(tokens[None], (tp, count, part)), 'tp', 0...  9.97 us
    all_to_all x1, starting transfers between devices, body(): lax.all_to_all(tiles.reshape(peers, count, part), ('kv', 'tp'), 0, 0, til...  9.7 us
    all_to_all x1, waiting for transfers between devices, body(): lax.all_to_all(jnp.broadcast_to(residual[None], (peers, count, part)), ('...  7.03 us
    unnamed x29, local copies, waits for them, and re-layouts  6.93 us
    dot_general x1, matrix products, body(): jnp.dot(hidden, weights[2], preferred_element_type=f32).astype(bf16)  3.19 us
  transfers between devices with their start and end apart: 7, of which 4 were waited for; matrix products, arithmetic and copies ran while one was open for 21% of the time, Pallas kernels for 0%

profile of v1, /device:TPU:1, one launch (start us, length us, event | category | flops | bytes accessed | tf_op | source)
XLA Modules:
  0.0 114.1 jit_solution(4641376498583350455)
XLA Ops:
  0.7 1.5 %broadcast_in_dim.4 = bf16[16,16,256]{2,1,0:T(8,128)(2,1)} broadcast(bf16[16,256]{1,0:T(8,128)(2,1)} %param.15), dimensions={1,2} | broadcast | bytes 139264 | tf_op jit(solution)/shard_map/broadcast_in_dim | solution.py:51
  2.1 10.0 %all-to-all-start = ((bf16[16,16,256]{2,1,0:T(8,128)(2,1)}), bf16[16,16,256]{2,1,0:T(8,128)(2,1)S(1)}, u32[]{:S(2)}, u32[]{:S(2)}) async-start(bf16[16,16,256]{2,1,0:T(8,128)(2,1)} %broadcast_in_dim.4), calls=%async_computation | async-start | bytes 262144 | tf_op jit(solution)/shard_map/all_to_all | solution.py:50
  12.1 3.0 %fusion.6 = (bf16[3,48,4096]{2,1,0:T(8,128)(2,1)}, bf16[3,192,4096]{2,1,0:T(8,128)(2,1)}) fusion(bf16[1,44,4096]{2,1,0:T(8,128)(2,1)} %bitcast.115, bf16[1,44,4096]{2,1,0:T(8,128)(2,1)} %bitcast.116, bf16[1,44,4096]{2,1,0:T(8,128)(2,1)} %bitcast.117), kind=kLoop, calls=%fused_computation.12 | loop fusion | flops 5898239 | bytes 3440640 | tf_op jit(solution)/shard_map/stack | solution.py:45
  15.1 1.3 %collective-permute-start = (bf16[3,48,4096]{2,1,0:T(8,128)(2,1)}, bf16[3,48,4096]{2,1,0:T(8,128)(2,1)S(1)}, u32[]{:S(2)}, u32[]{:S(2)}) collective-permute-start(bf16[3,48,4096]{2,1,0:T(8,128)(2,1)} %get-tuple-element.14), channel_id=1, source_target_pairs={{0,64},{16,80},{32,96},{48,112},{64,128},{80,144},{96,160},{112,17... | collective-permute-start | bytes 3538952 | tf_op jit(solution)/shard_map/ppermute | solution.py:47
  16.4 1.4 %collective-permute-start.1 = (bf16[3,48,4096]{2,1,0:T(8,128)(2,1)}, bf16[3,48,4096]{2,1,0:T(8,128)(2,1)}, u32[]{:S(2)}, u32[]{:S(2)}) collective-permute-start(bf16[3,48,4096]{2,1,0:T(8,128)(2,1)} %get-tuple-element.14), channel_id=1, source_target_pairs={{0,192},{16,208},{32,224},{48,240},{64,0},{80,16},{96,32},{112,48}... | collective-permute-start | bytes 3538952 | tf_op jit(solution)/shard_map/ppermute | solution.py:48
  19.1 1.9 %all-to-all-done = bf16[16,16,256]{2,1,0:T(8,128)(2,1)S(1)} async-done(((bf16[16,16,256]{2,1,0:T(8,128)(2,1)}), bf16[16,16,256]{2,1,0:T(8,128)(2,1)S(1)}, u32[]{:S(2)}, u32[]{:S(2)}) %all-to-all-start) | async-done | bytes 131104 | tf_op jit(solution)/shard_map/all_to_all | solution.py:50
  21.3 1.7 %multiply_reduce_fusion.3 = (f32[16]{0:T(128)S(1)}, f32[16,128]{1,0:T(8,128)S(1)}) fusion(bf16[16,4096]{1,0:T(8,128)(2,1)S(1)} %multiply_convert_fusion.1, bf16[4096,128]{1,0:T(8,128)(2,1)} %param.17), kind=kOutput, calls=%fused_computation.54 | convolution fusion | flops 16781296 | bytes 1187904 | tf_op jit(solution)/shard_map/dot_general | solution.py:56
  26.8 1.7 %convolution_convert_fusion.1 = bf16[16,4096]{1,0:T(8,128)(2,1)S(1)} fusion(bf16[128,4096]{1,0:T(8,128)(2,1)S(1)} %copy-done, f32[16,128]{1,0:T(8,128)} %bitcast.121, f32[128]{0:T(128)} %param.23, f32[16]{0:T(128)} %add_rsqrt_fusion.1, bf16[16,4096]{1,0:T(8,128)(2,1)S(1)} %multiply_convert_fusion.1, bf16[4096,128]{1,0:T(8,128)(2,1)} %param.20), kind=kOutput, calls=%fused_computation.1 | convolution fusion | flops 33636352 | bytes 2368064 | tf_op jit(solution)/shard_map/dot_general | solution.py:71
  28.5 14.5 %all_to_all.20 = bf16[16,16,256]{2,1,0:T(8,128)(2,1)S(1)} all-to-all(bf16[16,16,256]{2,1,0:T(8,128)(2,1)S(1)} %bitcast.114), channel_id=1, replica_groups=mesh['kv'=16,'tp'=16] {'tp'}, dimensions={0} | all-to-all | bytes 262144 | tf_op jit(solution)/shard_map/all_to_all | solution.py:73
  45.2 10.7 %all-to-all-start.2 = ((bf16[64,16,256]{2,1,0:T(8,128)(2,1)}), bf16[64,16,256]{2,1,0:T(8,128)(2,1)S(1)}, u32[]{:S(2)}, u32[]{:S(2)}) async-start(bf16[64,16,256]{2,1,0:T(8,128)(2,1)} %broadcast_in_dim.5), calls=%async_computation.2 | async-start | bytes 1048576 | tf_op jit(solution)/shard_map/all_to_all | solution.py:83
  56.0 2.0 %slice.25 = bf16[3,24,4096]{2,1,0:T(8,128)(2,1)} slice(bf16[3,48,4096]{2,1,0:T(8,128)(2,1)} %copy-done.2), slice={[0:3], [0:24], [0:4096]} | slice | bytes 1179648 | tf_op jit(solution)/shard_map/slice | solution.py:78
  59.1 2.0 %slice.26 = bf16[3,24,4096]{2,1,0:T(8,128)(2,1)} slice(bf16[3,48,4096]{2,1,0:T(8,128)(2,1)} %collective-permute-done.1), slice={[0:3], [24:48], [0:4096]} | slice | bytes 1179648 | tf_op jit(solution)/shard_map/slice | solution.py:79
  61.1 1.6 %collective-permute-start.3 = (bf16[3,24,4096]{2,1,0:T(8,128)(2,1)}, bf16[3,24,4096]{2,1,0:T(8,128)(2,1)}, u32[]{:S(2)}, u32[]{:S(2)}) collective-permute-start(bf16[3,24,4096]{2,1,0:T(8,128)(2,1)} %slice.26), channel_id=1, source_target_pairs={{0,192},{16,208},{32,224},{48,240},{64,0},{80,16},{96,32},{112,48}... | collective-permute-start | bytes 1769480 | tf_op jit(solution)/shard_map/ppermute | solution.py:79
  62.7 1.1 constant_dynamic-update-slice_fusion.3
  63.8 2.4 %constant_dynamic-update-slice_fusion.2 = bf16[3,192,4096]{2,1,0:T(8,128)(2,1)} fusion(bf16[3,192,4096]{2,1,0:T(8,128)(2,1)} %constant_dynamic-update-slice_fusion.3, bf16[3,48,4096]{2,1,0:T(8,128)(2,1)} %collective-permute-done.1), kind=kLoop, calls=%fused_computation.47 | loop fusion | bytes 2359296
  66.2 7.0 %all-to-all-done.2 = bf16[64,16,256]{2,1,0:T(8,128)(2,1)S(1)} async-done(((bf16[64,16,256]{2,1,0:T(8,128)(2,1)}), bf16[64,16,256]{2,1,0:T(8,128)(2,1)S(1)}, u32[]{:S(2)}, u32[]{:S(2)}) %all-to-all-start.2) | async-done | bytes 524320 | tf_op jit(solution)/shard_map/all_to_all | solution.py:83
  74.0 1.6 %copy.37 = f32[8,8,16,256]{3,1,2,0:T(8,128)} copy(f32[8,8,16,256]{3,2,1,0:T(8,128)S(1)} %bitcast.108) | data formatting | bytes 2097152
  75.9 1.4 %multiply_convert_fusion = bf16[64,4096]{1,0:T(8,128)(2,1)S(1)} fusion(f32[64,4096]{1,0:T(8,128)} %bitcast.107, f32[4096]{0:T(1024)S(1)} %copy-done.9, f32[64]{0:T(128)S(1)} %rsqrt.48), kind=kLoop, calls=%fused_computation.19 | loop fusion | flops 786432 | bytes 1589504 | tf_op jit(solution)/shard_map/convert_element_type | solution.py:94
  78.2 1.9 %constant_dynamic-update-slice_fusion = bf16[3,192,4096]{2,1,0:T(8,128)(2,1)} fusion(bf16[3,192,4096]{2,1,0:T(8,128)(2,1)} %constant_dynamic-update-slice_fusion.1, bf16[3,24,4096]{2,1,0:T(8,128)(2,1)} %collective-permute-done.3), kind=kLoop, calls=%fused_computation.45 | loop fusion | bytes 1179648 | tf_op jit(solution)/shard_map/concatenate | solution.py:96
  80.1 2.0 %fusion.3 = f32[64,192]{1,0:T(8,128)S(1)} fusion(bf16[64,4096]{1,0:T(8,128)(2,1)S(1)} %multiply_convert_fusion, bf16[3,192,4096]{2,1,0:T(8,128)(2,1)} %constant_dynamic-update-slice_fusion), kind=kOutput, calls=%fused_computation.8 | convolution fusion | flops 100663296 | bytes 2146304 | tf_op jit(solution)/shard_map/dot_general | solution.py:99
  82.2 3.2 %convolution_convert_fusion = bf16[64,4096]{1,0:T(8,128)(2,1)S(1)} fusion(bf16[3,192,4096]{2,1,0:T(8,128)(2,1)} %constant_dynamic-update-slice_fusion, f32[64,192]{1,0:T(8,128)S(1)} %fusion.3, bf16[64,4096]{1,0:T(8,128)(2,1)S(1)} %multiply_convert_fusion), kind=kOutput, calls=%fused_computation | convolution fusion | flops 201662464 | bytes 4243456 | tf_op jit(solution)/shard_map/dot_general | solution.py:101
  86.4 9.7 %all-to-all-start.3 = ((bf16[64,16,256]{2,1,0:T(8,128)(2,1)}), bf16[64,16,256]{2,1,0:T(8,128)(2,1)S(1)}, u32[]{:S(2)}, u32[]{:S(2)}) async-start(bf16[64,16,256]{2,1,0:T(8,128)(2,1)} %bitcast.30), calls=%async_computation.3 | async-start | bytes 1048576 | tf_op jit(solution)/shard_map/all_to_all | solution.py:103
  96.1 1.3 %multiply_add_fusion = f32[16,1,128,128]{3,2,1,0:T(8,128)} fusion(f32[16,1,128,128]{3,2,1,0:T(8,128)S(1)} %copy-done.1, f32[16,128]{1,0:T(8,128)S(1)} %fusion.7, f32[16,128]{1,0:T(8,128)S(1)} %broadcast_multiply_fusion, f32[16]{0:T(128)S(1)} %copy-done.11), kind=kLoop, calls=%fused_computation.17 | loop fusion | flops 786432 | bytes 2113600 | tf_op jit(solution)/shard_map/add | solution.py:67
  97.5 15.9 %all-to-all-done.3 = bf16[64,16,256]{2,1,0:T(8,128)(2,1)S(1)} async-done(((bf16[64,16,256]{2,1,0:T(8,128)(2,1)}), bf16[64,16,256]{2,1,0:T(8,128)(2,1)S(1)}, u32[]{:S(2)}, u32[]{:S(2)}) %all-to-all-start.3) | async-done | bytes 524320 | tf_op jit(solution)/shard_map/all_to_all | solution.py:103
  (65 shorter events, 11.6 us)
Async XLA Ops:
  0.6 26.1 %copy-start = (bf16[128,4096]{1,0:T(8,128)(2,1)S(1)}, bf16[128,4096]{1,0:T(8,128)(2,1)}, u32[]{:S(2)}) copy-start(bf16[128,4096]{1,0:T(8,128)(2,1)} %param.24) | copy-start | bytes 3145732
  0.6 17.2 %copy-start.7 = (f32[4096]{0:T(1024)S(1)}, f32[4096]{0:T(1024)}, u32[]{:S(2)}) copy-start(f32[4096]{0:T(1024)} %param.16) | copy-start | bytes 49156
  2.1 18.9 %all-to-all-start = ((bf16[16,16,256]{2,1,0:T(8,128)(2,1)}), bf16[16,16,256]{2,1,0:T(8,128)(2,1)S(1)}, u32[]{:S(2)}, u32[]{:S(2)}) async-start(bf16[16,16,256]{2,1,0:T(8,128)(2,1)} %broadcast_in_dim.4), calls=%async_computation | async-start | bytes 262144 | tf_op jit(solution)/shard_map/all_to_all | solution.py:50
  15.1 9.5 %copy-start.1 = (f32[16,1,128,128]{3,2,1,0:T(8,128)S(1)}, f32[16,1,128,128]{3,2,1,0:T(8,128)}, u32[]{:S(2)}) copy-start(f32[16,1,128,128]{3,2,1,0:T(8,128)} %param.25) | copy-start | bytes 3145732
  15.1 29.0 %collective-permute-start = (bf16[3,48,4096]{2,1,0:T(8,128)(2,1)}, bf16[3,48,4096]{2,1,0:T(8,128)(2,1)S(1)}, u32[]{:S(2)}, u32[]{:S(2)}) collective-permute-start(bf16[3,48,4096]{2,1,0:T(8,128)(2,1)} %get-tuple-element.14), channel_id=1, source_target_pairs={{0,64},{16,80},{32,96},{48,112},{64,128},{80,144},{96,160},{112,17... | collective-permute-start | bytes 3538952 | tf_op jit(solution)/shard_map/ppermute | solution.py:47
  16.4 27.7 %collective-permute-start.1 = (bf16[3,48,4096]{2,1,0:T(8,128)(2,1)}, bf16[3,48,4096]{2,1,0:T(8,128)(2,1)}, u32[]{:S(2)}, u32[]{:S(2)}) collective-permute-start(bf16[3,48,4096]{2,1,0:T(8,128)(2,1)} %get-tuple-element.14), channel_id=1, source_target_pairs={{0,192},{16,208},{32,224},{48,240},{64,0},{80,16},{96,32},{112,48}... | collective-permute-start | bytes 3538952 | tf_op jit(solution)/shard_map/ppermute | solution.py:48
  21.0 2.0 %copy-start.4 = (bf16[4096,128]{1,0:T(8,128)(2,1)S(1)}, bf16[4096,128]{1,0:T(8,128)(2,1)}, u32[]{:S(2)}) copy-start(bf16[4096,128]{1,0:T(8,128)(2,1)} %param.18) | copy-start | bytes 3145732
  21.0 2.4 %copy-start.8 = (f32[16,256]{1,0:T(8,128)S(1)}, f32[16,256]{1,0:T(8,128)}, u32[]{:S(2)}) copy-start(f32[16,256]{1,0:T(8,128)} %mul.197) | copy-start | bytes 49156
  21.0 3.9 %copy-start.5 = (bf16[4096,128]{1,0:T(8,128)(2,1)S(1)}, bf16[4096,128]{1,0:T(8,128)(2,1)}, u32[]{:S(2)}) copy-start(bf16[4096,128]{1,0:T(8,128)(2,1)} %param.19) | copy-start | bytes 3145732
  24.4 1.3 %copy-start.10 = (f32[16]{0:T(128)}, f32[16]{0:T(128)S(1)}, u32[]{:S(2)}) copy-start(f32[16]{0:T(128)S(1)} %fusion.30) | copy-start | bytes 196
  25.6 0.6 copy-start.6
  44.0 1.2 %copy-start.2 = (bf16[3,48,4096]{2,1,0:T(8,128)(2,1)}, bf16[3,48,4096]{2,1,0:T(8,128)(2,1)S(1)}, u32[]{:S(2)}) copy-start(bf16[3,48,4096]{2,1,0:T(8,128)(2,1)S(1)} %collective-permute-done) | copy-start | bytes 3538948
  45.2 28.0 %all-to-all-start.2 = ((bf16[64,16,256]{2,1,0:T(8,128)(2,1)}), bf16[64,16,256]{2,1,0:T(8,128)(2,1)S(1)}, u32[]{:S(2)}, u32[]{:S(2)}) async-start(bf16[64,16,256]{2,1,0:T(8,128)(2,1)} %broadcast_in_dim.5), calls=%async_computation.2 | async-start | bytes 1048576 | tf_op jit(solution)/shard_map/all_to_all | solution.py:83
  56.0 6.7 %copy-start.3 = (bf16[3,48,4096]{2,1,0:T(8,128)(2,1)S(1)}, bf16[3,48,4096]{2,1,0:T(8,128)(2,1)}, u32[]{:S(2)}) copy-start(bf16[3,48,4096]{2,1,0:T(8,128)(2,1)} %copy-done.2) | copy-start | bytes 3538948
  58.0 19.3 %collective-permute-start.2 = (bf16[3,24,4096]{2,1,0:T(8,128)(2,1)}, bf16[3,24,4096]{2,1,0:T(8,128)(2,1)S(1)}, u32[]{:S(2)}, u32[]{:S(2)}) collective-permute-start(bf16[3,24,4096]{2,1,0:T(8,128)(2,1)} %slice.25), channel_id=1, source_target_pairs={{0,64},{16,80},{32,96},{48,112},{64,128},{80,144},{96,160},{112,17... | collective-permute-start | bytes 1769480 | tf_op jit(solution)/shard_map/ppermute | solution.py:78
  61.1 16.3 %collective-permute-start.3 = (bf16[3,24,4096]{2,1,0:T(8,128)(2,1)}, bf16[3,24,4096]{2,1,0:T(8,128)(2,1)}, u32[]{:S(2)}, u32[]{:S(2)}) collective-permute-start(bf16[3,24,4096]{2,1,0:T(8,128)(2,1)} %slice.26), channel_id=1, source_target_pairs={{0,192},{16,208},{32,224},{48,240},{64,0},{80,16},{96,32},{112,48}... | collective-permute-start | bytes 1769480 | tf_op jit(solution)/shard_map/ppermute | solution.py:79
  73.4 2.5 %copy-start.9 = (f32[4096]{0:T(1024)S(1)}, f32[4096]{0:T(1024)}, u32[]{:S(2)}) copy-start(f32[4096]{0:T(1024)} %param.26) | copy-start | bytes 49156
  85.4 10.8 %copy-start.11 = (f32[16]{0:T(128)S(1)}, f32[16]{0:T(128)}, u32[]{:S(2)}) copy-start(f32[16]{0:T(128)} %copy-done.10) | copy-start | bytes 196
  86.4 27.0 %all-to-all-start.3 = ((bf16[64,16,256]{2,1,0:T(8,128)(2,1)}), bf16[64,16,256]{2,1,0:T(8,128)(2,1)S(1)}, u32[]{:S(2)}, u32[]{:S(2)}) async-start(bf16[64,16,256]{2,1,0:T(8,128)(2,1)} %bitcast.30), calls=%async_computation.3 | async-start | bytes 1048576 | tf_op jit(solution)/shard_map/all_to_all | solution.py:103

commit v2 on v1

v2 whole, which is shorter than its diff:
```python
import functools

import jax
import jax.numpy as jnp
from jax import lax
from jax.experimental import pallas as pl
from jax.experimental.pallas import tpu as pltpu
from jax.sharding import PartitionSpec as P


EPS = 1e-06
UNITS = 48
F32, BF16 = jnp.float32, jnp.bfloat16
NT = (((1,), (1,)), ((), ()))
VMEM = pl.BlockSpec(memory_space=pltpu.VMEM)
SMEM = pl.BlockSpec(memory_space=pltpu.SMEM)
HBM = pl.BlockSpec(memory_space=pltpu.HBM)


def in_vmem(*arrays):
    return [pltpu.with_memory_space_constraint(a, pltpu.VMEM) for a in arrays]


def y_ring(shift, side):
    return [
        (side * y + x, side * ((y + shift) % side) + x) for y in range(side) for x in range(side)
    ]


def plane_groups(side, tp):
    return [[(side * y + x) * tp + t for x in range(side) for t in range(tp)] for y in range(side)]


def silu(t):
    return t / (1.0 + jnp.exp(-t))


def norm_rows(tiles_ref, first, n_tiles, gain_ref, out_ref, at):
    rows, part = tiles_ref.shape[1:]
    total = jnp.zeros((rows, part), F32)
    for t in range(n_tiles):
        tile = tiles_ref[first + t].astype(F32)
        total = total + tile * tile
    mean = jnp.sum(total, axis=-1, keepdims=True) * (1.0 / (n_tiles * part))
    scale = lax.rsqrt(mean + EPS)
    for t in range(n_tiles):
        cols = slice(t * part, (t + 1) * part)
        tile = tiles_ref[first + t].astype(F32)
        out_ref[at : at + rows, cols] = (tile * scale * gain_ref[0:1, cols]).astype(BF16)


def attention_kernel(
    tiles_ref, gain_ref, wq_ref, wk_ref, wv_ref, wg_ref, wr_ref, rate_ref, head_gain_ref,
    wo_ref, state_ref, out_ref, new_state_ref, xn_ref, u_ref, w_ref,
):
    tp, count, part = tiles_ref.shape
    size = wq_ref.shape[1]
    norm_rows(tiles_ref, 0, tp, gain_ref, xn_ref, 0)
    xn = xn_ref[...]
    query = jnp.dot(xn, wq_ref[...], preferred_element_type=F32)
    key = jnp.dot(xn, wk_ref[...], preferred_element_type=F32)
    rates = lax.dot_general(xn, wr_ref[...], NT, preferred_element_type=F32)
    q = query * lax.rsqrt(jnp.sum(query * query, -1, keepdims=True) + EPS) * size**-0.5
    k = key * lax.rsqrt(jnp.sum(key * key, -1, keepdims=True) + EPS)
    q_high, k_high = q.astype(BF16), k.astype(BF16)
    q_low = (q - q_high.astype(F32)).astype(BF16)
    k_low = (k - k_high.astype(F32)).astype(BF16)
    probes = jnp.concatenate([k_high, k_low, q_high, q_low], axis=0)
    for b in range(count):
        read = jnp.dot(probes, state_ref[b].astype(BF16), preferred_element_type=F32)
        u_ref[b : b + 1, :] = read[b : b + 1] + read[count + b : count + b + 1]
        w_ref[b : b + 1, :] = read[2 * count + b : 2 * count + b + 1] + read[
            3 * count + b : 3 * count + b + 1
        ]
    value = jnp.dot(xn, wv_ref[...], preferred_element_type=F32)
    gate_in = jnp.dot(xn, wg_ref[...], preferred_element_type=F32)
    strength = 1.0 / (1.0 + jnp.exp(-rates[:, 0:1]))
    decay = rates[:, 1:2]
    softplus = jnp.maximum(decay, 0.0) + jnp.log(1.0 + jnp.exp(-jnp.abs(decay)))
    fade = jnp.exp(-rate_ref[...] * softplus)
    fresh = strength * (value - fade * u_ref[...])
    readout = fade * w_ref[...] + jnp.sum(q * k, -1, keepdims=True) * fresh
    scale = lax.rsqrt(jnp.mean(readout * readout, -1, keepdims=True) + EPS)
    mixed = (readout * scale * head_gain_ref[...] * silu(gate_in)).astype(BF16)
    for t in range(tp):
        cols = slice(t * part, (t + 1) * part)
        out_ref[t] = jnp.dot(mixed, wo_ref[:, cols], preferred_element_type=F32).astype(BF16)
    k_columns = k.T
    fade_rows = jnp.broadcast_to(fade, (count, size))
    for b in range(count):
        new_state_ref[b] = (
            fade_rows[b : b + 1, :] * state_ref[b]
            + k_columns[:, b : b + 1] * fresh[b : b + 1, :]
        )


def residual_kernel(tiles_ref, tokens_ref, out_ref, blocks_ref):
    total = tokens_ref[...].astype(F32)
    for t in range(tiles_ref.shape[0]):
        total = total + tiles_ref[t].astype(F32)
    residual = total.astype(BF16)
    out_ref[...] = residual
    for b in range(blocks_ref.shape[0]):
        blocks_ref[b] = residual


def pack_kernel(gate_ref, up_ref, down_ref, out_ref):
    units, width = gate_ref.shape
    for n, ref in enumerate((gate_ref, up_ref, down_ref)):
        out_ref[n, 0:units, :] = ref[...]
        out_ref[n, units:, :] = jnp.zeros((UNITS - units, width), BF16)


def feed_forward_kernel(
    side, tiles_ref, gain_ref, own_ref, above_ref, below_ref, far_low_ref, far_high_ref,
    out_ref, xn_ref,
):
    peers, count, part = tiles_ref.shape
    tp = peers // side
    half = far_low_ref.shape[2]
    for x in range(side):
        norm_rows(tiles_ref, x * tp, tp, gain_ref, xn_ref, x * count)
    xn = xn_ref[...]

    def pre_of(ref, cols):
        block = ref[0:2].reshape(2 * UNITS, ref.shape[2])
        return lax.dot_general(xn[:, cols], block, NT, preferred_element_type=F32)

    every = slice(None)
    pres = [pre_of(ref, every) for ref in (own_ref, above_ref, below_ref)]
    pres.append(
        pre_of(far_low_ref, slice(0, half)) + pre_of(far_high_ref, slice(half, 2 * half))
    )
    hidden = [(silu(pre[:, :UNITS]) * pre[:, UNITS:]).astype(BF16) for pre in pres]
    for t in range(tp):
        cols = slice(t * part, (t + 1) * part)
        if (t + 1) * part <= half:
            far = far_low_ref[2, :, cols]
        else:
            far = far_high_ref[2, :, slice(t * part - half, (t + 1) * part - half)]
        parts = (own_ref[2, :, cols], above_ref[2, :, cols], below_ref[2, :, cols], far)
        down = jnp.dot(hidden[0], parts[0], preferred_element_type=F32)
        for n in range(1, len(parts)):
            down = down + jnp.dot(hidden[n], parts[n], preferred_element_type=F32)
        down = down.astype(BF16)
        for x in range(side):
            out_ref[x * tp + t] = down[x * count : (x + 1) * count]


def body(
    tokens,
    attn_gain,
    w_query,
    w_key,
    w_value,
    w_outgate,
    w_rates,
    head_rate,
    head_gain,
    w_out,
    state,
    mlp_gain,
    w_gate,
    w_up,
    w_down,
):
    count, part = tokens.shape
    tp = lax.axis_size("tp")
    side = 4
    width = part * tp
    size = w_query.shape[1]
    peers = side * tp
    groups = plane_groups(side, tp)

    own = pl.pallas_call(
        pack_kernel,
        out_shape=pltpu.VMEM((3, UNITS, width), BF16),
        in_specs=[VMEM] * 3,
        out_specs=VMEM,
        compiler_params=pltpu.CompilerParams(vmem_limit_bytes=4 << 20),
        name="pack",
    )(w_gate.T, w_up.T, w_down.T)
    above = lax.ppermute(own, "kv", y_ring(1, side))
    below = lax.ppermute(own, "kv", y_ring(-1, side))
    copies = jnp.broadcast_to(tokens[None], (tp, count, part))
    copies, own = lax.optimization_barrier((copies, own))
    tiles = lax.all_to_all(copies, "tp", 0, 0, tiled=True)
    tiles, new_state = pl.pallas_call(
        attention_kernel,
        out_shape=(
            pltpu.VMEM((tp, count, part), BF16),
            jax.ShapeDtypeStruct((count, size, size), F32),
        ),
        in_specs=[VMEM] * 11,
        out_specs=(VMEM, VMEM),
        scratch_shapes=[
            pltpu.VMEM((count, width), BF16),
            pltpu.VMEM((count, size), F32),
            pltpu.VMEM((count, size), F32),
        ],
        compiler_params=pltpu.CompilerParams(vmem_limit_bytes=16 << 20),
        name="attention",
    )(
        tiles,
        attn_gain.reshape(1, width),
        w_query,
        w_key,
        w_value,
        w_outgate,
        w_rates.reshape(2, width),
        head_rate.reshape(1, 1),
        head_gain.reshape(1, size),
        w_out,
        state.reshape(count, size, size),
    )
    tiles = lax.all_to_all(tiles, "tp", 0, 0, tiled=True)
    residual, blocks = pl.pallas_call(
        residual_kernel,
        out_shape=(
            pltpu.VMEM((count, part), BF16),
            pltpu.VMEM((peers, count, part), BF16),
        ),
        in_specs=[VMEM, VMEM],
        out_specs=(VMEM, VMEM),
        compiler_params=pltpu.CompilerParams(vmem_limit_bytes=4 << 20),
        name="residual",
    )(tiles, tokens)

    blocks, above, below = lax.optimization_barrier((blocks, above, below))
    far_low = lax.ppermute(above[:, :, : width // 2], "kv", y_ring(1, side))
    far_high = lax.ppermute(below[:, :, width // 2 :], "kv", y_ring(-1, side))
    tiles = lax.all_to_all(
        blocks, ("kv", "tp"), 0, 0, tiled=True, axis_index_groups=groups
    )
    tiles = pl.pallas_call(
        functools.partial(feed_forward_kernel, side),
        out_shape=pltpu.VMEM((peers, count, part), BF16),
        in_specs=[VMEM] * 7,
        out_specs=VMEM,
        scratch_shapes=[pltpu.VMEM((side * count, width), BF16)],
        compiler_params=pltpu.CompilerParams(vmem_limit_bytes=16 << 20),
        name="feed_forward",
    )(tiles, mlp_gain.reshape(1, width), *in_vmem(own, above, below, far_low, far_high))
    tiles = lax.all_to_all(
        tiles, ("kv", "tp"), 0, 0, tiled=True, axis_index_groups=groups
    )
    down = jnp.sum(tiles.astype(F32), axis=0)
    result = (residual.astype(F32) + down).astype(BF16)
    return (result, new_state[:, None])


def solution(mesh):
    return jax.shard_map(
        body,
        mesh=mesh,
        in_specs=(
            P("kv", "tp"),
            P(),
            P(None, "tp"),
            P(None, "tp"),
            P(None, "tp"),
            P(None, "tp"),
            P(None, None, "tp"),
            P("tp"),
            P("tp"),
            P("tp", None),
            P("kv", "tp", None, None),
            P(),
            P(None, ("kv", "tp")),
            P(None, ("kv", "tp")),
            P(None, ("kv", "tp")),
        ),
        out_specs=(P("kv", "tp"), P("kv", "tp", None, None)),
        check_vma=False,
    )
```

time: 115 us -> 112 us (0.974)
  blocking collectives: 14.5 us -> 40.2 us
  starting transfers between devices: 35.8 us -> 22.2 us
  matrix products: 10.9 us -> 0 us
  other arithmetic: 8.72 us -> 0.7 us
  Pallas kernels: 0 us -> 6.46 us
  waiting for transfers between devices: 25.1 us -> 22.8 us
    all_to_all x0 -> x1, blocking collectives: none -> 28.7 us  [body(): lax.all_to_all(tiles, ('kv', 'tp'), 0, 0, tiled=True, axis_index_groups=g...]
    all_to_all x3 -> x2, waiting for transfers between devices: 24.9 us -> 8.34 us  [the longest x1 8.34 us: body(): tiles = lax.all_to_all(copies, 'tp', 0, 0, tiled=True)]
    all_to_all x3 -> x2, starting transfers between devices: 30.4 us -> 15.5 us  [the longest x1 9.43 us: body(): tiles = lax.all_to_all(copies, 'tp', 0, 0, tiled=True)]
    ppermute x2, waiting for transfers between devices: 0.01 us -> 14.4 us  [the longest x1 12.2 us: body(): far_high = lax.ppermute(below[:, :, width // 2:], 'kv', y_ring(-1, side))]
    dot_general x9 -> x0, matrix products: 10.9 us -> none  [the longest x1 3.19 us: body(): jnp.dot(hidden, weights[2], preferred_element_type=f32).astype(bf16)]
    unnamed x29 -> x42, local copies, waits for them, and re-layouts: 6.93 us -> 17 us
    pallas_call x0 -> x4, Pallas kernels: none -> 6.46 us  [the longest x1 3.24 us: body(): pl.pallas_call(attention_kernel, out_shape=(pltpu.VMEM((tp, count, part),...]
    slice x2, local copies, waits for them, and re-layouts: 4.01 us -> 0.09 us  [the longest x1 0.05 us: body(): far_low = lax.ppermute(above[:, :, :width // 2], 'kv', y_ring(1, side))]
  transfers between devices with their start and end apart: 7 -> 6, of which waited for: 4 -> 3; matrix products, arithmetic and copies ran while one was open for 21% -> 1% of each run, Pallas kernels for 0% -> 3%
where the time goes in v2:
time: 112 us; the launch traced here: 111 us
  blocking collectives  40.2 us (36%)
  waiting for transfers between devices  22.8 us (20%)
  starting transfers between devices  22.2 us (20%)
  local copies, waits for them, and re-layouts  17.7 us (16%)
  Pallas kernels  6.46 us (6%)
  between operations  1.38 us (1%)
    all_to_all x1, blocking collectives, body(): lax.all_to_all(tiles, ('kv', 'tp'), 0, 0, tiled=True, axis_index_groups=g...  28.7 us
    unnamed x42, local copies, waits for them, and re-layouts  17 us
    ppermute x1, waiting for transfers between devices, body(): far_high = lax.ppermute(below[:, :, width // 2:], 'kv', y_ring(-1, side))  12.2 us
    all_to_all x1, blocking collectives, body(): tiles = lax.all_to_all(tiles, 'tp', 0, 0, tiled=True)  11.5 us
    all_to_all x1, starting transfers between devices, body(): tiles = lax.all_to_all(copies, 'tp', 0, 0, tiled=True)  9.43 us
    all_to_all x1, waiting for transfers between devices, body(): tiles = lax.all_to_all(copies, 'tp', 0, 0, tiled=True)  8.34 us
    all_to_all x1, starting transfers between devices, body(): lax.all_to_all(blocks, ('kv', 'tp'), 0, 0, tiled=True, axis_index_groups=...  6.07 us
    ppermute x1, starting transfers between devices, body(): below = lax.ppermute(own, 'kv', y_ring(-1, side))  3.63 us
  transfers between devices with their start and end apart: 6, of which 3 were waited for; matrix products, arithmetic and copies ran while one was open for 1% of the time, Pallas kernels for 3%

profile of v2, /device:TPU:1, one launch (start us, length us, event | category | flops | bytes accessed | tf_op | source)
XLA Modules:
  0.0 111.5 jit_solution(4957226522757939592)
XLA Ops:
  0.6 1.0 copy-done.11
  1.6 1.0 copy-done.12
  2.6 1.0 copy-done.13
  3.7 3.6 %collective-permute-start.1 = (bf16[3,48,4096]{2,1,0:T(8,128)(2,1)S(1)}, bf16[3,48,4096]{2,1,0:T(8,128)(2,1)S(1)}, u32[]{:S(2)}, u32[]{:S(2)}) collective-permute-start(bf16[3,48,4096]{2,1,0:T(8,128)(2,1)S(1)} %pack.1.own_ref), channel_id=1, source_target_pairs={{0,192},{16,208},{32,224},{48,240},{64,0},{80,16},{96,32},{112,48}... | collective-permute-start | bytes 3538952 | tf_op jit(solution)/shard_map/ppermute | solution.py:184
  8.0 9.4 %all-to-all-start = ((bf16[16,16,256]{2,1,0:T(8,128)(2,1)}), bf16[16,16,256]{2,1,0:T(8,128)(2,1)}, u32[]{:S(2)}, u32[]{:S(2)}) async-start(bf16[16,16,256]{2,1,0:T(8,128)(2,1)} %broadcast_in_dim.4), calls=%async_computation | async-start | bytes 262144 | tf_op jit(solution)/shard_map/all_to_all | solution.py:187
  18.1 8.3 %all-to-all-done.tiles_ref = bf16[16,16,256]{2,1,0:T(8,128)(2,1)} async-done(((bf16[16,16,256]{2,1,0:T(8,128)(2,1)}), bf16[16,16,256]{2,1,0:T(8,128)(2,1)}, u32[]{:S(2)}, u32[]{:S(2)}) %all-to-all-start) | async-done | bytes 131104 | tf_op jit(solution)/shard_map/all_to_all | solution.py:187
  26.4 1.2 %copy-done = bf16[4096,128]{1,0:T(8,128)(2,1)S(1)} copy-done((bf16[4096,128]{1,0:T(8,128)(2,1)S(1)}, bf16[4096,128]{1,0:T(8,128)(2,1)}, u32[]{:S(2)}) %copy-start) | copy-done | bytes 1048600
  27.7 1.2 %copy-done.1 = bf16[4096,128]{1,0:T(8,128)(2,1)S(1)} copy-done((bf16[4096,128]{1,0:T(8,128)(2,1)S(1)}, bf16[4096,128]{1,0:T(8,128)(2,1)}, u32[]{:S(2)}) %copy-start.1) | copy-done | bytes 1048600
  28.9 1.2 %copy-done.2 = bf16[4096,128]{1,0:T(8,128)(2,1)S(1)} copy-done((bf16[4096,128]{1,0:T(8,128)(2,1)S(1)}, bf16[4096,128]{1,0:T(8,128)(2,1)}, u32[]{:S(2)}) %copy-start.2) | copy-done | bytes 1048600
  30.1 1.2 %copy-done.3 = bf16[4096,128]{1,0:T(8,128)(2,1)S(1)} copy-done((bf16[4096,128]{1,0:T(8,128)(2,1)S(1)}, bf16[4096,128]{1,0:T(8,128)(2,1)}, u32[]{:S(2)}) %copy-start.3) | copy-done | bytes 1048600
  31.4 1.2 %copy-done.4 = bf16[128,4096]{1,0:T(8,128)(2,1)S(1)} copy-done((bf16[128,4096]{1,0:T(8,128)(2,1)S(1)}, bf16[128,4096]{1,0:T(8,128)(2,1)}, u32[]{:S(2)}) %copy-start.4) | copy-done | bytes 1048600
  32.6 1.2 %copy-done.5 = f32[16,1,128,128]{3,2,1,0:T(8,128)S(1)} copy-done((f32[16,1,128,128]{3,2,1,0:T(8,128)S(1)}, f32[16,1,128,128]{3,2,1,0:T(8,128)}, u32[]{:S(2)}) %copy-start.5) | copy-done | bytes 1048600
  35.2 3.2 %attention.1 = (bf16[16,16,256]{2,1,0:T(8,128)(2,1)S(1)}, f32[16,128,128]{2,1,0:T(8,128)}) custom-call(bf16[16,16,256]{2,1,0:T(8,128)(2,1)} %all-to-all-done.tiles_ref, f32[1,4096]{1,0:T(1,128)S(1)} %bitcast.17, bf16[4096,128]{1,0:T(8,128)(2,1)S(1)} %copy-done, bf16[4096,128]{1,0:T(8,128)(2,1)S(1)} %copy-done.1, bf16[4096,128]{1,0:T(8,128)(2,1)S(1)} %copy-done.2, ...), custom_call_target="tpu_custom_call" | custom-call | tf_op jit(solution)/shard_map/attention/pallas_call | solution.py:188
  38.5 11.5 %all_to_all.20.tiles_ref = bf16[16,16,256]{2,1,0:T(8,128)(2,1)S(1)} all-to-all(bf16[16,16,256]{2,1,0:T(8,128)(2,1)S(1)} %get-tuple-element.12), channel_id=1, replica_groups=mesh['kv'=16,'tp'=16] {'tp'}, dimensions={0} | all-to-all | bytes 262144 | tf_op jit(solution)/shard_map/all_to_all | solution.py:216
  51.5 6.1 %all-to-all-start.2 = ((bf16[64,16,256]{2,1,0:T(8,128)(2,1)}), bf16[64,16,256]{2,1,0:T(8,128)(2,1)}, u32[]{:S(2)}, u32[]{:S(2)}) async-start(bf16[64,16,256]{2,1,0:T(8,128)(2,1)} %copy-done.10), calls=%async_computation.2 | async-start | bytes 1048576 | tf_op jit(solution)/shard_map/all_to_all | solution.py:232
  57.7 3.0 %collective-permute-start.3 = (bf16[3,48,2048]{2,1,0:T(8,128)(2,1)S(1)}, bf16[3,48,2048]{2,1,0:T(8,128)(2,1)S(1)}, u32[]{:S(2)}, u32[]{:S(2)}) collective-permute-start(bf16[3,48,2048]{2,1,0:T(8,128)(2,1)S(1)} %slice.7), channel_id=1, source_target_pairs={{0,192},{16,208},{32,224},{48,240},{64,0},{80,16},{96,32},{112,48}... | collective-permute-start | bytes 1769480 | tf_op jit(solution)/shard_map/ppermute | solution.py:231
  60.7 12.2 %collective-permute-done.3.far_high_ref = bf16[3,48,2048]{2,1,0:T(8,128)(2,1)S(1)} collective-permute-done((bf16[3,48,2048]{2,1,0:T(8,128)(2,1)S(1)}, bf16[3,48,2048]{2,1,0:T(8,128)(2,1)S(1)}, u32[]{:S(2)}, u32[]{:S(2)}) %collective-permute-start.3) | collective-permute-done | bytes 589856 | tf_op jit(solution)/shard_map/ppermute | solution.py:231
  72.9 0.8 copy-done.6
  73.7 2.3 %collective-permute-done.2.far_low_ref = bf16[3,48,2048]{2,1,0:T(8,128)(2,1)S(1)} collective-permute-done((bf16[3,48,2048]{2,1,0:T(8,128)(2,1)S(1)}, bf16[3,48,2048]{2,1,0:T(8,128)(2,1)S(1)}, u32[]{:S(2)}, u32[]{:S(2)}) %collective-permute-start.2) | collective-permute-done | bytes 589856 | tf_op jit(solution)/shard_map/ppermute | solution.py:230
  76.0 0.8 copy-done.8
  76.8 1.1 copy-done.7
  77.9 1.1 copy-done.9
  79.0 3.1 %feed_forward.1 = bf16[64,16,256]{2,1,0:T(8,128)(2,1)S(1)} custom-call(bf16[64,16,256]{2,1,0:T(8,128)(2,1)} %all-to-all-done.2.tiles_ref, f32[1,4096]{1,0:T(1,128)S(1)} %bitcast.19, bf16[3,48,4096]{2,1,0:T(8,128)(2,1)S(1)} %pack.1.own_ref, bf16[3,48,4096]{2,1,0:T(8,128)(2,1)S(1)} %collective-permute-done.above_ref, ...), custom_call_target="tpu_custom_call" | custom-call | tf_op jit(solution)/shard_map/feed_forward/pallas_call | solution.py:235
  82.1 28.7 %all_to_all.21 = bf16[64,16,256]{2,1,0:T(8,128)(2,1)S(1)} all-to-all(bf16[64,16,256]{2,1,0:T(8,128)(2,1)S(1)} %feed_forward.1), channel_id=1, replica_groups={{0,1,2,3,4,5,6,7,8,9,10,11,12,13,14,15,16,17,18,19,20,21,22,23,24,25,26..., dimensions={0} | all-to-all | bytes 1048576 | tf_op jit(solution)/shard_map/all_to_all | solution.py:244
  (41 shorter events, 4.5 us)
Async XLA Ops:
  0.6 1.0 copy-start.11
  1.6 1.0 copy-start.12
  2.6 1.0 copy-start.13
  3.6 3.7 %copy-start.14 = (bf16[16,256]{1,0:T(8,128)(2,1)S(1)}, bf16[16,256]{1,0:T(8,128)(2,1)}, u32[]{:S(2)}) copy-start(bf16[16,256]{1,0:T(8,128)(2,1)} %tokens_ref.1) | copy-start | bytes 24580
  3.6 22.8 %copy-start.20 = (f32[128]{0:T(128)S(1)}, f32[128]{0:T(128)}, u32[]{:S(2)}) copy-start(f32[128]{0:T(128)} %param.23) | copy-start | bytes 1540
  3.7 47.7 %collective-permute-start.1 = (bf16[3,48,4096]{2,1,0:T(8,128)(2,1)S(1)}, bf16[3,48,4096]{2,1,0:T(8,128)(2,1)S(1)}, u32[]{:S(2)}, u32[]{:S(2)}) collective-permute-start(bf16[3,48,4096]{2,1,0:T(8,128)(2,1)S(1)} %pack.1.own_ref), channel_id=1, source_target_pairs={{0,192},{16,208},{32,224},{48,240},{64,0},{80,16},{96,32},{112,48}... | collective-permute-start | bytes 3538952 | tf_op jit(solution)/shard_map/ppermute | solution.py:184
  7.3 44.1 %collective-permute-start = (bf16[3,48,4096]{2,1,0:T(8,128)(2,1)S(1)}, bf16[3,48,4096]{2,1,0:T(8,128)(2,1)S(1)}, u32[]{:S(2)}, u32[]{:S(2)}) collective-permute-start(bf16[3,48,4096]{2,1,0:T(8,128)(2,1)S(1)} %pack.1.own_ref), channel_id=1, source_target_pairs={{0,64},{16,80},{32,96},{48,112},{64,128},{80,144},{96,160},{112,17... | collective-permute-start | bytes 3538952 | tf_op jit(solution)/shard_map/ppermute | solution.py:183
  8.0 18.4 %all-to-all-start = ((bf16[16,16,256]{2,1,0:T(8,128)(2,1)}), bf16[16,16,256]{2,1,0:T(8,128)(2,1)}, u32[]{:S(2)}, u32[]{:S(2)}) async-start(bf16[16,16,256]{2,1,0:T(8,128)(2,1)} %broadcast_in_dim.4), calls=%async_computation | async-start | bytes 262144 | tf_op jit(solution)/shard_map/all_to_all | solution.py:187
  26.4 1.2 %copy-start = (bf16[4096,128]{1,0:T(8,128)(2,1)S(1)}, bf16[4096,128]{1,0:T(8,128)(2,1)}, u32[]{:S(2)}) copy-start(bf16[4096,128]{1,0:T(8,128)(2,1)} %wq_ref.1) | copy-start | bytes 3145732
  27.7 1.2 %copy-start.1 = (bf16[4096,128]{1,0:T(8,128)(2,1)S(1)}, bf16[4096,128]{1,0:T(8,128)(2,1)}, u32[]{:S(2)}) copy-start(bf16[4096,128]{1,0:T(8,128)(2,1)} %wk_ref.1) | copy-start | bytes 3145732
  28.9 1.2 %copy-start.2 = (bf16[4096,128]{1,0:T(8,128)(2,1)S(1)}, bf16[4096,128]{1,0:T(8,128)(2,1)}, u32[]{:S(2)}) copy-start(bf16[4096,128]{1,0:T(8,128)(2,1)} %wv_ref.1) | copy-start | bytes 3145732
  30.1 1.2 %copy-start.3 = (bf16[4096,128]{1,0:T(8,128)(2,1)S(1)}, bf16[4096,128]{1,0:T(8,128)(2,1)}, u32[]{:S(2)}) copy-start(bf16[4096,128]{1,0:T(8,128)(2,1)} %wg_ref.1) | copy-start | bytes 3145732
  31.3 1.2 %copy-start.4 = (bf16[128,4096]{1,0:T(8,128)(2,1)S(1)}, bf16[128,4096]{1,0:T(8,128)(2,1)}, u32[]{:S(2)}) copy-start(bf16[128,4096]{1,0:T(8,128)(2,1)} %wo_ref.1) | copy-start | bytes 3145732
  32.6 1.2 %copy-start.5 = (f32[16,1,128,128]{3,2,1,0:T(8,128)S(1)}, f32[16,1,128,128]{3,2,1,0:T(8,128)}, u32[]{:S(2)}) copy-start(f32[16,1,128,128]{3,2,1,0:T(8,128)} %param.25) | copy-start | bytes 3145732
  50.1 0.8 copy-start.10
  51.5 25.4 %all-to-all-start.2 = ((bf16[64,16,256]{2,1,0:T(8,128)(2,1)}), bf16[64,16,256]{2,1,0:T(8,128)(2,1)}, u32[]{:S(2)}, u32[]{:S(2)}) async-start(bf16[64,16,256]{2,1,0:T(8,128)(2,1)} %copy-done.10), calls=%async_computation.2 | async-start | bytes 1048576 | tf_op jit(solution)/shard_map/all_to_all | solution.py:232
  57.6 19.3 %copy-start.17 = (f32[4096]{0:T(1024)S(1)}, f32[4096]{0:T(1024)}, u32[]{:S(2)}) copy-start(f32[4096]{0:T(1024)} %param.26) | copy-start | bytes 49156
  57.7 15.2 %collective-permute-start.3 = (bf16[3,48,2048]{2,1,0:T(8,128)(2,1)S(1)}, bf16[3,48,2048]{2,1,0:T(8,128)(2,1)S(1)}, u32[]{:S(2)}, u32[]{:S(2)}) collective-permute-start(bf16[3,48,2048]{2,1,0:T(8,128)(2,1)S(1)} %slice.7), channel_id=1, source_target_pairs={{0,192},{16,208},{32,224},{48,240},{64,0},{80,16},{96,32},{112,48}... | collective-permute-start | bytes 1769480 | tf_op jit(solution)/shard_map/ppermute | solution.py:231
  60.7 15.3 %collective-permute-start.2 = (bf16[3,48,2048]{2,1,0:T(8,128)(2,1)S(1)}, bf16[3,48,2048]{2,1,0:T(8,128)(2,1)S(1)}, u32[]{:S(2)}, u32[]{:S(2)}) collective-permute-start(bf16[3,48,2048]{2,1,0:T(8,128)(2,1)S(1)} %slice.6), channel_id=1, source_target_pairs={{0,64},{16,80},{32,96},{48,112},{64,128},{80,144},{96,160},{112,17... | collective-permute-start | bytes 1769480 | tf_op jit(solution)/shard_map/ppermute | solution.py:230
  72.9 0.8 copy-start.6
  76.0 0.8 copy-start.8
  76.8 1.1 copy-start.7
  77.9 1.1 copy-start.9
  82.1 28.8 %copy-start.19 = (bf16[16,256]{1,0:T(8,128)(2,1)S(1)}, bf16[16,256]{1,0:T(8,128)(2,1)}, u32[]{:S(2)}) copy-start(bf16[16,256]{1,0:T(8,128)(2,1)} %copy-done.18) | copy-start | bytes 24580
  (3 other events, 2.0 us)

commit v3 on v2

--- a/solution.py
+++ b/solution.py
@@ -15,6 +15,10 @@
 VMEM = pl.BlockSpec(memory_space=pltpu.VMEM)
 SMEM = pl.BlockSpec(memory_space=pltpu.SMEM)
 HBM = pl.BlockSpec(memory_space=pltpu.HBM)
+
+
+def in_hbm(*arrays):
+    return [pltpu.with_memory_space_constraint(a, pltpu.HBM) for a in arrays]
 
 
 def in_vmem(*arrays):
@@ -50,48 +54,79 @@
 
 
 def attention_kernel(
-    tiles_ref, gain_ref, wq_ref, wk_ref, wv_ref, wg_ref, wr_ref, rate_ref, head_gain_ref,
-    wo_ref, state_ref, out_ref, new_state_ref, xn_ref, u_ref, w_ref,
+    tiles_ref, gain_ref, wr_ref, rate_ref, head_gain_ref, wq_hbm, wk_hbm, wv_hbm, wg_hbm, wo_hbm,
+    state_hbm, out_ref, new_state_hbm, xn_ref, u_ref, w_ref, wq_ref, wk_ref, wv_ref, wg_ref,
+    wo_ref, state_ref, new_state_ref, sems, out_sems,
 ):
     tp, count, part = tiles_ref.shape
     size = wq_ref.shape[1]
+    loads = [
+        pltpu.make_async_copy(source, target, sems.at[n])
+        for n, (source, target) in enumerate(
+            (
+                (wq_hbm, wq_ref),
+                (wk_hbm, wk_ref),
+                (state_hbm, state_ref),
+                (wv_hbm, wv_ref),
+                (wg_hbm, wg_ref),
+                (wo_hbm, wo_ref),
+            )
+        )
+    ]
+    for load in loads:
+        load.start()
     norm_rows(tiles_ref, 0, tp, gain_ref, xn_ref, 0)
     xn = xn_ref[...]
+    rates = lax.dot_general(xn, wr_ref[...], NT, preferred_element_type=F32)
+    loads[0].wait()
     query = jnp.dot(xn, wq_ref[...], preferred_element_type=F32)
+    loads[1].wait()
     key = jnp.dot(xn, wk_ref[...], preferred_element_type=F32)
-    rates = lax.dot_general(xn, wr_ref[...], NT, preferred_element_type=F32)
+    strength = 1.0 / (1.0 + jnp.exp(-rates[:, 0:1]))
+    decay = rates[:, 1:2]
+    softplus = jnp.maximum(decay, 0.0) + jnp.log(1.0 + jnp.exp(-jnp.abs(decay)))
+    fade = jnp.exp(-rate_ref[...] * softplus)
     q = query * lax.rsqrt(jnp.sum(query * query, -1, keepdims=True) + EPS) * size**-0.5
     k = key * lax.rsqrt(jnp.sum(key * key, -1, keepdims=True) + EPS)
     q_high, k_high = q.astype(BF16), k.astype(BF16)
     q_low = (q - q_high.astype(F32)).astype(BF16)
     k_low = (k - k_high.astype(F32)).astype(BF16)
     probes = jnp.concatenate([k_high, k_low, q_high, q_low], axis=0)
+    loads[2].wait()
     for b in range(count):
         read = jnp.dot(probes, state_ref[b].astype(BF16), preferred_element_type=F32)
         u_ref[b : b + 1, :] = read[b : b + 1] + read[count + b : count + b + 1]
         w_ref[b : b + 1, :] = read[2 * count + b : 2 * count + b + 1] + read[
             3 * count + b : 3 * count + b + 1
         ]
+    loads[3].wait()
     value = jnp.dot(xn, wv_ref[...], preferred_element_type=F32)
+    loads[4].wait()
     gate_in = jnp.dot(xn, wg_ref[...], preferred_element_type=F32)
-    strength = 1.0 / (1.0 + jnp.exp(-rates[:, 0:1]))
-    decay = rates[:, 1:2]
-    softplus = jnp.maximum(decay, 0.0) + jnp.log(1.0 + jnp.exp(-jnp.abs(decay)))
-    fade = jnp.exp(-rate_ref[...] * softplus)
     fresh = strength * (value - fade * u_ref[...])
     readout = fade * w_ref[...] + jnp.sum(q * k, -1, keepdims=True) * fresh
+    k_columns = k.T
+    stores = []
+    for b in range(count):
+        new_state_ref[b] = (
+            fade[b : b + 1, :] * state_ref[b] + k_columns[:, b : b + 1] * fresh[b : b + 1, :]
+        )
+        if b % 4 == 3:
+            rows = pl.ds(b - 3, 4)
+            stores.append(
+                pltpu.make_async_copy(
+                    new_state_ref.at[rows], new_state_hbm.at[rows], out_sems.at[b // 4]
+                )
+            )
+            stores[-1].start()
     scale = lax.rsqrt(jnp.mean(readout * readout, -1, keepdims=True) + EPS)
     mixed = (readout * scale * head_gain_ref[...] * silu(gate_in)).astype(BF16)
+    loads[5].wait()
     for t in range(tp):
         cols = slice(t * part, (t + 1) * part)
         out_ref[t] = jnp.dot(mixed, wo_ref[:, cols], preferred_element_type=F32).astype(BF16)
-    k_columns = k.T
-    fade_rows = jnp.broadcast_to(fade, (count, size))
-    for b in range(count):
-        new_state_ref[b] = (
-            fade_rows[b : b + 1, :] * state_ref[b]
-            + k_columns[:, b : b + 1] * fresh[b : b + 1, :]
-        )
+    for store in stores:
+        store.wait()
 
 
 def residual_kernel(tiles_ref, tokens_ref, out_ref, blocks_ref):
@@ -104,34 +139,54 @@
         blocks_ref[b] = residual
 
 
-def pack_kernel(gate_ref, up_ref, down_ref, out_ref):
-    units, width = gate_ref.shape
-    for n, ref in enumerate((gate_ref, up_ref, down_ref)):
-        out_ref[n, 0:units, :] = ref[...]
-        out_ref[n, units:, :] = jnp.zeros((UNITS - units, width), BF16)
-
-
-def feed_forward_kernel(
-    side, tiles_ref, gain_ref, own_ref, above_ref, below_ref, far_low_ref, far_high_ref,
-    out_ref, xn_ref,
+def pack_kernel(
+    rate_ref, gate_ref, up_ref, down_ref, tokens_ref, own_ref, copies_ref, rate_row_ref,
+    gate_at, up_at, down_at, sems,
 ):
-    peers, count, part = tiles_ref.shape
+    units = gate_ref.shape[0]
+    landed = (gate_at, up_at, down_at)
+    moves = [
+        pltpu.make_async_copy(ref, at, sems.at[n])
+        for n, (ref, at) in enumerate(zip((gate_ref, up_ref, down_ref), landed))
+    ]
+    for move in moves:
+        move.start()
+    for b in range(copies_ref.shape[0]):
+        copies_ref[b] = tokens_ref[...]
+    rate_row_ref[...] = jnp.full(rate_row_ref.shape, rate_ref[0], F32)
+    for n, (move, at) in enumerate(zip(moves, landed)):
+        move.wait()
+        own_ref[n, 0:units, :] = at[...]
+        own_ref[n, units:, :] = jnp.zeros((UNITS - units, own_ref.shape[2]), BF16)
+
+
+def pre_of(xn, ref):
+    block = ref[0:2].reshape(2 * UNITS, ref.shape[2])
+    return lax.dot_general(xn, block, NT, preferred_element_type=F32)
+
+
+def hidden_of(pre):
+    return (silu(pre[:, :UNITS]) * pre[:, UNITS:]).astype(BF16)
+
+
+def near_kernel(side, tiles_ref, gain_ref, own_ref, above_ref, below_ref, xn_ref, hidden_ref):
+    peers, count, _ = tiles_ref.shape
     tp = peers // side
-    half = far_low_ref.shape[2]
     for x in range(side):
         norm_rows(tiles_ref, x * tp, tp, gain_ref, xn_ref, x * count)
     xn = xn_ref[...]
-
-    def pre_of(ref, cols):
-        block = ref[0:2].reshape(2 * UNITS, ref.shape[2])
-        return lax.dot_general(xn[:, cols], block, NT, preferred_element_type=F32)
-
-    every = slice(None)
-    pres = [pre_of(ref, every) for ref in (own_ref, above_ref, below_ref)]
-    pres.append(
-        pre_of(far_low_ref, slice(0, half)) + pre_of(far_high_ref, slice(half, 2 * half))
-    )
-    hidden = [(silu(pre[:, :UNITS]) * pre[:, UNITS:]).astype(BF16) for pre in pres]
+    for n, ref in enumerate((own_ref, above_ref, below_ref)):
+        hidden_ref[n] = hidden_of(pre_of(xn, ref))
+
+
+def far_kernel(
+    side, xn_ref, hidden_ref, own_ref, above_ref, below_ref, far_low_ref, far_high_ref, out_ref
+):
+    peers, count, part = out_ref.shape
+    tp = peers // side
+    half = far_low_ref.shape[2]
+    pre = pre_of(xn_ref[:, :half], far_low_ref) + pre_of(xn_ref[:, half:], far_high_ref)
+    hidden = [hidden_ref[n] for n in range(3)] + [hidden_of(pre)]
     for t in range(tp):
         cols = slice(t * part, (t + 1) * part)
         if (t + 1) * part <= half:
@@ -172,46 +227,58 @@
     peers = side * tp
     groups = plane_groups(side, tp)
 
-    own = pl.pallas_call(
+    own, copies, rate_row = pl.pallas_call(
         pack_kernel,
-        out_shape=pltpu.VMEM((3, UNITS, width), BF16),
-        in_specs=[VMEM] * 3,
-        out_specs=VMEM,
+        out_shape=(
+            pltpu.VMEM((3, UNITS, width), BF16),
+            pltpu.VMEM((tp, count, part), BF16),
+            pltpu.VMEM((1, size), F32),
+        ),
+        in_specs=[SMEM] + [HBM] * 3 + [VMEM],
+        out_specs=(VMEM, VMEM, VMEM),
+        scratch_shapes=[pltpu.VMEM((w_gate.shape[1], width), BF16)] * 3
+        + [pltpu.SemaphoreType.DMA((3,))],
         compiler_params=pltpu.CompilerParams(vmem_limit_bytes=4 << 20),
         name="pack",
-    )(w_gate.T, w_up.T, w_down.T)
+    )(head_rate, *in_hbm(w_gate.T, w_up.T, w_down.T), tokens)
     above = lax.ppermute(own, "kv", y_ring(1, side))
     below = lax.ppermute(own, "kv", y_ring(-1, side))
-    copies = jnp.broadcast_to(tokens[None], (tp, count, part))
-    copies, own = lax.optimization_barrier((copies, own))
     tiles = lax.all_to_all(copies, "tp", 0, 0, tiled=True)
+    weight = pltpu.VMEM((width, size), BF16)
+    states = pltpu.VMEM((count, size, size), F32)
     tiles, new_state = pl.pallas_call(
         attention_kernel,
         out_shape=(
             pltpu.VMEM((tp, count, part), BF16),
-            jax.ShapeDtypeStruct((count, size, size), F32),
-        ),
-        in_specs=[VMEM] * 11,
-        out_specs=(VMEM, VMEM),
+            pltpu.HBM((count, size, size), F32),
+        ),
+        in_specs=[VMEM] * 5 + [HBM] * 6,
+        out_specs=(VMEM, HBM),
         scratch_shapes=[
             pltpu.VMEM((count, width), BF16),
             pltpu.VMEM((count, size), F32),
             pltpu.VMEM((count, size), F32),
+            weight,
+            weight,
+            weight,
+            weight,
+            pltpu.VMEM((size, width), BF16),
+            states,
+            states,
+            pltpu.SemaphoreType.DMA((6,)),
+            pltpu.SemaphoreType.DMA((4,)),
         ],
         compiler_params=pltpu.CompilerParams(vmem_limit_bytes=16 << 20),
         name="attention",
     )(
         tiles,
         attn_gain.reshape(1, width),
-        w_query,
-        w_key,
-        w_value,
-        w_outgate,
         w_rates.reshape(2, width),
-        head_rate.reshape(1, 1),
+        rate_row,
         head_gain.reshape(1, size),
-        w_out,
-        state.reshape(count, size, size),
+        *in_hbm(
+            w_query, w_key, w_value, w_outgate, w_out, state.reshape(count, size, size)
+        ),
     )
     tiles = lax.all_to_all(tiles, "tp", 0, 0, tiled=True)
     residual, blocks = pl.pallas_call(
@@ -232,15 +299,25 @@
     tiles = lax.all_to_all(
         blocks, ("kv", "tp"), 0, 0, tiled=True, axis_index_groups=groups
     )
+    xn, hidden = pl.pallas_call(
+        functools.partial(near_kernel, side),
+        out_shape=(
+            pltpu.VMEM((side * count, width), BF16),
+            pltpu.VMEM((3, side * count, UNITS), BF16),
+        ),
+        in_specs=[VMEM] * 5,
+        out_specs=(VMEM, VMEM),
+        compiler_params=pltpu.CompilerParams(vmem_limit_bytes=16 << 20),
+        name="near",
+    )(tiles, mlp_gain.reshape(1, width), *in_vmem(own, above, below))
     tiles = pl.pallas_call(
-        functools.partial(feed_forward_kernel, side),
+        functools.partial(far_kernel, side),
         out_shape=pltpu.VMEM((peers, count, part), BF16),
         in_specs=[VMEM] * 7,
         out_specs=VMEM,
-        scratch_shapes=[pltpu.VMEM((side * count, width), BF16)],
         compiler_params=pltpu.CompilerParams(vmem_limit_bytes=16 << 20),
-        name="feed_forward",
-    )(tiles, mlp_gain.reshape(1, width), *in_vmem(own, above, below, far_low, far_high))
+        name="far",
+    )(xn, hidden, *in_vmem(own, above, below, far_low, far_high))
     tiles = lax.all_to_all(
         tiles, ("kv", "tp"), 0, 0, tiled=True, axis_index_groups=groups
     )

time: 112 us -> 101 us (0.902)
  blocking collectives: 40.2 us -> 58.3 us
  local copies, waits for them, and re-layouts: 17.7 us -> 3.85 us
  starting transfers between devices: 22.2 us -> 12.7 us
  waiting for transfers between devices: 22.8 us -> 13.4 us
  Pallas kernels: 6.46 us -> 10 us
    all_to_all x0 -> x1, blocking collectives: none -> 18.1 us  [body(): tiles = lax.all_to_all(copies, 'tp', 0, 0, tiled=True)]
    unnamed x42 -> x18, local copies, waits for them, and re-layouts: 17 us -> 2.1 us
    all_to_all x1, waiting for transfers between devices: 0.01 us -> 12.7 us  [body(): lax.all_to_all(blocks, ('kv', 'tp'), 0, 0, tiled=True, axis_index_groups=...]
    ppermute x1, waiting for transfers between devices: 12.2 us -> 0.01 us  [body(): far_high = lax.ppermute(below[:, :, width // 2:], 'kv', y_ring(-1, side))]
    all_to_all x1 -> x0, starting transfers between devices: 9.43 us -> none  [body(): tiles = lax.all_to_all(copies, 'tp', 0, 0, tiled=True)]
    all_to_all x1 -> x0, waiting for transfers between devices: 8.34 us -> none  [body(): tiles = lax.all_to_all(copies, 'tp', 0, 0, tiled=True)]
    pallas_call x2 -> x3, Pallas kernels: 3.17 us -> 6.11 us  [the longest x1 2.66 us: body(): pl.pallas_call(functools.partial(far_kernel, side), out_shape=pltpu.VMEM(...]
    ppermute x1, waiting for transfers between devices: 2.3 us -> 0.73 us  [body(): far_low = lax.ppermute(above[:, :, :width // 2], 'kv', y_ring(1, side))]
  transfers between devices with their start and end apart: 6 -> 5, of which waited for: 3 -> 2; matrix products, arithmetic and copies ran while one was open for 1% -> 2% of each run, Pallas kernels for 3% -> 6%
where the time goes in v3:
time: 101 us; the launch traced here: 100 us
  blocking collectives  58.3 us (58%)
  waiting for transfers between devices  13.4 us (13%)
  starting transfers between devices  12.7 us (13%)
  Pallas kernels  10 us (10%)
  local copies, waits for them, and re-layouts  3.85 us (4%)
  between operations  1.41 us (1%)
    all_to_all x1, blocking collectives, body(): lax.all_to_all(tiles, ('kv', 'tp'), 0, 0, tiled=True, axis_index_groups=g...  28.7 us
    all_to_all x1, blocking collectives, body(): tiles = lax.all_to_all(copies, 'tp', 0, 0, tiled=True)  18.1 us
    all_to_all x1, waiting for transfers between devices, body(): lax.all_to_all(blocks, ('kv', 'tp'), 0, 0, tiled=True, axis_index_groups=...  12.7 us
    all_to_all x1, blocking collectives, body(): tiles = lax.all_to_all(tiles, 'tp', 0, 0, tiled=True)  11.6 us
    all_to_all x1, starting transfers between devices, body(): lax.all_to_all(blocks, ('kv', 'tp'), 0, 0, tiled=True, axis_index_groups=...  6.28 us
    pallas_call x1, Pallas kernels, body(): pl.pallas_call(attention_kernel, out_shape=(pltpu.VMEM((tp, count, part),...  3.83 us
    ppermute x1, starting transfers between devices, body(): below = lax.ppermute(own, 'kv', y_ring(-1, side))  3.63 us
    ppermute x1, starting transfers between devices, body(): far_high = lax.ppermute(below[:, :, width // 2:], 'kv', y_ring(-1, side))  2.74 us
  transfers between devices with their start and end apart: 5, of which 2 were waited for; matrix products, arithmetic and copies ran while one was open for 2% of the time, Pallas kernels for 6%

profile of v3, /device:TPU:1, one launch (start us, length us, event | category | flops | bytes accessed | tf_op | source)
XLA Modules:
  0.0 100.4 jit_solution(7173855978919830034)
XLA Ops:
  1.3 0.0 copy-start.1
  1.3 0.7 copy-done.1
  2.0 1.3 %pack.1 = (bf16[3,48,4096]{2,1,0:T(8,128)(2,1)S(1)}, bf16[16,16,256]{2,1,0:T(8,128)(2,1)S(1)}, f32[1,128]{1,0:T(1,128)S(1)}) custom-call(f32[1]{0:T(128)S(6)} %copy.18.rate_ref, bf16[44,4096]{1,0:T(8,128)(2,1)} %bitcast.16, bf16[44,4096]{1,0:T(8,128)(2,1)} %bitcast.17, bf16[44,4096]{1,0:T(8,128)(2,1)} %bitcast.18, bf16[16,256]{1,0:T(8,128)(2,1)S(1)} %copy-done.1), custom_call_target="tpu_custom_call" | custom-call | tf_op jit(solution)/shard_map/pack/pallas_call | solution.py:230
  3.3 3.6 %collective-permute-start.1 = (bf16[3,48,4096]{2,1,0:T(8,128)(2,1)S(1)}, bf16[3,48,4096]{2,1,0:T(8,128)(2,1)S(1)}, u32[]{:S(2)}, u32[]{:S(2)}) collective-permute-start(bf16[3,48,4096]{2,1,0:T(8,128)(2,1)S(1)} %get-tuple-element.19.own_ref), channel_id=1, source_target_pairs={{0,192},{16,208},{32,224},{48,240},{64,0},{80,16},{96,32},{112,48}... | collective-permute-start | bytes 3538952 | tf_op jit(solution)/shard_map/ppermute | solution.py:245
  6.9 18.1 %all_to_all.20.tiles_ref = bf16[16,16,256]{2,1,0:T(8,128)(2,1)S(1)} all-to-all(bf16[16,16,256]{2,1,0:T(8,128)(2,1)S(1)} %get-tuple-element.14), channel_id=1, replica_groups=mesh['kv'=16,'tp'=16] {'tp'}, dimensions={0} | all-to-all | bytes 262144 | tf_op jit(solution)/shard_map/all_to_all | solution.py:246
  25.1 0.0 copy-start.2
  25.1 3.8 %attention.1 = (bf16[16,16,256]{2,1,0:T(8,128)(2,1)S(1)}, f32[16,128,128]{2,1,0:T(8,128)}) custom-call(bf16[16,16,256]{2,1,0:T(8,128)(2,1)S(1)} %all_to_all.20.tiles_ref, f32[1,4096]{1,0:T(1,128)S(1)} %bitcast.11, bf16[2,4096]{1,0:T(2,128)(2,1)S(1)} %bitcast.12, f32[1,128]{1,0:T(1,128)S(1)} %get-tuple-element.15.rate_ref, f32[1,128]{1,0:T(1,128)S(1)} %bitcast.14, ...), custom_call_target="tpu_custom_call" | custom-call | tf_op jit(solution)/shard_map/attention/pallas_call | solution.py:249
  28.9 11.6 %all_to_all.21.tiles_ref = bf16[16,16,256]{2,1,0:T(8,128)(2,1)S(1)} all-to-all(bf16[16,16,256]{2,1,0:T(8,128)(2,1)S(1)} %get-tuple-element.16), channel_id=1, replica_groups=mesh['kv'=16,'tp'=16] {'tp'}, dimensions={0} | all-to-all | bytes 262144 | tf_op jit(solution)/shard_map/all_to_all | solution.py:283
  40.5 0.1 residual.1
  40.5 0.8 copy-done
  41.3 0.6 copy-done.6
  41.9 6.3 %all-to-all-start.2 = ((bf16[64,16,256]{2,1,0:T(8,128)(2,1)}), bf16[64,16,256]{2,1,0:T(8,128)(2,1)}, u32[]{:S(2)}, u32[]{:S(2)}) async-start(bf16[64,16,256]{2,1,0:T(8,128)(2,1)} %copy-done), calls=%async_computation.2 | async-start | bytes 1048576 | tf_op jit(solution)/shard_map/all_to_all | solution.py:299
  48.2 0.0 copy-start.5
  48.2 0.9 slice.6
  49.1 0.9 slice.7
  50.0 2.7 %collective-permute-start.3 = (bf16[3,48,2048]{2,1,0:T(8,128)(2,1)}, bf16[3,48,2048]{2,1,0:T(8,128)(2,1)}, u32[]{:S(2)}, u32[]{:S(2)}) collective-permute-start(bf16[3,48,2048]{2,1,0:T(8,128)(2,1)} %slice.7), channel_id=1, source_target_pairs={{0,192},{16,208},{32,224},{48,240},{64,0},{80,16},{96,32},{112,48}... | collective-permute-start | bytes 1769480 | tf_op jit(solution)/shard_map/ppermute | solution.py:298
  52.7 12.7 %all-to-all-done.2.tiles_ref = bf16[64,16,256]{2,1,0:T(8,128)(2,1)} async-done(((bf16[64,16,256]{2,1,0:T(8,128)(2,1)}), bf16[64,16,256]{2,1,0:T(8,128)(2,1)}, u32[]{:S(2)}, u32[]{:S(2)}) %all-to-all-start.2) | async-done | bytes 524320 | tf_op jit(solution)/shard_map/all_to_all | solution.py:299
  65.4 2.1 %near.1 = (bf16[64,4096]{1,0:T(8,128)(2,1)S(1)}, bf16[3,64,48]{2,1,0:T(8,128)(2,1)S(1)}) custom-call(bf16[64,16,256]{2,1,0:T(8,128)(2,1)} %all-to-all-done.2.tiles_ref, f32[1,4096]{1,0:T(1,128)S(1)} %bitcast.13, bf16[3,48,4096]{2,1,0:T(8,128)(2,1)S(1)} %get-tuple-element.19.own_ref, bf16[3,48,4096]{2,1,0:T(8,128)(2,1)S(1)} %collective-permute-done.above_ref, ...), custom_call_target="tpu_custom_call" | custom-call | tf_op jit(solution)/shard_map/near/pallas_call | solution.py:302
  67.6 0.7 collective-permute-done.2.far_low_ref
  68.3 2.7 %far.1 = bf16[64,16,256]{2,1,0:T(8,128)(2,1)S(1)} custom-call(bf16[64,4096]{1,0:T(8,128)(2,1)S(1)} %get-tuple-element.23.xn_ref, bf16[3,64,48]{2,1,0:T(8,128)(2,1)S(1)} %get-tuple-element.24.hidden_ref, bf16[3,48,4096]{2,1,0:T(8,128)(2,1)S(1)} %get-tuple-element.19.own_ref, bf16[3,48,4096]{2,1,0:T(8,128)(2,1)S(1)} %collective-permute-done.above_ref, ...), custom_call_target="tpu_custom_call" | custom-call | tf_op jit(solution)/shard_map/far/pallas_call | solution.py:313
  71.0 0.0 copy-start.7
  71.0 28.7 %all_to_all.22 = bf16[64,16,256]{2,1,0:T(8,128)(2,1)S(1)} all-to-all(bf16[64,16,256]{2,1,0:T(8,128)(2,1)S(1)} %far.1), channel_id=1, replica_groups={{0,1,2,3,4,5,6,7,8,9,10,11,12,13,14,15,16,17,18,19,20,21,22,23,24,25,26..., dimensions={0} | all-to-all | bytes 1048576 | tf_op jit(solution)/shard_map/all_to_all | solution.py:321
  99.7 0.1 convert_reduce_fusion
  99.8 0.6 add_convert_fusion
  (16 shorter events, 0.0 us)
Async XLA Ops:
  0.6 24.4 %copy-start.8 = (f32[128]{0:T(128)S(1)}, f32[128]{0:T(128)}, u32[]{:S(2)}) copy-start(f32[128]{0:T(128)} %param.23) | copy-start | bytes 1540
  1.3 0.7 copy-start.1
  2.0 23.1 %copy-start.3 = (f32[4096]{0:T(1024)S(1)}, f32[4096]{0:T(1024)}, u32[]{:S(2)}) copy-start(f32[4096]{0:T(1024)} %param.16) | copy-start | bytes 49156
  2.0 23.1 %copy-start.4 = (bf16[2,4096,1]{1,0,2:T(2,128)(2,1)S(1)}, bf16[2,4096,1]{1,0,2:T(2,128)(2,1)}, u32[]{:S(2)}) copy-start(bf16[2,4096,1]{1,0,2:T(2,128)(2,1)} %param.21) | copy-start | bytes 49156
  3.3 38.6 %collective-permute-start.1 = (bf16[3,48,4096]{2,1,0:T(8,128)(2,1)S(1)}, bf16[3,48,4096]{2,1,0:T(8,128)(2,1)S(1)}, u32[]{:S(2)}, u32[]{:S(2)}) collective-permute-start(bf16[3,48,4096]{2,1,0:T(8,128)(2,1)S(1)} %get-tuple-element.19.own_ref), channel_id=1, source_target_pairs={{0,192},{16,208},{32,224},{48,240},{64,0},{80,16},{96,32},{112,48}... | collective-permute-start | bytes 3538952 | tf_op jit(solution)/shard_map/ppermute | solution.py:245
  6.9 35.0 %collective-permute-start = (bf16[3,48,4096]{2,1,0:T(8,128)(2,1)S(1)}, bf16[3,48,4096]{2,1,0:T(8,128)(2,1)S(1)}, u32[]{:S(2)}, u32[]{:S(2)}) collective-permute-start(bf16[3,48,4096]{2,1,0:T(8,128)(2,1)S(1)} %get-tuple-element.19.own_ref), channel_id=1, source_target_pairs={{0,64},{16,80},{32,96},{48,112},{64,128},{80,144},{96,160},{112,17... | collective-permute-start | bytes 3538952 | tf_op jit(solution)/shard_map/ppermute | solution.py:244
  25.1 15.4 %copy-start.2 = (bf16[16,256]{1,0:T(8,128)(2,1)S(1)}, bf16[16,256]{1,0:T(8,128)(2,1)}, u32[]{:S(2)}) copy-start(bf16[16,256]{1,0:T(8,128)(2,1)} %tokens_ref.3) | copy-start | bytes 24580
  40.5 0.8 copy-start
  41.3 0.6 copy-start.6
  41.9 23.5 %all-to-all-start.2 = ((bf16[64,16,256]{2,1,0:T(8,128)(2,1)}), bf16[64,16,256]{2,1,0:T(8,128)(2,1)}, u32[]{:S(2)}, u32[]{:S(2)}) async-start(bf16[64,16,256]{2,1,0:T(8,128)(2,1)} %copy-done), calls=%async_computation.2 | async-start | bytes 1048576 | tf_op jit(solution)/shard_map/all_to_all | solution.py:299
  48.2 17.2 %copy-start.5 = (f32[4096]{0:T(1024)S(1)}, f32[4096]{0:T(1024)}, u32[]{:S(2)}) copy-start(f32[4096]{0:T(1024)} %param.26) | copy-start | bytes 49156
  50.0 17.6 %collective-permute-start.3 = (bf16[3,48,2048]{2,1,0:T(8,128)(2,1)}, bf16[3,48,2048]{2,1,0:T(8,128)(2,1)}, u32[]{:S(2)}, u32[]{:S(2)}) collective-permute-start(bf16[3,48,2048]{2,1,0:T(8,128)(2,1)} %slice.7), channel_id=1, source_target_pairs={{0,192},{16,208},{32,224},{48,240},{64,0},{80,16},{96,32},{112,48}... | collective-permute-start | bytes 1769480 | tf_op jit(solution)/shard_map/ppermute | solution.py:298
  52.7 15.6 %collective-permute-start.2 = (bf16[3,48,2048]{2,1,0:T(8,128)(2,1)}, bf16[3,48,2048]{2,1,0:T(8,128)(2,1)}, u32[]{:S(2)}, u32[]{:S(2)}) collective-permute-start(bf16[3,48,2048]{2,1,0:T(8,128)(2,1)} %slice.6), channel_id=1, source_target_pairs={{0,64},{16,80},{32,96},{48,112},{64,128},{80,144},{96,160},{112,17... | collective-permute-start | bytes 1769480 | tf_op jit(solution)/shard_map/ppermute | solution.py:297
  71.0 28.8 %copy-start.7 = (bf16[16,256]{1,0:T(8,128)(2,1)S(1)}, bf16[16,256]{1,0:T(8,128)(2,1)}, u32[]{:S(2)}) copy-start(bf16[16,256]{1,0:T(8,128)(2,1)} %copy-done.6) | copy-start | bytes 24580

commit v4 on v3

--- a/solution.py
+++ b/solution.py
@@ -135,8 +135,10 @@
         total = total + tiles_ref[t].astype(F32)
     residual = total.astype(BF16)
     out_ref[...] = residual
+    rows = blocks_ref.shape[1]
     for b in range(blocks_ref.shape[0]):
-        blocks_ref[b] = residual
+        at = (b % 2) * rows
+        blocks_ref[b] = residual[at : at + rows]
 
 
 def pack_kernel(
@@ -169,34 +171,49 @@
     return (silu(pre[:, :UNITS]) * pre[:, UNITS:]).astype(BF16)
 
 
-def near_kernel(side, tiles_ref, gain_ref, own_ref, above_ref, below_ref, xn_ref, hidden_ref):
+def norm_kernel(side, tiles_ref, gain_ref, xn_ref):
     peers, count, _ = tiles_ref.shape
     tp = peers // side
     for x in range(side):
         norm_rows(tiles_ref, x * tp, tp, gain_ref, xn_ref, x * count)
+
+
+def far_parts(far_low_ref, far_high_ref, part):
+    half = far_low_ref.shape[2]
+
+    def pre(xn_ref):
+        return pre_of(xn_ref[:, :half], far_low_ref) + pre_of(xn_ref[:, half:], far_high_ref)
+
+    def columns(t):
+        if (t + 1) * part <= half:
+            return far_low_ref[2, :, t * part : (t + 1) * part]
+        return far_high_ref[2, :, t * part - half : (t + 1) * part - half]
+
+    return pre, columns
+
+
+def near_kernel(part, xn_ref, *refs):
+    *whole, far_low_ref, far_high_ref, out_ref = refs
+    far_pre, far_columns = far_parts(far_low_ref, far_high_ref, part)
     xn = xn_ref[...]
-    for n, ref in enumerate((own_ref, above_ref, below_ref)):
-        hidden_ref[n] = hidden_of(pre_of(xn, ref))
-
-
-def far_kernel(
-    side, xn_ref, hidden_ref, own_ref, above_ref, below_ref, far_low_ref, far_high_ref, out_ref
-):
+    hidden = [hidden_of(pre_of(xn, ref)) for ref in whole]
+    hidden.append(hidden_of(far_pre(xn_ref)))
+    for t in range(out_ref.shape[1] // part):
+        cols = slice(t * part, (t + 1) * part)
+        down = jnp.dot(hidden[-1], far_columns(t), preferred_element_type=F32)
+        for n, ref in enumerate(whole):
+            down = down + jnp.dot(hidden[n], ref[2, :, cols], preferred_element_type=F32)
+        out_ref[:, cols] = down
+
+
+def far_kernel(side, xn_ref, near_ref, far_low_ref, far_high_ref, out_ref):
     peers, count, part = out_ref.shape
     tp = peers // side
-    half = far_low_ref.shape[2]
-    pre = pre_of(xn_ref[:, :half], far_low_ref) + pre_of(xn_ref[:, half:], far_high_ref)
-    hidden = [hidden_ref[n] for n in range(3)] + [hidden_of(pre)]
+    far_pre, far_columns = far_parts(far_low_ref, far_high_ref, part)
+    hidden = hidden_of(far_pre(xn_ref))
     for t in range(tp):
         cols = slice(t * part, (t + 1) * part)
-        if (t + 1) * part <= half:
-            far = far_low_ref[2, :, cols]
-        else:
-            far = far_high_ref[2, :, slice(t * part - half, (t + 1) * part - half)]
-        parts = (own_ref[2, :, cols], above_ref[2, :, cols], below_ref[2, :, cols], far)
-        down = jnp.dot(hidden[0], parts[0], preferred_element_type=F32)
-        for n in range(1, len(parts)):
-            down = down + jnp.dot(hidden[n], parts[n], preferred_element_type=F32)
+        down = near_ref[:, cols] + jnp.dot(hidden, far_columns(t), preferred_element_type=F32)
         down = down.astype(BF16)
         for x in range(side):
             out_ref[x * tp + t] = down[x * count : (x + 1) * count]
@@ -281,11 +298,12 @@
         ),
     )
     tiles = lax.all_to_all(tiles, "tp", 0, 0, tiled=True)
+    half_count = count // 2
     residual, blocks = pl.pallas_call(
         residual_kernel,
         out_shape=(
             pltpu.VMEM((count, part), BF16),
-            pltpu.VMEM((peers, count, part), BF16),
+            pltpu.VMEM((peers, half_count, part), BF16),
         ),
         in_specs=[VMEM, VMEM],
         out_specs=(VMEM, VMEM),
@@ -293,36 +311,52 @@
         name="residual",
     )(tiles, tokens)
 
-    blocks, above, below = lax.optimization_barrier((blocks, above, below))
+    blocks, own, above, below = lax.optimization_barrier((blocks, own, above, below))
     far_low = lax.ppermute(above[:, :, : width // 2], "kv", y_ring(1, side))
     far_high = lax.ppermute(below[:, :, width // 2 :], "kv", y_ring(-1, side))
+    partner = [(t, t ^ 1) for t in range(tp)]
+    own_2 = lax.ppermute(own, "tp", partner)
+    above_2 = lax.ppermute(above, "tp", partner)
+    below_2 = lax.ppermute(below, "tp", partner)
     tiles = lax.all_to_all(
         blocks, ("kv", "tp"), 0, 0, tiled=True, axis_index_groups=groups
     )
-    xn, hidden = pl.pallas_call(
-        functools.partial(near_kernel, side),
-        out_shape=(
-            pltpu.VMEM((side * count, width), BF16),
-            pltpu.VMEM((3, side * count, UNITS), BF16),
-        ),
-        in_specs=[VMEM] * 5,
-        out_specs=(VMEM, VMEM),
-        compiler_params=pltpu.CompilerParams(vmem_limit_bytes=16 << 20),
+    rows = side * half_count
+    xn = pl.pallas_call(
+        functools.partial(norm_kernel, side),
+        out_shape=pltpu.VMEM((rows, width), BF16),
+        in_specs=[VMEM] * 2,
+        out_specs=VMEM,
+        compiler_params=pltpu.CompilerParams(vmem_limit_bytes=4 << 20),
+        name="norm",
+    )(tiles, mlp_gain.reshape(1, width))
+    xn, far_low, far_high = lax.optimization_barrier((xn, far_low, far_high))
+    far_low_2 = lax.ppermute(far_low, "tp", partner)
+    far_high_2 = lax.ppermute(far_high, "tp", partner)
+    near = pl.pallas_call(
+        functools.partial(near_kernel, part),
+        out_shape=pltpu.VMEM((rows, width), F32),
+        in_specs=[VMEM] * 9,
+        out_specs=VMEM,
+        compiler_params=pltpu.CompilerParams(vmem_limit_bytes=8 << 20),
+        cost_estimate=pl.CostEstimate(
+            flops=8_000_000_000, bytes_accessed=8_000_000, transcendentals=0
+        ),
         name="near",
-    )(tiles, mlp_gain.reshape(1, width), *in_vmem(own, above, below))
+    )(xn, *in_vmem(own, above, below, own_2, above_2, below_2, far_low, far_high))
     tiles = pl.pallas_call(
         functools.partial(far_kernel, side),
-        out_shape=pltpu.VMEM((peers, count, part), BF16),
-        in_specs=[VMEM] * 7,
+        out_shape=pltpu.VMEM((peers, half_count, part), BF16),
+        in_specs=[VMEM] * 4,
         out_specs=VMEM,
-        compiler_params=pltpu.CompilerParams(vmem_limit_bytes=16 << 20),
+        compiler_params=pltpu.CompilerParams(vmem_limit_bytes=8 << 20),
         name="far",
-    )(xn, hidden, *in_vmem(own, above, below, far_low, far_high))
+    )(xn, near, *in_vmem(far_low_2, far_high_2))
     tiles = lax.all_to_all(
         tiles, ("kv", "tp"), 0, 0, tiled=True, axis_index_groups=groups
     )
-    down = jnp.sum(tiles.astype(F32), axis=0)
-    result = (residual.astype(F32) + down).astype(BF16)
+    tiles = tiles.astype(F32).reshape(peers // 2, count, part)
+    result = (residual.astype(F32) + jnp.sum(tiles, axis=0)).astype(BF16)
     return (result, new_state[:, None])
 
 

time: 101 us -> 85.9 us (0.85)
  waiting for transfers between devices: 13.4 us -> 0.03 us
  blocking collectives: 58.3 us -> 65.7 us
  starting transfers between devices: 12.7 us -> 7.81 us
  local copies, waits for them, and re-layouts: 3.85 us -> 0.8 us
    all_to_all x0 -> x1, blocking collectives: none -> 18.2 us  [body(): lax.all_to_all(blocks, ('kv', 'tp'), 0, 0, tiled=True, axis_index_groups=...]
    all_to_all x1 -> x0, waiting for transfers between devices: 12.7 us -> none  [body(): lax.all_to_all(blocks, ('kv', 'tp'), 0, 0, tiled=True, axis_index_groups=...]
    all_to_all x1, blocking collectives: 28.7 us -> 17.7 us  [body(): lax.all_to_all(tiles, ('kv', 'tp'), 0, 0, tiled=True, axis_index_groups=g...]
    all_to_all x1 -> x0, starting transfers between devices: 6.28 us -> none  [body(): lax.all_to_all(blocks, ('kv', 'tp'), 0, 0, tiled=True, axis_index_groups=...]
    ppermute x1, starting transfers between devices: 0.01 us -> 2.19 us  [body(): above = lax.ppermute(own, 'kv', y_ring(1, side))]
    ppermute x1, starting transfers between devices: 3.63 us -> 1.53 us  [body(): below = lax.ppermute(own, 'kv', y_ring(-1, side))]
    pallas_call x1, Pallas kernels: 2.66 us -> 0.75 us  [body(): pl.pallas_call(functools.partial(far_kernel, side), out_shape=pltpu.VMEM(...]
    unnamed x18 -> x12, local copies, waits for them, and re-layouts: 2.1 us -> 0.72 us
  transfers between devices with their start and end apart: 5 -> 9, of which waited for: 2 -> 0; matrix products, arithmetic and copies ran while one was open for 2% -> 0% of each run, Pallas kernels for 6% -> 8%
where the time goes in v4:
time: 85.9 us; the launch traced here: 85.6 us
  blocking collectives  65.7 us (76%)
  Pallas kernels  9.1 us (11%)
  starting transfers between devices  7.81 us (9%)
  between operations  1.43 us (2%)
    all_to_all x1, blocking collectives, body(): tiles = lax.all_to_all(copies, 'tp', 0, 0, tiled=True)  18.2 us
    all_to_all x1, blocking collectives, body(): lax.all_to_all(blocks, ('kv', 'tp'), 0, 0, tiled=True, axis_index_groups=...  18.2 us
    all_to_all x1, blocking collectives, body(): lax.all_to_all(tiles, ('kv', 'tp'), 0, 0, tiled=True, axis_index_groups=g...  17.7 us
    all_to_all x1, blocking collectives, body(): tiles = lax.all_to_all(tiles, 'tp', 0, 0, tiled=True)  11.6 us
    pallas_call x1, Pallas kernels, body(): pl.pallas_call(attention_kernel, out_shape=(pltpu.VMEM((tp, count, part),...  3.83 us
    pallas_call x1, Pallas kernels, body(): pl.pallas_call(functools.partial(near_kernel, part), out_shape=pltpu.VMEM...  3.02 us
    ppermute x1, starting transfers between devices, body(): far_high = lax.ppermute(below[:, :, width // 2:], 'kv', y_ring(-1, side))  2.59 us
    ppermute x1, starting transfers between devices, body(): above = lax.ppermute(own, 'kv', y_ring(1, side))  2.19 us
  transfers between devices with their start and end apart: 9, of which 0 were waited for; matrix products, arithmetic and copies ran while one was open for 0% of the time, Pallas kernels for 8%

profile of v4, /device:TPU:1, one launch (start us, length us, event | category | flops | bytes accessed | tf_op | source)
XLA Modules:
  0.0 85.6 jit_solution(7672355199467190078)
XLA Ops:
  1.3 0.0 copy-start
  1.3 0.7 copy-done
  2.0 1.3 %pack.1 = (bf16[3,48,4096]{2,1,0:T(8,128)(2,1)S(1)}, bf16[16,16,256]{2,1,0:T(8,128)(2,1)S(1)}, f32[1,128]{1,0:T(1,128)S(1)}) custom-call(f32[1]{0:T(128)S(6)} %copy.18.rate_ref, bf16[44,4096]{1,0:T(8,128)(2,1)} %bitcast.21, bf16[44,4096]{1,0:T(8,128)(2,1)} %bitcast.22, bf16[44,4096]{1,0:T(8,128)(2,1)} %bitcast.23, bf16[16,256]{1,0:T(8,128)(2,1)S(1)} %copy-done), custom_call_target="tpu_custom_call" | custom-call | tf_op jit(solution)/shard_map/pack/pallas_call | solution.py:247
  3.3 2.2 %collective-permute-start = (bf16[3,48,4096]{2,1,0:T(8,128)(2,1)S(1)}, bf16[3,48,4096]{2,1,0:T(8,128)(2,1)S(1)}, u32[]{:S(2)}, u32[]{:S(2)}) collective-permute-start(bf16[3,48,4096]{2,1,0:T(8,128)(2,1)S(1)} %get-tuple-element.26.refs_0_), channel_id=1, source_target_pairs={{0,64},{16,80},{32,96},{48,112},{64,128},{80,144},{96,160},{112,17... | collective-permute-start | bytes 3538952 | tf_op jit(solution)/shard_map/ppermute | solution.py:261
  5.5 1.5 %collective-permute-start.1 = (bf16[3,48,4096]{2,1,0:T(8,128)(2,1)S(1)}, bf16[3,48,4096]{2,1,0:T(8,128)(2,1)S(1)}, u32[]{:S(2)}, u32[]{:S(2)}) collective-permute-start(bf16[3,48,4096]{2,1,0:T(8,128)(2,1)S(1)} %get-tuple-element.26.refs_0_), channel_id=1, source_target_pairs={{0,192},{16,208},{32,224},{48,240},{64,0},{80,16},{96,32},{112,48}... | collective-permute-start | bytes 3538952 | tf_op jit(solution)/shard_map/ppermute | solution.py:262
  7.0 18.2 %all_to_all.20.tiles_ref = bf16[16,16,256]{2,1,0:T(8,128)(2,1)S(1)} all-to-all(bf16[16,16,256]{2,1,0:T(8,128)(2,1)S(1)} %get-tuple-element.16), channel_id=1, replica_groups=mesh['kv'=16,'tp'=16] {'tp'}, dimensions={0} | all-to-all | bytes 262144 | tf_op jit(solution)/shard_map/all_to_all | solution.py:263
  25.3 0.0 copy-start.1
  25.3 3.8 %attention.1 = (bf16[16,16,256]{2,1,0:T(8,128)(2,1)S(1)}, f32[16,128,128]{2,1,0:T(8,128)}) custom-call(bf16[16,16,256]{2,1,0:T(8,128)(2,1)S(1)} %all_to_all.20.tiles_ref, f32[1,4096]{1,0:T(1,128)S(1)} %bitcast.15, bf16[2,4096]{1,0:T(2,128)(2,1)S(1)} %bitcast.16, f32[1,128]{1,0:T(1,128)S(1)} %get-tuple-element.17.rate_ref, f32[1,128]{1,0:T(1,128)S(1)} %bitcast.18, ...), custom_call_target="tpu_custom_call" | custom-call | tf_op jit(solution)/shard_map/attention/pallas_call | solution.py:266
  29.1 11.6 %all_to_all.21.tiles_ref = bf16[16,16,256]{2,1,0:T(8,128)(2,1)S(1)} all-to-all(bf16[16,16,256]{2,1,0:T(8,128)(2,1)S(1)} %get-tuple-element.18), channel_id=1, replica_groups=mesh['kv'=16,'tp'=16] {'tp'}, dimensions={0} | all-to-all | bytes 262144 | tf_op jit(solution)/shard_map/all_to_all | solution.py:300
  40.8 0.0 copy-start.4
  40.8 0.1 collective-permute-start.5
  40.9 0.5 collective-permute-start.6
  41.4 0.1 collective-permute-start.4
  41.6 0.2 collective-permute-start.2
  41.7 2.6 %collective-permute-start.3 = (bf16[3,48,2048]{2,1,0:T(8,128)(2,1)S(1)}, bf16[3,48,2048]{2,1,0:T(8,128)(2,1)S(1)}, u32[]{:S(2)}, u32[]{:S(2)}) collective-permute-start(bf16[3,48,2048]{2,1,0:T(8,128)(2,1)S(1)} %slice.7), channel_id=1, source_target_pairs={{0,192},{16,208},{32,224},{48,240},{64,0},{80,16},{96,32},{112,48}... | collective-permute-start | bytes 1769480 | tf_op jit(solution)/shard_map/ppermute | solution.py:316
  44.3 18.2 %all_to_all.22.tiles_ref = bf16[64,8,256]{2,1,0:T(8,128)(2,1)S(1)} all-to-all(bf16[64,8,256]{2,1,0:T(8,128)(2,1)S(1)} %get-tuple-element.22), channel_id=1, replica_groups={{0,1,2,3,4,5,6,7,8,9,10,11,12,13,14,15,16,17,18,19,20,21,22,23,24,25,26..., dimensions={0} | all-to-all | bytes 524288 | tf_op jit(solution)/shard_map/all_to_all | solution.py:321
  62.5 0.2 norm.1.xn_ref
  62.7 0.5 collective-permute-start.7
  63.3 0.1 collective-permute-start.8
  63.4 3.0 %near.1.near_ref = f32[32,4096]{1,0:T(8,128)S(1)} custom-call(bf16[32,4096]{1,0:T(8,128)(2,1)S(1)} %norm.1.xn_ref, bf16[3,48,4096]{2,1,0:T(8,128)(2,1)S(1)} %get-tuple-element.26.refs_0_, bf16[3,48,4096]{2,1,0:T(8,128)(2,1)S(1)} %collective-permute-done.refs_1_, bf16[3,48,4096]{2,1,0:T(8,128)(2,1)S(1)} %collective-permute-done.1.refs_2_, ...), custom_call_target="tpu_custom_call" | custom-call | flops 8000000000 | bytes 8000000 | tf_op jit(solution)/shard_map/near/pallas_call | solution.py:336
  66.4 0.0 collective-permute-done.8.far_high_ref
  66.4 0.8 far.1
  67.2 17.7 %all_to_all.23 = bf16[64,8,256]{2,1,0:T(8,128)(2,1)S(1)} all-to-all(bf16[64,8,256]{2,1,0:T(8,128)(2,1)S(1)} %far.1), channel_id=1, replica_groups={{0,1,2,3,4,5,6,7,8,9,10,11,12,13,14,15,16,17,18,19,20,21,22,23,24,25,26..., dimensions={0} | all-to-all | bytes 524288 | tf_op jit(solution)/shard_map/all_to_all | solution.py:355
  85.0 0.6 add_convert_fusion
  (20 shorter events, 0.2 us)
Async XLA Ops:
  0.6 24.6 %copy-start.5 = (f32[128]{0:T(128)S(1)}, f32[128]{0:T(128)}, u32[]{:S(2)}) copy-start(f32[128]{0:T(128)} %param.23) | copy-start | bytes 1540
  1.3 0.7 copy-start
  2.0 23.3 %copy-start.2 = (f32[4096]{0:T(1024)S(1)}, f32[4096]{0:T(1024)}, u32[]{:S(2)}) copy-start(f32[4096]{0:T(1024)} %param.16) | copy-start | bytes 49156
  2.0 23.3 %copy-start.3 = (bf16[2,4096,1]{1,0,2:T(2,128)(2,1)S(1)}, bf16[2,4096,1]{1,0,2:T(2,128)(2,1)}, u32[]{:S(2)}) copy-start(bf16[2,4096,1]{1,0,2:T(2,128)(2,1)} %param.21) | copy-start | bytes 49156
  3.3 37.4 %collective-permute-start = (bf16[3,48,4096]{2,1,0:T(8,128)(2,1)S(1)}, bf16[3,48,4096]{2,1,0:T(8,128)(2,1)S(1)}, u32[]{:S(2)}, u32[]{:S(2)}) collective-permute-start(bf16[3,48,4096]{2,1,0:T(8,128)(2,1)S(1)} %get-tuple-element.26.refs_0_), channel_id=1, source_target_pairs={{0,64},{16,80},{32,96},{48,112},{64,128},{80,144},{96,160},{112,17... | collective-permute-start | bytes 3538952 | tf_op jit(solution)/shard_map/ppermute | solution.py:261
  5.5 35.2 %collective-permute-start.1 = (bf16[3,48,4096]{2,1,0:T(8,128)(2,1)S(1)}, bf16[3,48,4096]{2,1,0:T(8,128)(2,1)S(1)}, u32[]{:S(2)}, u32[]{:S(2)}) collective-permute-start(bf16[3,48,4096]{2,1,0:T(8,128)(2,1)S(1)} %get-tuple-element.26.refs_0_), channel_id=1, source_target_pairs={{0,192},{16,208},{32,224},{48,240},{64,0},{80,16},{96,32},{112,48}... | collective-permute-start | bytes 3538952 | tf_op jit(solution)/shard_map/ppermute | solution.py:262
  25.3 15.4 %copy-start.1 = (bf16[16,256]{1,0:T(8,128)(2,1)S(1)}, bf16[16,256]{1,0:T(8,128)(2,1)}, u32[]{:S(2)}) copy-start(bf16[16,256]{1,0:T(8,128)(2,1)} %tokens_ref.3) | copy-start | bytes 24580
  40.8 21.8 %copy-start.4 = (f32[4096]{0:T(1024)S(1)}, f32[4096]{0:T(1024)}, u32[]{:S(2)}) copy-start(f32[4096]{0:T(1024)} %param.26) | copy-start | bytes 49156
  40.8 22.6 %collective-permute-start.5 = (bf16[3,48,4096]{2,1,0:T(8,128)(2,1)S(1)}, bf16[3,48,4096]{2,1,0:T(8,128)(2,1)S(1)}, u32[]{:S(2)}, u32[]{:S(2)}) collective-permute-start(bf16[3,48,4096]{2,1,0:T(8,128)(2,1)S(1)} %collective-permute-done.refs_1_), channel_id=1, source_target_pairs={{0,1},{1,0},{2,3},{3,2},{4,5},{5,4},{6,7},{7,6},{8,9},{9,8},{10,11... | collective-permute-start | bytes 3538952 | tf_op jit(solution)/shard_map/ppermute | solution.py:319
  40.9 22.5 %collective-permute-start.6 = (bf16[3,48,4096]{2,1,0:T(8,128)(2,1)S(1)}, bf16[3,48,4096]{2,1,0:T(8,128)(2,1)S(1)}, u32[]{:S(2)}, u32[]{:S(2)}) collective-permute-start(bf16[3,48,4096]{2,1,0:T(8,128)(2,1)S(1)} %collective-permute-done.1.refs_2_), channel_id=1, source_target_pairs={{0,1},{1,0},{2,3},{3,2},{4,5},{5,4},{6,7},{7,6},{8,9},{9,8},{10,11... | collective-permute-start | bytes 3538952 | tf_op jit(solution)/shard_map/ppermute | solution.py:320
  41.4 22.0 %collective-permute-start.4 = (bf16[3,48,4096]{2,1,0:T(8,128)(2,1)S(1)}, bf16[3,48,4096]{2,1,0:T(8,128)(2,1)S(1)}, u32[]{:S(2)}, u32[]{:S(2)}) collective-permute-start(bf16[3,48,4096]{2,1,0:T(8,128)(2,1)S(1)} %get-tuple-element.26.refs_0_), channel_id=1, source_target_pairs={{0,1},{1,0},{2,3},{3,2},{4,5},{5,4},{6,7},{7,6},{8,9},{9,8},{10,11... | collective-permute-start | bytes 3538952 | tf_op jit(solution)/shard_map/ppermute | solution.py:318
  41.6 21.1 %collective-permute-start.2 = (bf16[3,48,2048]{2,1,0:T(8,128)(2,1)S(1)}, bf16[3,48,2048]{2,1,0:T(8,128)(2,1)S(1)}, u32[]{:S(2)}, u32[]{:S(2)}) collective-permute-start(bf16[3,48,2048]{2,1,0:T(8,128)(2,1)S(1)} %slice.6), channel_id=1, source_target_pairs={{0,64},{16,80},{32,96},{48,112},{64,128},{80,144},{96,160},{112,17... | collective-permute-start | bytes 1769480 | tf_op jit(solution)/shard_map/ppermute | solution.py:315
  41.7 21.0 %collective-permute-start.3 = (bf16[3,48,2048]{2,1,0:T(8,128)(2,1)S(1)}, bf16[3,48,2048]{2,1,0:T(8,128)(2,1)S(1)}, u32[]{:S(2)}, u32[]{:S(2)}) collective-permute-start(bf16[3,48,2048]{2,1,0:T(8,128)(2,1)S(1)} %slice.7), channel_id=1, source_target_pairs={{0,192},{16,208},{32,224},{48,240},{64,0},{80,16},{96,32},{112,48}... | collective-permute-start | bytes 1769480 | tf_op jit(solution)/shard_map/ppermute | solution.py:316
  62.7 3.7 %collective-permute-start.7 = (bf16[3,48,2048]{2,1,0:T(8,128)(2,1)S(1)}, bf16[3,48,2048]{2,1,0:T(8,128)(2,1)S(1)}, u32[]{:S(2)}, u32[]{:S(2)}) collective-permute-start(bf16[3,48,2048]{2,1,0:T(8,128)(2,1)S(1)} %collective-permute-done.2.refs_6_), channel_id=1, source_target_pairs={{0,1},{1,0},{2,3},{3,2},{4,5},{5,4},{6,7},{7,6},{8,9},{9,8},{10,11... | collective-permute-start | bytes 1769480 | tf_op jit(solution)/shard_map/ppermute | solution.py:334
  63.3 3.1 %collective-permute-start.8 = (bf16[3,48,2048]{2,1,0:T(8,128)(2,1)S(1)}, bf16[3,48,2048]{2,1,0:T(8,128)(2,1)S(1)}, u32[]{:S(2)}, u32[]{:S(2)}) collective-permute-start(bf16[3,48,2048]{2,1,0:T(8,128)(2,1)S(1)} %collective-permute-done.3.refs_7_), channel_id=1, source_target_pairs={{0,1},{1,0},{2,3},{3,2},{4,5},{5,4},{6,7},{7,6},{8,9},{9,8},{10,11... | collective-permute-start | bytes 1769480 | tf_op jit(solution)/shard_map/ppermute | solution.py:335

commit v5 on v4

--- a/solution.py
+++ b/solution.py
@@ -54,33 +54,15 @@
 
 
 def attention_kernel(
-    tiles_ref, gain_ref, wr_ref, rate_ref, head_gain_ref, wq_hbm, wk_hbm, wv_hbm, wg_hbm, wo_hbm,
-    state_hbm, out_ref, new_state_hbm, xn_ref, u_ref, w_ref, wq_ref, wk_ref, wv_ref, wg_ref,
-    wo_ref, state_ref, new_state_ref, sems, out_sems,
+    tiles_ref, gain_ref, wr_ref, rate_ref, head_gain_ref, wq_ref, wk_ref, wv_ref, wg_ref, wo_ref,
+    state_ref, out_ref, new_state_hbm, xn_ref, u_ref, w_ref, new_state_ref, out_sems,
 ):
     tp, count, part = tiles_ref.shape
     size = wq_ref.shape[1]
-    loads = [
-        pltpu.make_async_copy(source, target, sems.at[n])
-        for n, (source, target) in enumerate(
-            (
-                (wq_hbm, wq_ref),
-                (wk_hbm, wk_ref),
-                (state_hbm, state_ref),
-                (wv_hbm, wv_ref),
-                (wg_hbm, wg_ref),
-                (wo_hbm, wo_ref),
-            )
-        )
-    ]
-    for load in loads:
-        load.start()
     norm_rows(tiles_ref, 0, tp, gain_ref, xn_ref, 0)
     xn = xn_ref[...]
     rates = lax.dot_general(xn, wr_ref[...], NT, preferred_element_type=F32)
-    loads[0].wait()
     query = jnp.dot(xn, wq_ref[...], preferred_element_type=F32)
-    loads[1].wait()
     key = jnp.dot(xn, wk_ref[...], preferred_element_type=F32)
     strength = 1.0 / (1.0 + jnp.exp(-rates[:, 0:1]))
     decay = rates[:, 1:2]
@@ -92,16 +74,13 @@
     q_low = (q - q_high.astype(F32)).astype(BF16)
     k_low = (k - k_high.astype(F32)).astype(BF16)
     probes = jnp.concatenate([k_high, k_low, q_high, q_low], axis=0)
-    loads[2].wait()
     for b in range(count):
         read = jnp.dot(probes, state_ref[b].astype(BF16), preferred_element_type=F32)
         u_ref[b : b + 1, :] = read[b : b + 1] + read[count + b : count + b + 1]
         w_ref[b : b + 1, :] = read[2 * count + b : 2 * count + b + 1] + read[
             3 * count + b : 3 * count + b + 1
         ]
-    loads[3].wait()
     value = jnp.dot(xn, wv_ref[...], preferred_element_type=F32)
-    loads[4].wait()
     gate_in = jnp.dot(xn, wg_ref[...], preferred_element_type=F32)
     fresh = strength * (value - fade * u_ref[...])
     readout = fade * w_ref[...] + jnp.sum(q * k, -1, keepdims=True) * fresh
@@ -121,7 +100,6 @@
             stores[-1].start()
     scale = lax.rsqrt(jnp.mean(readout * readout, -1, keepdims=True) + EPS)
     mixed = (readout * scale * head_gain_ref[...] * silu(gate_in)).astype(BF16)
-    loads[5].wait()
     for t in range(tp):
         cols = slice(t * part, (t + 1) * part)
         out_ref[t] = jnp.dot(mixed, wo_ref[:, cols], preferred_element_type=F32).astype(BF16)
@@ -142,24 +120,31 @@
 
 
 def pack_kernel(
-    rate_ref, gate_ref, up_ref, down_ref, tokens_ref, own_ref, copies_ref, rate_row_ref,
-    gate_at, up_at, down_at, sems,
+    rate_ref, gate_hbm, up_hbm, down_hbm, tokens_hbm, own_ref, rate_row_ref, tokens_ref,
+    gate_ref, up_ref, down_ref, sems,
 ):
     units = gate_ref.shape[0]
-    landed = (gate_at, up_at, down_at)
-    moves = [
-        pltpu.make_async_copy(ref, at, sems.at[n])
-        for n, (ref, at) in enumerate(zip((gate_ref, up_ref, down_ref), landed))
+    landed = (tokens_ref, gate_ref, up_ref, down_ref)
+    loads = [
+        pltpu.make_async_copy(source, at, sems.at[n])
+        for n, (source, at) in enumerate(
+            zip((tokens_hbm, gate_hbm, up_hbm, down_hbm), landed)
+        )
     ]
-    for move in moves:
-        move.start()
+    for load in loads:
+        load.start()
+    for n in range(3):
+        own_ref[n, units:, :] = jnp.zeros((UNITS - units, own_ref.shape[2]), BF16)
+    rate_row_ref[...] = jnp.full(rate_row_ref.shape, rate_ref[0], F32)
+    for n in range(3):
+        loads[1 + n].wait()
+        own_ref[n, 0:units, :] = landed[1 + n][...]
+    loads[0].wait()
+
+
+def spread_kernel(tokens_ref, copies_ref):
     for b in range(copies_ref.shape[0]):
         copies_ref[b] = tokens_ref[...]
-    rate_row_ref[...] = jnp.full(rate_row_ref.shape, rate_ref[0], F32)
-    for n, (move, at) in enumerate(zip(moves, landed)):
-        move.wait()
-        own_ref[n, 0:units, :] = at[...]
-        own_ref[n, units:, :] = jnp.zeros((UNITS - units, own_ref.shape[2]), BF16)
 
 
 def pre_of(xn, ref):
@@ -244,24 +229,34 @@
     peers = side * tp
     groups = plane_groups(side, tp)
 
-    own, copies, rate_row = pl.pallas_call(
+    own, rate_row, kept = pl.pallas_call(
         pack_kernel,
         out_shape=(
             pltpu.VMEM((3, UNITS, width), BF16),
-            pltpu.VMEM((tp, count, part), BF16),
             pltpu.VMEM((1, size), F32),
-        ),
-        in_specs=[SMEM] + [HBM] * 3 + [VMEM],
+            pltpu.VMEM((count, part), BF16),
+        ),
+        in_specs=[SMEM] + [HBM] * 4,
         out_specs=(VMEM, VMEM, VMEM),
         scratch_shapes=[pltpu.VMEM((w_gate.shape[1], width), BF16)] * 3
-        + [pltpu.SemaphoreType.DMA((3,))],
+        + [pltpu.SemaphoreType.DMA((4,))],
         compiler_params=pltpu.CompilerParams(vmem_limit_bytes=4 << 20),
         name="pack",
-    )(head_rate, *in_hbm(w_gate.T, w_up.T, w_down.T), tokens)
+    )(head_rate, *in_hbm(w_gate.T, w_up.T, w_down.T, tokens))
     above = lax.ppermute(own, "kv", y_ring(1, side))
     below = lax.ppermute(own, "kv", y_ring(-1, side))
+    copies = pl.pallas_call(
+        spread_kernel,
+        out_shape=pltpu.VMEM((tp, count, part), BF16),
+        in_specs=[VMEM],
+        out_specs=VMEM,
+        compiler_params=pltpu.CompilerParams(vmem_limit_bytes=1 << 20),
+        cost_estimate=pl.CostEstimate(
+            flops=20_000_000_000, bytes_accessed=200_000, transcendentals=0
+        ),
+        name="spread",
+    )(kept)
     tiles = lax.all_to_all(copies, "tp", 0, 0, tiled=True)
-    weight = pltpu.VMEM((width, size), BF16)
     states = pltpu.VMEM((count, size, size), F32)
     tiles, new_state = pl.pallas_call(
         attention_kernel,
@@ -269,20 +264,13 @@
             pltpu.VMEM((tp, count, part), BF16),
             pltpu.HBM((count, size, size), F32),
         ),
-        in_specs=[VMEM] * 5 + [HBM] * 6,
+        in_specs=[VMEM] * 11,
         out_specs=(VMEM, HBM),
         scratch_shapes=[
             pltpu.VMEM((count, width), BF16),
             pltpu.VMEM((count, size), F32),
             pltpu.VMEM((count, size), F32),
-            weight,
-            weight,
-            weight,
-            weight,
-            pltpu.VMEM((size, width), BF16),
             states,
-            states,
-            pltpu.SemaphoreType.DMA((6,)),
             pltpu.SemaphoreType.DMA((4,)),
         ],
         compiler_params=pltpu.CompilerParams(vmem_limit_bytes=16 << 20),
@@ -293,7 +281,7 @@
         w_rates.reshape(2, width),
         rate_row,
         head_gain.reshape(1, size),
-        *in_hbm(
+        *in_vmem(
             w_query, w_key, w_value, w_outgate, w_out, state.reshape(count, size, size)
         ),
     )
@@ -309,7 +297,7 @@
         out_specs=(VMEM, VMEM),
         compiler_params=pltpu.CompilerParams(vmem_limit_bytes=4 << 20),
         name="residual",
-    )(tiles, tokens)
+    )(tiles, kept)
 
     blocks, own, above, below = lax.optimization_barrier((blocks, own, above, below))
     far_low = lax.ppermute(above[:, :, : width // 2], "kv", y_ring(1, side))

time: 85.9 us -> 83.8 us (0.976)
  Pallas kernels: 9.1 us -> 7.39 us
    pallas_call x1, Pallas kernels: 3.83 us -> 2.13 us  [body(): pl.pallas_call(attention_kernel, out_shape=(pltpu.VMEM((tp, count, part),...]
  transfers between devices with their start and end apart: 9 -> 9, of which waited for: 0 -> 0; matrix products, arithmetic and copies ran while one was open for 0% -> 0% of each run, Pallas kernels for 8% -> 6%
where the time goes in v5:
time: 83.8 us; the launch traced here: 83.5 us
  blocking collectives  66 us (79%)
  starting transfers between devices  7.81 us (9%)
  Pallas kernels  7.39 us (9%)
  between operations  1.49 us (2%)
    all_to_all x1, blocking collectives, body(): tiles = lax.all_to_all(copies, 'tp', 0, 0, tiled=True)  18.5 us
    all_to_all x1, blocking collectives, body(): lax.all_to_all(blocks, ('kv', 'tp'), 0, 0, tiled=True, axis_index_groups=...  18.2 us
    all_to_all x1, blocking collectives, body(): lax.all_to_all(tiles, ('kv', 'tp'), 0, 0, tiled=True, axis_index_groups=g...  17.7 us
    all_to_all x1, blocking collectives, body(): tiles = lax.all_to_all(tiles, 'tp', 0, 0, tiled=True)  11.6 us
    pallas_call x1, Pallas kernels, body(): pl.pallas_call(functools.partial(near_kernel, part), out_shape=pltpu.VMEM...  2.99 us
    ppermute x1, starting transfers between devices, body(): far_high = lax.ppermute(below[:, :, width // 2:], 'kv', y_ring(-1, side))  2.59 us
    ppermute x1, starting transfers between devices, body(): above = lax.ppermute(own, 'kv', y_ring(1, side))  2.19 us
    pallas_call x1, Pallas kernels, body(): pl.pallas_call(attention_kernel, out_shape=(pltpu.VMEM((tp, count, part),...  2.13 us
  transfers between devices with their start and end apart: 9, of which 0 were waited for; matrix products, arithmetic and copies ran while one was open for 0% of the time, Pallas kernels for 6%

profile of v5, /device:TPU:1, one launch (start us, length us, event | category | flops | bytes accessed | tf_op | source)
XLA Modules:
  0.0 83.5 jit_solution(17001316525234596699)
XLA Ops:
  1.3 1.3 %pack.1 = (bf16[3,48,4096]{2,1,0:T(8,128)(2,1)S(1)}, f32[1,128]{1,0:T(1,128)S(1)}, bf16[16,256]{1,0:T(8,128)(2,1)S(1)}) custom-call(f32[1]{0:T(128)S(6)} %copy.18.rate_ref, bf16[44,4096]{1,0:T(8,128)(2,1)} %bitcast.21, bf16[44,4096]{1,0:T(8,128)(2,1)} %bitcast.22, bf16[44,4096]{1,0:T(8,128)(2,1)} %bitcast.23, bf16[16,256]{1,0:T(8,128)(2,1)} %tokens_hbm.1), custom_call_target="tpu_custom_call" | custom-call | tf_op jit(solution)/shard_map/pack/pallas_call | solution.py:232
  2.6 2.2 %collective-permute-start = (bf16[3,48,4096]{2,1,0:T(8,128)(2,1)S(1)}, bf16[3,48,4096]{2,1,0:T(8,128)(2,1)S(1)}, u32[]{:S(2)}, u32[]{:S(2)}) collective-permute-start(bf16[3,48,4096]{2,1,0:T(8,128)(2,1)S(1)} %get-tuple-element.26.refs_0_), channel_id=1, source_target_pairs={{0,64},{16,80},{32,96},{48,112},{64,128},{80,144},{96,160},{112,17... | collective-permute-start | bytes 3538952 | tf_op jit(solution)/shard_map/ppermute | solution.py:246
  4.8 1.5 %collective-permute-start.1 = (bf16[3,48,4096]{2,1,0:T(8,128)(2,1)S(1)}, bf16[3,48,4096]{2,1,0:T(8,128)(2,1)S(1)}, u32[]{:S(2)}, u32[]{:S(2)}) collective-permute-start(bf16[3,48,4096]{2,1,0:T(8,128)(2,1)S(1)} %get-tuple-element.26.refs_0_), channel_id=1, source_target_pairs={{0,192},{16,208},{32,224},{48,240},{64,0},{80,16},{96,32},{112,48}... | collective-permute-start | bytes 3538952 | tf_op jit(solution)/shard_map/ppermute | solution.py:247
  6.3 0.0 copy-start.4
  6.4 0.0 copy-start.6
  6.4 0.0 copy-start.7
  6.4 18.5 %all_to_all.20.tiles_ref = bf16[16,16,256]{2,1,0:T(8,128)(2,1)S(1)} all-to-all(bf16[16,16,256]{2,1,0:T(8,128)(2,1)S(1)} %spread.1), channel_id=1, replica_groups=mesh['kv'=16,'tp'=16] {'tp'}, dimensions={0} | all-to-all | bytes 262144 | tf_op jit(solution)/shard_map/all_to_all | solution.py:259
  25.0 2.1 %attention.1 = (bf16[16,16,256]{2,1,0:T(8,128)(2,1)S(1)}, f32[16,128,128]{2,1,0:T(8,128)}) custom-call(bf16[16,16,256]{2,1,0:T(8,128)(2,1)S(1)} %all_to_all.20.tiles_ref, f32[1,4096]{1,0:T(1,128)S(1)} %bitcast.16, bf16[2,4096]{1,0:T(2,128)(2,1)S(1)} %bitcast.17, f32[1,128]{1,0:T(1,128)S(1)} %get-tuple-element.17.rate_ref, f32[1,128]{1,0:T(1,128)S(1)} %bitcast.19, ...), custom_call_target="tpu_custom_call" | custom-call | tf_op jit(solution)/shard_map/attention/pallas_call | solution.py:261
  27.1 11.6 %all_to_all.21.tiles_ref = bf16[16,16,256]{2,1,0:T(8,128)(2,1)S(1)} all-to-all(bf16[16,16,256]{2,1,0:T(8,128)(2,1)S(1)} %get-tuple-element.18), channel_id=1, replica_groups=mesh['kv'=16,'tp'=16] {'tp'}, dimensions={0} | all-to-all | bytes 262144 | tf_op jit(solution)/shard_map/all_to_all | solution.py:288
  38.7 0.0 copy-start.8
  38.8 0.1 collective-permute-start.5
  38.9 0.5 collective-permute-start.6
  39.4 0.1 collective-permute-start.4
  39.5 0.2 collective-permute-start.2
  39.7 2.6 %collective-permute-start.3 = (bf16[3,48,2048]{2,1,0:T(8,128)(2,1)S(1)}, bf16[3,48,2048]{2,1,0:T(8,128)(2,1)S(1)}, u32[]{:S(2)}, u32[]{:S(2)}) collective-permute-start(bf16[3,48,2048]{2,1,0:T(8,128)(2,1)S(1)} %slice.7), channel_id=1, source_target_pairs={{0,192},{16,208},{32,224},{48,240},{64,0},{80,16},{96,32},{112,48}... | collective-permute-start | bytes 1769480 | tf_op jit(solution)/shard_map/ppermute | solution.py:304
  42.3 18.2 %all_to_all.22.tiles_ref = bf16[64,8,256]{2,1,0:T(8,128)(2,1)S(1)} all-to-all(bf16[64,8,256]{2,1,0:T(8,128)(2,1)S(1)} %get-tuple-element.22), channel_id=1, replica_groups={{0,1,2,3,4,5,6,7,8,9,10,11,12,13,14,15,16,17,18,19,20,21,22,23,24,25,26..., dimensions={0} | all-to-all | bytes 524288 | tf_op jit(solution)/shard_map/all_to_all | solution.py:309
  60.5 0.2 norm.1.xn_ref
  60.7 0.5 collective-permute-start.7
  61.2 0.1 collective-permute-start.8
  61.4 3.0 %near.1.near_ref = f32[32,4096]{1,0:T(8,128)S(1)} custom-call(bf16[32,4096]{1,0:T(8,128)(2,1)S(1)} %norm.1.xn_ref, bf16[3,48,4096]{2,1,0:T(8,128)(2,1)S(1)} %get-tuple-element.26.refs_0_, bf16[3,48,4096]{2,1,0:T(8,128)(2,1)S(1)} %collective-permute-done.refs_1_, bf16[3,48,4096]{2,1,0:T(8,128)(2,1)S(1)} %collective-permute-done.1.refs_2_, ...), custom_call_target="tpu_custom_call" | custom-call | flops 8000000000 | bytes 8000000 | tf_op jit(solution)/shard_map/near/pallas_call | solution.py:324
  64.3 0.0 collective-permute-done.8.far_high_ref
  64.4 0.8 far.1
  65.1 17.7 %all_to_all.23 = bf16[64,8,256]{2,1,0:T(8,128)(2,1)S(1)} all-to-all(bf16[64,8,256]{2,1,0:T(8,128)(2,1)S(1)} %far.1), channel_id=1, replica_groups={{0,1,2,3,4,5,6,7,8,9,10,11,12,13,14,15,16,17,18,19,20,21,22,23,24,25,26..., dimensions={0} | all-to-all | bytes 524288 | tf_op jit(solution)/shard_map/all_to_all | solution.py:343
  82.9 0.6 add_convert_fusion
  (29 shorter events, 0.2 us)
Async XLA Ops:
  2.6 36.1 %collective-permute-start = (bf16[3,48,4096]{2,1,0:T(8,128)(2,1)S(1)}, bf16[3,48,4096]{2,1,0:T(8,128)(2,1)S(1)}, u32[]{:S(2)}, u32[]{:S(2)}) collective-permute-start(bf16[3,48,4096]{2,1,0:T(8,128)(2,1)S(1)} %get-tuple-element.26.refs_0_), channel_id=1, source_target_pairs={{0,64},{16,80},{32,96},{48,112},{64,128},{80,144},{96,160},{112,17... | collective-permute-start | bytes 3538952 | tf_op jit(solution)/shard_map/ppermute | solution.py:246
  4.8 33.9 %collective-permute-start.1 = (bf16[3,48,4096]{2,1,0:T(8,128)(2,1)S(1)}, bf16[3,48,4096]{2,1,0:T(8,128)(2,1)S(1)}, u32[]{:S(2)}, u32[]{:S(2)}) collective-permute-start(bf16[3,48,4096]{2,1,0:T(8,128)(2,1)S(1)} %get-tuple-element.26.refs_0_), channel_id=1, source_target_pairs={{0,192},{16,208},{32,224},{48,240},{64,0},{80,16},{96,32},{112,48}... | collective-permute-start | bytes 3538952 | tf_op jit(solution)/shard_map/ppermute | solution.py:247
  6.3 18.6 %copy-start = (bf16[4096,128]{1,0:T(8,128)(2,1)S(1)}, bf16[4096,128]{1,0:T(8,128)(2,1)}, u32[]{:S(2)}) copy-start(bf16[4096,128]{1,0:T(8,128)(2,1)} %wq_ref.1) | copy-start | bytes 3145732
  6.3 18.6 %copy-start.1 = (bf16[4096,128]{1,0:T(8,128)(2,1)S(1)}, bf16[4096,128]{1,0:T(8,128)(2,1)}, u32[]{:S(2)}) copy-start(bf16[4096,128]{1,0:T(8,128)(2,1)} %wk_ref.1) | copy-start | bytes 3145732
  6.3 18.6 %copy-start.2 = (bf16[4096,128]{1,0:T(8,128)(2,1)S(1)}, bf16[4096,128]{1,0:T(8,128)(2,1)}, u32[]{:S(2)}) copy-start(bf16[4096,128]{1,0:T(8,128)(2,1)} %wv_ref.1) | copy-start | bytes 3145732
  6.3 18.6 %copy-start.3 = (bf16[4096,128]{1,0:T(8,128)(2,1)S(1)}, bf16[4096,128]{1,0:T(8,128)(2,1)}, u32[]{:S(2)}) copy-start(bf16[4096,128]{1,0:T(8,128)(2,1)} %wg_ref.1) | copy-start | bytes 3145732
  6.3 18.6 %copy-start.4 = (bf16[128,4096]{1,0:T(8,128)(2,1)S(1)}, bf16[128,4096]{1,0:T(8,128)(2,1)}, u32[]{:S(2)}) copy-start(bf16[128,4096]{1,0:T(8,128)(2,1)} %wo_ref.1) | copy-start | bytes 3145732
  6.3 18.6 %copy-start.5 = (f32[16,1,128,128]{3,2,1,0:T(8,128)S(1)}, f32[16,1,128,128]{3,2,1,0:T(8,128)}, u32[]{:S(2)}) copy-start(f32[16,1,128,128]{3,2,1,0:T(8,128)} %param.25) | copy-start | bytes 3145732
  6.4 18.6 %copy-start.6 = (f32[4096]{0:T(1024)S(1)}, f32[4096]{0:T(1024)}, u32[]{:S(2)}) copy-start(f32[4096]{0:T(1024)} %param.16) | copy-start | bytes 49156
  6.4 18.6 %copy-start.7 = (bf16[2,4096,1]{1,0,2:T(2,128)(2,1)S(1)}, bf16[2,4096,1]{1,0,2:T(2,128)(2,1)}, u32[]{:S(2)}) copy-start(bf16[2,4096,1]{1,0,2:T(2,128)(2,1)} %param.21) | copy-start | bytes 49156
  6.4 18.6 %copy-start.9 = (f32[128]{0:T(128)S(1)}, f32[128]{0:T(128)}, u32[]{:S(2)}) copy-start(f32[128]{0:T(128)} %param.23) | copy-start | bytes 1540
  38.7 21.8 %copy-start.8 = (f32[4096]{0:T(1024)S(1)}, f32[4096]{0:T(1024)}, u32[]{:S(2)}) copy-start(f32[4096]{0:T(1024)} %param.26) | copy-start | bytes 49156
  38.8 22.6 %collective-permute-start.5 = (bf16[3,48,4096]{2,1,0:T(8,128)(2,1)S(1)}, bf16[3,48,4096]{2,1,0:T(8,128)(2,1)S(1)}, u32[]{:S(2)}, u32[]{:S(2)}) collective-permute-start(bf16[3,48,4096]{2,1,0:T(8,128)(2,1)S(1)} %collective-permute-done.refs_1_), channel_id=1, source_target_pairs={{0,1},{1,0},{2,3},{3,2},{4,5},{5,4},{6,7},{7,6},{8,9},{9,8},{10,11... | collective-permute-start | bytes 3538952 | tf_op jit(solution)/shard_map/ppermute | solution.py:307
  38.9 22.5 %collective-permute-start.6 = (bf16[3,48,4096]{2,1,0:T(8,128)(2,1)S(1)}, bf16[3,48,4096]{2,1,0:T(8,128)(2,1)S(1)}, u32[]{:S(2)}, u32[]{:S(2)}) collective-permute-start(bf16[3,48,4096]{2,1,0:T(8,128)(2,1)S(1)} %collective-permute-done.1.refs_2_), channel_id=1, source_target_pairs={{0,1},{1,0},{2,3},{3,2},{4,5},{5,4},{6,7},{7,6},{8,9},{9,8},{10,11... | collective-permute-start | bytes 3538952 | tf_op jit(solution)/shard_map/ppermute | solution.py:308
  39.4 22.0 %collective-permute-start.4 = (bf16[3,48,4096]{2,1,0:T(8,128)(2,1)S(1)}, bf16[3,48,4096]{2,1,0:T(8,128)(2,1)S(1)}, u32[]{:S(2)}, u32[]{:S(2)}) collective-permute-start(bf16[3,48,4096]{2,1,0:T(8,128)(2,1)S(1)} %get-tuple-element.26.refs_0_), channel_id=1, source_target_pairs={{0,1},{1,0},{2,3},{3,2},{4,5},{5,4},{6,7},{7,6},{8,9},{9,8},{10,11... | collective-permute-start | bytes 3538952 | tf_op jit(solution)/shard_map/ppermute | solution.py:306
  39.5 21.1 %collective-permute-start.2 = (bf16[3,48,2048]{2,1,0:T(8,128)(2,1)S(1)}, bf16[3,48,2048]{2,1,0:T(8,128)(2,1)S(1)}, u32[]{:S(2)}, u32[]{:S(2)}) collective-permute-start(bf16[3,48,2048]{2,1,0:T(8,128)(2,1)S(1)} %slice.6), channel_id=1, source_target_pairs={{0,64},{16,80},{32,96},{48,112},{64,128},{80,144},{96,160},{112,17... | collective-permute-start | bytes 1769480 | tf_op jit(solution)/shard_map/ppermute | solution.py:303
  39.7 21.0 %collective-permute-start.3 = (bf16[3,48,2048]{2,1,0:T(8,128)(2,1)S(1)}, bf16[3,48,2048]{2,1,0:T(8,128)(2,1)S(1)}, u32[]{:S(2)}, u32[]{:S(2)}) collective-permute-start(bf16[3,48,2048]{2,1,0:T(8,128)(2,1)S(1)} %slice.7), channel_id=1, source_target_pairs={{0,192},{16,208},{32,224},{48,240},{64,0},{80,16},{96,32},{112,48}... | collective-permute-start | bytes 1769480 | tf_op jit(solution)/shard_map/ppermute | solution.py:304
  60.7 3.6 %collective-permute-start.7 = (bf16[3,48,2048]{2,1,0:T(8,128)(2,1)S(1)}, bf16[3,48,2048]{2,1,0:T(8,128)(2,1)S(1)}, u32[]{:S(2)}, u32[]{:S(2)}) collective-permute-start(bf16[3,48,2048]{2,1,0:T(8,128)(2,1)S(1)} %collective-permute-done.2.refs_6_), channel_id=1, source_target_pairs={{0,1},{1,0},{2,3},{3,2},{4,5},{5,4},{6,7},{7,6},{8,9},{9,8},{10,11... | collective-permute-start | bytes 1769480 | tf_op jit(solution)/shard_map/ppermute | solution.py:322
  61.2 3.1 %collective-permute-start.8 = (bf16[3,48,2048]{2,1,0:T(8,128)(2,1)S(1)}, bf16[3,48,2048]{2,1,0:T(8,128)(2,1)S(1)}, u32[]{:S(2)}, u32[]{:S(2)}) collective-permute-start(bf16[3,48,2048]{2,1,0:T(8,128)(2,1)S(1)} %collective-permute-done.3.refs_7_), channel_id=1, source_target_pairs={{0,1},{1,0},{2,3},{3,2},{4,5},{5,4},{6,7},{7,6},{8,9},{9,8},{10,11... | collective-permute-start | bytes 1769480 | tf_op jit(solution)/shard_map/ppermute | solution.py:323

commit v6 on v5

--- a/solution.py
+++ b/solution.py
@@ -9,7 +9,6 @@
 
 
 EPS = 1e-06
-UNITS = 48
 F32, BF16 = jnp.float32, jnp.bfloat16
 NT = (((1,), (1,)), ((), ()))
 VMEM = pl.BlockSpec(memory_space=pltpu.VMEM)
@@ -120,26 +119,16 @@
 
 
 def pack_kernel(
-    rate_ref, gate_hbm, up_hbm, down_hbm, tokens_hbm, own_ref, rate_row_ref, tokens_ref,
-    gate_ref, up_ref, down_ref, sems,
+    rate_ref, gate_hbm, up_hbm, down_hbm, tokens_hbm, own_ref, rate_row_ref, tokens_ref, sems
 ):
-    units = gate_ref.shape[0]
-    landed = (tokens_ref, gate_ref, up_ref, down_ref)
-    loads = [
-        pltpu.make_async_copy(source, at, sems.at[n])
-        for n, (source, at) in enumerate(
-            zip((tokens_hbm, gate_hbm, up_hbm, down_hbm), landed)
-        )
-    ]
+    loads = [pltpu.make_async_copy(tokens_hbm, tokens_ref, sems.at[3])]
+    for n, source in enumerate((gate_hbm, up_hbm, down_hbm)):
+        loads.append(pltpu.make_async_copy(source, own_ref.at[n], sems.at[n]))
     for load in loads:
         load.start()
-    for n in range(3):
-        own_ref[n, units:, :] = jnp.zeros((UNITS - units, own_ref.shape[2]), BF16)
     rate_row_ref[...] = jnp.full(rate_row_ref.shape, rate_ref[0], F32)
-    for n in range(3):
-        loads[1 + n].wait()
-        own_ref[n, 0:units, :] = landed[1 + n][...]
-    loads[0].wait()
+    for load in loads:
+        load.wait()
 
 
 def spread_kernel(tokens_ref, copies_ref):
@@ -147,13 +136,21 @@
         copies_ref[b] = tokens_ref[...]
 
 
-def pre_of(xn, ref):
-    block = ref[0:2].reshape(2 * UNITS, ref.shape[2])
-    return lax.dot_general(xn, block, NT, preferred_element_type=F32)
-
-
-def hidden_of(pre):
-    return (silu(pre[:, :UNITS]) * pre[:, UNITS:]).astype(BF16)
+def hidden_of(xn, ref):
+    gate_pre = lax.dot_general(xn, ref[0], NT, preferred_element_type=F32)
+    up_pre = lax.dot_general(xn, ref[1], NT, preferred_element_type=F32)
+    return (silu(gate_pre) * up_pre).astype(BF16)
+
+
+def hidden_of_halves(xn_ref, low_ref, high_ref):
+    half = low_ref.shape[2]
+    low, high = xn_ref[:, :half], xn_ref[:, half:]
+    pre = [
+        lax.dot_general(low, low_ref[n], NT, preferred_element_type=F32)
+        + lax.dot_general(high, high_ref[n], NT, preferred_element_type=F32)
+        for n in range(2)
+    ]
+    return (silu(pre[0]) * pre[1]).astype(BF16)
 
 
 def norm_kernel(side, tiles_ref, gain_ref, xn_ref):
@@ -163,42 +160,30 @@
         norm_rows(tiles_ref, x * tp, tp, gain_ref, xn_ref, x * count)
 
 
-def far_parts(far_low_ref, far_high_ref, part):
+def near_kernel(xn_ref, *refs):
+    *whole, far_low_ref, far_high_ref, out_ref = refs
     half = far_low_ref.shape[2]
-
-    def pre(xn_ref):
-        return pre_of(xn_ref[:, :half], far_low_ref) + pre_of(xn_ref[:, half:], far_high_ref)
-
-    def columns(t):
-        if (t + 1) * part <= half:
-            return far_low_ref[2, :, t * part : (t + 1) * part]
-        return far_high_ref[2, :, t * part - half : (t + 1) * part - half]
-
-    return pre, columns
-
-
-def near_kernel(part, xn_ref, *refs):
-    *whole, far_low_ref, far_high_ref, out_ref = refs
-    far_pre, far_columns = far_parts(far_low_ref, far_high_ref, part)
     xn = xn_ref[...]
-    hidden = [hidden_of(pre_of(xn, ref)) for ref in whole]
-    hidden.append(hidden_of(far_pre(xn_ref)))
-    for t in range(out_ref.shape[1] // part):
-        cols = slice(t * part, (t + 1) * part)
-        down = jnp.dot(hidden[-1], far_columns(t), preferred_element_type=F32)
-        for n, ref in enumerate(whole):
-            down = down + jnp.dot(hidden[n], ref[2, :, cols], preferred_element_type=F32)
-        out_ref[:, cols] = down
+    hidden = [hidden_of(xn, ref) for ref in whole]
+    far = hidden_of_halves(xn_ref, far_low_ref, far_high_ref)
+    out_ref[:, :half] = jnp.dot(far, far_low_ref[2], preferred_element_type=F32)
+    out_ref[:, half:] = jnp.dot(far, far_high_ref[2], preferred_element_type=F32)
+    for n, ref in enumerate(whole):
+        out_ref[...] += jnp.dot(hidden[n], ref[2], preferred_element_type=F32)
 
 
 def far_kernel(side, xn_ref, near_ref, far_low_ref, far_high_ref, out_ref):
     peers, count, part = out_ref.shape
     tp = peers // side
-    far_pre, far_columns = far_parts(far_low_ref, far_high_ref, part)
-    hidden = hidden_of(far_pre(xn_ref))
+    half = far_low_ref.shape[2]
+    hidden = hidden_of_halves(xn_ref, far_low_ref, far_high_ref)
     for t in range(tp):
         cols = slice(t * part, (t + 1) * part)
-        down = near_ref[:, cols] + jnp.dot(hidden, far_columns(t), preferred_element_type=F32)
+        if (t + 1) * part <= half:
+            weight = far_low_ref[2, :, cols]
+        else:
+            weight = far_high_ref[2, :, t * part - half : (t + 1) * part - half]
+        down = near_ref[:, cols] + jnp.dot(hidden, weight, preferred_element_type=F32)
         down = down.astype(BF16)
         for x in range(side):
             out_ref[x * tp + t] = down[x * count : (x + 1) * count]
@@ -232,14 +217,13 @@
     own, rate_row, kept = pl.pallas_call(
         pack_kernel,
         out_shape=(
-            pltpu.VMEM((3, UNITS, width), BF16),
+            pltpu.VMEM((3, w_gate.shape[1], width), BF16),
             pltpu.VMEM((1, size), F32),
             pltpu.VMEM((count, part), BF16),
         ),
         in_specs=[SMEM] + [HBM] * 4,
         out_specs=(VMEM, VMEM, VMEM),
-        scratch_shapes=[pltpu.VMEM((w_gate.shape[1], width), BF16)] * 3
-        + [pltpu.SemaphoreType.DMA((4,))],
+        scratch_shapes=[pltpu.SemaphoreType.DMA((4,))],
         compiler_params=pltpu.CompilerParams(vmem_limit_bytes=4 << 20),
         name="pack",
     )(head_rate, *in_hbm(w_gate.T, w_up.T, w_down.T, tokens))
@@ -322,7 +306,7 @@
     far_low_2 = lax.ppermute(far_low, "tp", partner)
     far_high_2 = lax.ppermute(far_high, "tp", partner)
     near = pl.pallas_call(
-        functools.partial(near_kernel, part),
+        near_kernel,
         out_shape=pltpu.VMEM((rows, width), F32),
         in_specs=[VMEM] * 9,
         out_specs=VMEM,

time: 83.8 us -> 82.9 us (0.989)
  Pallas kernels: 7.39 us -> 6.35 us
  transfers between devices with their start and end apart: 9 -> 9, of which waited for: 0 -> 1; matrix products, arithmetic and copies ran while one was open for 0% -> 0% of each run, Pallas kernels for 6% -> 5%
where the time goes in v6:
time: 82.9 us; the launch traced here: 82.6 us
  blocking collectives  66 us (80%)
  starting transfers between devices  7.81 us (9%)
  Pallas kernels  6.35 us (8%)
  between operations  1.5 us (2%)
    all_to_all x1, blocking collectives, body(): tiles = lax.all_to_all(copies, 'tp', 0, 0, tiled=True)  18.5 us
    all_to_all x1, blocking collectives, body(): lax.all_to_all(blocks, ('kv', 'tp'), 0, 0, tiled=True, axis_index_groups=...  18.2 us
    all_to_all x1, blocking collectives, body(): lax.all_to_all(tiles, ('kv', 'tp'), 0, 0, tiled=True, axis_index_groups=g...  17.7 us
    all_to_all x1, blocking collectives, body(): tiles = lax.all_to_all(tiles, 'tp', 0, 0, tiled=True)  11.6 us
    ppermute x1, starting transfers between devices, body(): far_high = lax.ppermute(below[:, :, width // 2:], 'kv', y_ring(-1, side))  2.59 us
    ppermute x1, starting transfers between devices, body(): above = lax.ppermute(own, 'kv', y_ring(1, side))  2.19 us
    pallas_call x1, Pallas kernels, body(): pl.pallas_call(near_kernel, out_shape=pltpu.VMEM((rows, width), F32), in_...  2.18 us
    pallas_call x1, Pallas kernels, body(): pl.pallas_call(attention_kernel, out_shape=(pltpu.VMEM((tp, count, part),...  2.13 us
  transfers between devices with their start and end apart: 9, of which 1 were waited for; matrix products, arithmetic and copies ran while one was open for 0% of the time, Pallas kernels for 5%

profile of v6, /device:TPU:1, one launch (start us, length us, event | category | flops | bytes accessed | tf_op | source)
XLA Modules:
  0.0 82.6 jit_solution(2671998988092907598)
XLA Ops:
  1.3 1.3 %pack.1 = (bf16[3,44,4096]{2,1,0:T(8,128)(2,1)S(1)}, f32[1,128]{1,0:T(1,128)S(1)}, bf16[16,256]{1,0:T(8,128)(2,1)S(1)}) custom-call(f32[1]{0:T(128)S(6)} %copy.18.rate_ref, bf16[44,4096]{1,0:T(8,128)(2,1)} %bitcast.21, bf16[44,4096]{1,0:T(8,128)(2,1)} %bitcast.22, bf16[44,4096]{1,0:T(8,128)(2,1)} %bitcast.23, bf16[16,256]{1,0:T(8,128)(2,1)} %tokens_hbm.1), custom_call_target="tpu_custom_call" | custom-call | tf_op jit(solution)/shard_map/pack/pallas_call | solution.py:217
  2.6 2.2 %collective-permute-start = (bf16[3,44,4096]{2,1,0:T(8,128)(2,1)S(1)}, bf16[3,44,4096]{2,1,0:T(8,128)(2,1)S(1)}, u32[]{:S(2)}, u32[]{:S(2)}) collective-permute-start(bf16[3,44,4096]{2,1,0:T(8,128)(2,1)S(1)} %get-tuple-element.26.refs_0_), channel_id=1, source_target_pairs={{0,64},{16,80},{32,96},{48,112},{64,128},{80,144},{96,160},{112,17... | collective-permute-start | bytes 3244040 | tf_op jit(solution)/shard_map/ppermute | solution.py:230
  4.8 1.5 %collective-permute-start.1 = (bf16[3,44,4096]{2,1,0:T(8,128)(2,1)S(1)}, bf16[3,44,4096]{2,1,0:T(8,128)(2,1)S(1)}, u32[]{:S(2)}, u32[]{:S(2)}) collective-permute-start(bf16[3,44,4096]{2,1,0:T(8,128)(2,1)S(1)} %get-tuple-element.26.refs_0_), channel_id=1, source_target_pairs={{0,192},{16,208},{32,224},{48,240},{64,0},{80,16},{96,32},{112,48}... | collective-permute-start | bytes 3244040 | tf_op jit(solution)/shard_map/ppermute | solution.py:231
  6.3 0.0 copy-start.4
  6.3 0.0 copy-start.5
  6.3 0.0 copy-start.7
  6.3 0.0 copy-start.9
  6.4 18.5 %all_to_all.20.tiles_ref = bf16[16,16,256]{2,1,0:T(8,128)(2,1)S(1)} all-to-all(bf16[16,16,256]{2,1,0:T(8,128)(2,1)S(1)} %spread.1), channel_id=1, replica_groups=mesh['kv'=16,'tp'=16] {'tp'}, dimensions={0} | all-to-all | bytes 262144 | tf_op jit(solution)/shard_map/all_to_all | solution.py:243
  25.0 2.1 %attention.1 = (bf16[16,16,256]{2,1,0:T(8,128)(2,1)S(1)}, f32[16,128,128]{2,1,0:T(8,128)}) custom-call(bf16[16,16,256]{2,1,0:T(8,128)(2,1)S(1)} %all_to_all.20.tiles_ref, f32[1,4096]{1,0:T(1,128)S(1)} %bitcast.16, bf16[2,4096]{1,0:T(2,128)(2,1)S(1)} %bitcast.17, f32[1,128]{1,0:T(1,128)S(1)} %get-tuple-element.17.rate_ref, f32[1,128]{1,0:T(1,128)S(1)} %bitcast.19, ...), custom_call_target="tpu_custom_call" | custom-call | tf_op jit(solution)/shard_map/attention/pallas_call | solution.py:245
  27.1 11.6 %all_to_all.21.tiles_ref = bf16[16,16,256]{2,1,0:T(8,128)(2,1)S(1)} all-to-all(bf16[16,16,256]{2,1,0:T(8,128)(2,1)S(1)} %get-tuple-element.18), channel_id=1, replica_groups=mesh['kv'=16,'tp'=16] {'tp'}, dimensions={0} | all-to-all | bytes 262144 | tf_op jit(solution)/shard_map/all_to_all | solution.py:272
  38.7 0.1 collective-permute-start.5
  38.8 0.5 collective-permute-start.6
  39.3 0.1 collective-permute-start.4
  39.5 0.2 collective-permute-start.2
  39.7 2.6 %collective-permute-start.3 = (bf16[3,44,2048]{2,1,0:T(8,128)(2,1)S(1)}, bf16[3,44,2048]{2,1,0:T(8,128)(2,1)S(1)}, u32[]{:S(2)}, u32[]{:S(2)}) collective-permute-start(bf16[3,44,2048]{2,1,0:T(8,128)(2,1)S(1)} %slice.7), channel_id=1, source_target_pairs={{0,192},{16,208},{32,224},{48,240},{64,0},{80,16},{96,32},{112,48}... | collective-permute-start | bytes 1622024 | tf_op jit(solution)/shard_map/ppermute | solution.py:288
  42.3 18.2 %all_to_all.22.tiles_ref = bf16[64,8,256]{2,1,0:T(8,128)(2,1)S(1)} all-to-all(bf16[64,8,256]{2,1,0:T(8,128)(2,1)S(1)} %get-tuple-element.22), channel_id=1, replica_groups={{0,1,2,3,4,5,6,7,8,9,10,11,12,13,14,15,16,17,18,19,20,21,22,23,24,25,26..., dimensions={0} | all-to-all | bytes 524288 | tf_op jit(solution)/shard_map/all_to_all | solution.py:293
  60.5 0.2 norm.1.xn_ref
  60.7 0.5 collective-permute-start.7
  61.2 0.1 collective-permute-start.8
  61.3 2.2 %near.1.near_ref = f32[32,4096]{1,0:T(8,128)S(1)} custom-call(bf16[32,4096]{1,0:T(8,128)(2,1)S(1)} %norm.1.xn_ref, bf16[3,44,4096]{2,1,0:T(8,128)(2,1)S(1)} %get-tuple-element.26.refs_0_, bf16[3,44,4096]{2,1,0:T(8,128)(2,1)S(1)} %collective-permute-done.refs_1_, bf16[3,44,4096]{2,1,0:T(8,128)(2,1)S(1)} %collective-permute-done.1.refs_2_, ...), custom_call_target="tpu_custom_call" | custom-call | flops 8000000000 | bytes 8000000 | tf_op jit(solution)/shard_map/near/pallas_call | solution.py:308
  63.5 0.2 collective-permute-done.8.far_high_ref
  63.7 0.5 far.1
  64.2 17.7 %all_to_all.23 = bf16[64,8,256]{2,1,0:T(8,128)(2,1)S(1)} all-to-all(bf16[64,8,256]{2,1,0:T(8,128)(2,1)S(1)} %far.1), channel_id=1, replica_groups={{0,1,2,3,4,5,6,7,8,9,10,11,12,13,14,15,16,17,18,19,20,21,22,23,24,25,26..., dimensions={0} | all-to-all | bytes 524288 | tf_op jit(solution)/shard_map/all_to_all | solution.py:327
  82.0 0.6 add_convert_fusion
  (29 shorter events, 0.2 us)
Async XLA Ops:
  2.6 36.1 %collective-permute-start = (bf16[3,44,4096]{2,1,0:T(8,128)(2,1)S(1)}, bf16[3,44,4096]{2,1,0:T(8,128)(2,1)S(1)}, u32[]{:S(2)}, u32[]{:S(2)}) collective-permute-start(bf16[3,44,4096]{2,1,0:T(8,128)(2,1)S(1)} %get-tuple-element.26.refs_0_), channel_id=1, source_target_pairs={{0,64},{16,80},{32,96},{48,112},{64,128},{80,144},{96,160},{112,17... | collective-permute-start | bytes 3244040 | tf_op jit(solution)/shard_map/ppermute | solution.py:230
  4.8 33.9 %collective-permute-start.1 = (bf16[3,44,4096]{2,1,0:T(8,128)(2,1)S(1)}, bf16[3,44,4096]{2,1,0:T(8,128)(2,1)S(1)}, u32[]{:S(2)}, u32[]{:S(2)}) collective-permute-start(bf16[3,44,4096]{2,1,0:T(8,128)(2,1)S(1)} %get-tuple-element.26.refs_0_), channel_id=1, source_target_pairs={{0,192},{16,208},{32,224},{48,240},{64,0},{80,16},{96,32},{112,48}... | collective-permute-start | bytes 3244040 | tf_op jit(solution)/shard_map/ppermute | solution.py:231
  6.3 18.6 %copy-start = (bf16[4096,128]{1,0:T(8,128)(2,1)S(1)}, bf16[4096,128]{1,0:T(8,128)(2,1)}, u32[]{:S(2)}) copy-start(bf16[4096,128]{1,0:T(8,128)(2,1)} %wq_ref.1) | copy-start | bytes 3145732
  6.3 18.6 %copy-start.1 = (bf16[4096,128]{1,0:T(8,128)(2,1)S(1)}, bf16[4096,128]{1,0:T(8,128)(2,1)}, u32[]{:S(2)}) copy-start(bf16[4096,128]{1,0:T(8,128)(2,1)} %wk_ref.1) | copy-start | bytes 3145732
  6.3 18.6 %copy-start.2 = (bf16[4096,128]{1,0:T(8,128)(2,1)S(1)}, bf16[4096,128]{1,0:T(8,128)(2,1)}, u32[]{:S(2)}) copy-start(bf16[4096,128]{1,0:T(8,128)(2,1)} %wv_ref.1) | copy-start | bytes 3145732
  6.3 18.6 %copy-start.3 = (bf16[4096,128]{1,0:T(8,128)(2,1)S(1)}, bf16[4096,128]{1,0:T(8,128)(2,1)}, u32[]{:S(2)}) copy-start(bf16[4096,128]{1,0:T(8,128)(2,1)} %wg_ref.1) | copy-start | bytes 3145732
  6.3 18.6 %copy-start.4 = (bf16[128,4096]{1,0:T(8,128)(2,1)S(1)}, bf16[128,4096]{1,0:T(8,128)(2,1)}, u32[]{:S(2)}) copy-start(bf16[128,4096]{1,0:T(8,128)(2,1)} %wo_ref.1) | copy-start | bytes 3145732
  6.3 18.6 %copy-start.5 = (f32[16,1,128,128]{3,2,1,0:T(8,128)S(1)}, f32[16,1,128,128]{3,2,1,0:T(8,128)}, u32[]{:S(2)}) copy-start(f32[16,1,128,128]{3,2,1,0:T(8,128)} %param.25) | copy-start | bytes 3145732
  6.3 18.6 %copy-start.6 = (f32[4096]{0:T(1024)S(1)}, f32[4096]{0:T(1024)}, u32[]{:S(2)}) copy-start(f32[4096]{0:T(1024)} %param.16) | copy-start | bytes 49156
  6.3 18.6 %copy-start.7 = (bf16[2,4096,1]{1,0,2:T(2,128)(2,1)S(1)}, bf16[2,4096,1]{1,0,2:T(2,128)(2,1)}, u32[]{:S(2)}) copy-start(bf16[2,4096,1]{1,0,2:T(2,128)(2,1)} %param.21) | copy-start | bytes 49156
  6.3 18.6 %copy-start.9 = (f32[128]{0:T(128)S(1)}, f32[128]{0:T(128)}, u32[]{:S(2)}) copy-start(f32[128]{0:T(128)} %param.23) | copy-start | bytes 1540
  38.7 21.8 %copy-start.8 = (f32[4096]{0:T(1024)S(1)}, f32[4096]{0:T(1024)}, u32[]{:S(2)}) copy-start(f32[4096]{0:T(1024)} %param.26) | copy-start | bytes 49156
  38.7 22.6 %collective-permute-start.5 = (bf16[3,44,4096]{2,1,0:T(8,128)(2,1)S(1)}, bf16[3,44,4096]{2,1,0:T(8,128)(2,1)S(1)}, u32[]{:S(2)}, u32[]{:S(2)}) collective-permute-start(bf16[3,44,4096]{2,1,0:T(8,128)(2,1)S(1)} %collective-permute-done.refs_1_), channel_id=1, source_target_pairs={{0,1},{1,0},{2,3},{3,2},{4,5},{5,4},{6,7},{7,6},{8,9},{9,8},{10,11... | collective-permute-start | bytes 3244040 | tf_op jit(solution)/shard_map/ppermute | solution.py:291
  38.8 22.5 %collective-permute-start.6 = (bf16[3,44,4096]{2,1,0:T(8,128)(2,1)S(1)}, bf16[3,44,4096]{2,1,0:T(8,128)(2,1)S(1)}, u32[]{:S(2)}, u32[]{:S(2)}) collective-permute-start(bf16[3,44,4096]{2,1,0:T(8,128)(2,1)S(1)} %collective-permute-done.1.refs_2_), channel_id=1, source_target_pairs={{0,1},{1,0},{2,3},{3,2},{4,5},{5,4},{6,7},{7,6},{8,9},{9,8},{10,11... | collective-permute-start | bytes 3244040 | tf_op jit(solution)/shard_map/ppermute | solution.py:292
  39.3 22.0 %collective-permute-start.4 = (bf16[3,44,4096]{2,1,0:T(8,128)(2,1)S(1)}, bf16[3,44,4096]{2,1,0:T(8,128)(2,1)S(1)}, u32[]{:S(2)}, u32[]{:S(2)}) collective-permute-start(bf16[3,44,4096]{2,1,0:T(8,128)(2,1)S(1)} %get-tuple-element.26.refs_0_), channel_id=1, source_target_pairs={{0,1},{1,0},{2,3},{3,2},{4,5},{5,4},{6,7},{7,6},{8,9},{9,8},{10,11... | collective-permute-start | bytes 3244040 | tf_op jit(solution)/shard_map/ppermute | solution.py:290
  39.5 21.1 %collective-permute-start.2 = (bf16[3,44,2048]{2,1,0:T(8,128)(2,1)S(1)}, bf16[3,44,2048]{2,1,0:T(8,128)(2,1)S(1)}, u32[]{:S(2)}, u32[]{:S(2)}) collective-permute-start(bf16[3,44,2048]{2,1,0:T(8,128)(2,1)S(1)} %slice.6), channel_id=1, source_target_pairs={{0,64},{16,80},{32,96},{48,112},{64,128},{80,144},{96,160},{112,17... | collective-permute-start | bytes 1622024 | tf_op jit(solution)/shard_map/ppermute | solution.py:287
  39.7 21.0 %collective-permute-start.3 = (bf16[3,44,2048]{2,1,0:T(8,128)(2,1)S(1)}, bf16[3,44,2048]{2,1,0:T(8,128)(2,1)S(1)}, u32[]{:S(2)}, u32[]{:S(2)}) collective-permute-start(bf16[3,44,2048]{2,1,0:T(8,128)(2,1)S(1)} %slice.7), channel_id=1, source_target_pairs={{0,192},{16,208},{32,224},{48,240},{64,0},{80,16},{96,32},{112,48}... | collective-permute-start | bytes 1622024 | tf_op jit(solution)/shard_map/ppermute | solution.py:288
  60.7 2.8 %collective-permute-start.7 = (bf16[3,44,2048]{2,1,0:T(8,128)(2,1)S(1)}, bf16[3,44,2048]{2,1,0:T(8,128)(2,1)S(1)}, u32[]{:S(2)}, u32[]{:S(2)}) collective-permute-start(bf16[3,44,2048]{2,1,0:T(8,128)(2,1)S(1)} %collective-permute-done.2.refs_6_), channel_id=1, source_target_pairs={{0,1},{1,0},{2,3},{3,2},{4,5},{5,4},{6,7},{7,6},{8,9},{9,8},{10,11... | collective-permute-start | bytes 1622024 | tf_op jit(solution)/shard_map/ppermute | solution.py:306
  61.2 2.5 %collective-permute-start.8 = (bf16[3,44,2048]{2,1,0:T(8,128)(2,1)S(1)}, bf16[3,44,2048]{2,1,0:T(8,128)(2,1)S(1)}, u32[]{:S(2)}, u32[]{:S(2)}) collective-permute-start(bf16[3,44,2048]{2,1,0:T(8,128)(2,1)S(1)} %collective-permute-done.3.refs_7_), channel_id=1, source_target_pairs={{0,1},{1,0},{2,3},{3,2},{4,5},{5,4},{6,7},{7,6},{8,9},{9,8},{10,11... | collective-permute-start | bytes 1622024 | tf_op jit(solution)/shard_map/ppermute | solution.py:307

commit v7 on v6

--- a/solution.py
+++ b/solution.py
@@ -24,31 +24,42 @@
     return [pltpu.with_memory_space_constraint(a, pltpu.VMEM) for a in arrays]
 
 
-def y_ring(shift, side):
+def y_ring(shift, side, tp):
     return [
-        (side * y + x, side * ((y + shift) % side) + x) for y in range(side) for x in range(side)
+        ((side * y + x) * tp + t, (side * ((y + (1 - 2 * (t % 2)) * shift) % side) + x) * tp + t)
+        for y in range(side)
+        for x in range(side)
+        for t in range(tp)
     ]
 
 
+def ring_order(tp):
+    return list(range(tp))
+
+
+def plane_order(side, tp):
+    return [(x, t) for x in range(side) for t in range(tp)]
+
+
 def plane_groups(side, tp):
-    return [[(side * y + x) * tp + t for x in range(side) for t in range(tp)] for y in range(side)]
+    return [[(side * y + x) * tp + t for x, t in plane_order(side, tp)] for y in range(side)]
 
 
 def silu(t):
     return t / (1.0 + jnp.exp(-t))
 
 
-def norm_rows(tiles_ref, first, n_tiles, gain_ref, out_ref, at):
+def norm_rows(tiles_ref, places, gain_ref, out_ref, at):
     rows, part = tiles_ref.shape[1:]
     total = jnp.zeros((rows, part), F32)
-    for t in range(n_tiles):
-        tile = tiles_ref[first + t].astype(F32)
+    for place in places:
+        tile = tiles_ref[place].astype(F32)
         total = total + tile * tile
-    mean = jnp.sum(total, axis=-1, keepdims=True) * (1.0 / (n_tiles * part))
+    mean = jnp.sum(total, axis=-1, keepdims=True) * (1.0 / (len(places) * part))
     scale = lax.rsqrt(mean + EPS)
-    for t in range(n_tiles):
+    for t, place in enumerate(places):
         cols = slice(t * part, (t + 1) * part)
-        tile = tiles_ref[first + t].astype(F32)
+        tile = tiles_ref[place].astype(F32)
         out_ref[at : at + rows, cols] = (tile * scale * gain_ref[0:1, cols]).astype(BF16)
 
 
@@ -58,7 +69,8 @@
 ):
     tp, count, part = tiles_ref.shape
     size = wq_ref.shape[1]
-    norm_rows(tiles_ref, 0, tp, gain_ref, xn_ref, 0)
+    order = ring_order(tp)
+    norm_rows(tiles_ref, [order.index(t) for t in range(tp)], gain_ref, xn_ref, 0)
     xn = xn_ref[...]
     rates = lax.dot_general(xn, wr_ref[...], NT, preferred_element_type=F32)
     query = jnp.dot(xn, wq_ref[...], preferred_element_type=F32)
@@ -99,23 +111,23 @@
             stores[-1].start()
     scale = lax.rsqrt(jnp.mean(readout * readout, -1, keepdims=True) + EPS)
     mixed = (readout * scale * head_gain_ref[...] * silu(gate_in)).astype(BF16)
-    for t in range(tp):
+    for n, t in enumerate(order):
         cols = slice(t * part, (t + 1) * part)
-        out_ref[t] = jnp.dot(mixed, wo_ref[:, cols], preferred_element_type=F32).astype(BF16)
+        out_ref[n] = jnp.dot(mixed, wo_ref[:, cols], preferred_element_type=F32).astype(BF16)
     for store in stores:
         store.wait()
 
 
-def residual_kernel(tiles_ref, tokens_ref, out_ref, blocks_ref):
+def residual_kernel(order, tiles_ref, tokens_ref, out_ref, blocks_ref):
     total = tokens_ref[...].astype(F32)
     for t in range(tiles_ref.shape[0]):
         total = total + tiles_ref[t].astype(F32)
     residual = total.astype(BF16)
     out_ref[...] = residual
     rows = blocks_ref.shape[1]
-    for b in range(blocks_ref.shape[0]):
-        at = (b % 2) * rows
-        blocks_ref[b] = residual[at : at + rows]
+    for n, (_, t) in enumerate(order):
+        at = (t % 2) * rows
+        blocks_ref[n] = residual[at : at + rows]
 
 
 def pack_kernel(
@@ -142,51 +154,44 @@
     return (silu(gate_pre) * up_pre).astype(BF16)
 
 
-def hidden_of_halves(xn_ref, low_ref, high_ref):
-    half = low_ref.shape[2]
-    low, high = xn_ref[:, :half], xn_ref[:, half:]
-    pre = [
-        lax.dot_general(low, low_ref[n], NT, preferred_element_type=F32)
-        + lax.dot_general(high, high_ref[n], NT, preferred_element_type=F32)
-        for n in range(2)
-    ]
-    return (silu(pre[0]) * pre[1]).astype(BF16)
-
-
-def norm_kernel(side, tiles_ref, gain_ref, xn_ref):
+def norm_kernel(side, order, tiles_ref, gain_ref, xn_ref):
     peers, count, _ = tiles_ref.shape
     tp = peers // side
     for x in range(side):
-        norm_rows(tiles_ref, x * tp, tp, gain_ref, xn_ref, x * count)
+        places = [order.index((x, t)) for t in range(tp)]
+        norm_rows(tiles_ref, places, gain_ref, xn_ref, x * count)
+
+
+def last_kernel(order, tiles_ref, residual_ref, out_ref):
+    rows = tiles_ref.shape[1]
+    for half in range(2):
+        at = slice(half * rows, (half + 1) * rows)
+        total = residual_ref[at].astype(F32)
+        for n, (_, t) in enumerate(order):
+            if t % 2 == half:
+                total = total + tiles_ref[n].astype(F32)
+        out_ref[at] = total.astype(BF16)
 
 
 def near_kernel(xn_ref, *refs):
-    *whole, far_low_ref, far_high_ref, out_ref = refs
-    half = far_low_ref.shape[2]
+    *blocks, out_ref = refs
     xn = xn_ref[...]
-    hidden = [hidden_of(xn, ref) for ref in whole]
-    far = hidden_of_halves(xn_ref, far_low_ref, far_high_ref)
-    out_ref[:, :half] = jnp.dot(far, far_low_ref[2], preferred_element_type=F32)
-    out_ref[:, half:] = jnp.dot(far, far_high_ref[2], preferred_element_type=F32)
-    for n, ref in enumerate(whole):
-        out_ref[...] += jnp.dot(hidden[n], ref[2], preferred_element_type=F32)
-
-
-def far_kernel(side, xn_ref, near_ref, far_low_ref, far_high_ref, out_ref):
+    hidden = [hidden_of(xn, ref) for ref in blocks]
+    for n, ref in enumerate(blocks):
+        down = jnp.dot(hidden[n], ref[2], preferred_element_type=F32)
+        out_ref[...] = down if n == 0 else out_ref[...] + down
+
+
+def far_kernel(side, order, xn_ref, near_ref, far_ref, out_ref):
     peers, count, part = out_ref.shape
     tp = peers // side
-    half = far_low_ref.shape[2]
-    hidden = hidden_of_halves(xn_ref, far_low_ref, far_high_ref)
+    hidden = hidden_of(xn_ref[...], far_ref)
     for t in range(tp):
         cols = slice(t * part, (t + 1) * part)
-        if (t + 1) * part <= half:
-            weight = far_low_ref[2, :, cols]
-        else:
-            weight = far_high_ref[2, :, t * part - half : (t + 1) * part - half]
-        down = near_ref[:, cols] + jnp.dot(hidden, weight, preferred_element_type=F32)
-        down = down.astype(BF16)
+        down = jnp.dot(hidden, far_ref[2, :, cols], preferred_element_type=F32)
+        down = (near_ref[:, cols] + down).astype(BF16)
         for x in range(side):
-            out_ref[x * tp + t] = down[x * count : (x + 1) * count]
+            out_ref[order.index((x, t))] = down[x * count : (x + 1) * count]
 
 
 def body(
@@ -213,6 +218,8 @@
     size = w_query.shape[1]
     peers = side * tp
     groups = plane_groups(side, tp)
+    order = plane_order(side, tp)
+    ring = [ring_order(tp)]
 
     own, rate_row, kept = pl.pallas_call(
         pack_kernel,
@@ -227,8 +234,8 @@
         compiler_params=pltpu.CompilerParams(vmem_limit_bytes=4 << 20),
         name="pack",
     )(head_rate, *in_hbm(w_gate.T, w_up.T, w_down.T, tokens))
-    above = lax.ppermute(own, "kv", y_ring(1, side))
-    below = lax.ppermute(own, "kv", y_ring(-1, side))
+    above = lax.ppermute(own, ("kv", "tp"), y_ring(1, side, tp))
+    below = lax.ppermute(own, ("kv", "tp"), y_ring(-1, side, tp))
     copies = pl.pallas_call(
         spread_kernel,
         out_shape=pltpu.VMEM((tp, count, part), BF16),
@@ -240,7 +247,7 @@
         ),
         name="spread",
     )(kept)
-    tiles = lax.all_to_all(copies, "tp", 0, 0, tiled=True)
+    tiles = lax.all_to_all(copies, "tp", 0, 0, tiled=True, axis_index_groups=ring)
     states = pltpu.VMEM((count, size, size), F32)
     tiles, new_state = pl.pallas_call(
         attention_kernel,
@@ -269,10 +276,10 @@
             w_query, w_key, w_value, w_outgate, w_out, state.reshape(count, size, size)
         ),
     )
-    tiles = lax.all_to_all(tiles, "tp", 0, 0, tiled=True)
+    tiles = lax.all_to_all(tiles, "tp", 0, 0, tiled=True, axis_index_groups=ring)
     half_count = count // 2
     residual, blocks = pl.pallas_call(
-        residual_kernel,
+        functools.partial(residual_kernel, order),
         out_shape=(
             pltpu.VMEM((count, part), BF16),
             pltpu.VMEM((peers, half_count, part), BF16),
@@ -284,8 +291,7 @@
     )(tiles, kept)
 
     blocks, own, above, below = lax.optimization_barrier((blocks, own, above, below))
-    far_low = lax.ppermute(above[:, :, : width // 2], "kv", y_ring(1, side))
-    far_high = lax.ppermute(below[:, :, width // 2 :], "kv", y_ring(-1, side))
+    far = lax.ppermute(above, ("kv", "tp"), y_ring(1, side, tp))
     partner = [(t, t ^ 1) for t in range(tp)]
     own_2 = lax.ppermute(own, "tp", partner)
     above_2 = lax.ppermute(above, "tp", partner)
@@ -295,40 +301,45 @@
     )
     rows = side * half_count
     xn = pl.pallas_call(
-        functools.partial(norm_kernel, side),
+        functools.partial(norm_kernel, side, order),
         out_shape=pltpu.VMEM((rows, width), BF16),
         in_specs=[VMEM] * 2,
         out_specs=VMEM,
         compiler_params=pltpu.CompilerParams(vmem_limit_bytes=4 << 20),
         name="norm",
     )(tiles, mlp_gain.reshape(1, width))
-    xn, far_low, far_high = lax.optimization_barrier((xn, far_low, far_high))
-    far_low_2 = lax.ppermute(far_low, "tp", partner)
-    far_high_2 = lax.ppermute(far_high, "tp", partner)
+    xn, far = lax.optimization_barrier((xn, far))
+    far_2 = lax.ppermute(far, "tp", partner)
     near = pl.pallas_call(
         near_kernel,
         out_shape=pltpu.VMEM((rows, width), F32),
-        in_specs=[VMEM] * 9,
+        in_specs=[VMEM] * 8,
         out_specs=VMEM,
         compiler_params=pltpu.CompilerParams(vmem_limit_bytes=8 << 20),
         cost_estimate=pl.CostEstimate(
             flops=8_000_000_000, bytes_accessed=8_000_000, transcendentals=0
         ),
         name="near",
-    )(xn, *in_vmem(own, above, below, own_2, above_2, below_2, far_low, far_high))
+    )(xn, *in_vmem(own, above, below, own_2, above_2, below_2, far))
     tiles = pl.pallas_call(
-        functools.partial(far_kernel, side),
+        functools.partial(far_kernel, side, order),
         out_shape=pltpu.VMEM((peers, half_count, part), BF16),
-        in_specs=[VMEM] * 4,
+        in_specs=[VMEM] * 3,
         out_specs=VMEM,
         compiler_params=pltpu.CompilerParams(vmem_limit_bytes=8 << 20),
         name="far",
-    )(xn, near, *in_vmem(far_low_2, far_high_2))
+    )(xn, near, *in_vmem(far_2))
     tiles = lax.all_to_all(
         tiles, ("kv", "tp"), 0, 0, tiled=True, axis_index_groups=groups
     )
-    tiles = tiles.astype(F32).reshape(peers // 2, count, part)
-    result = (residual.astype(F32) + jnp.sum(tiles, axis=0)).astype(BF16)
+    result = pl.pallas_call(
+        functools.partial(last_kernel, order),
+        out_shape=jax.ShapeDtypeStruct((count, part), BF16),
+        in_specs=[VMEM] * 2,
+        out_specs=VMEM,
+        compiler_params=pltpu.CompilerParams(vmem_limit_bytes=1 << 20),
+        name="last",
+    )(tiles, residual)
     return (result, new_state[:, None])
 
 

time: 82.9 us -> 82.2 us (level)
    ppermute x6 -> x4, starting transfers between devices: 7.12 us -> 7.29 us  [the longest x1 3.02 us: body(): far = lax.ppermute(above, ('kv', 'tp'), y_ring(1, side, tp))]
  transfers between devices with their start and end apart: 9 -> 7, of which waited for: 1 -> 1; matrix products, arithmetic and copies ran while one was open for 0% -> 0% of each run, Pallas kernels for 5% -> 5%
where the time goes in v7:
time: 82.2 us; the launch traced here: 81.9 us
  blocking collectives  65.3 us (79%)
  starting transfers between devices  7.8 us (9%)
  Pallas kernels  6.85 us (8%)
  between operations  1.46 us (2%)
    all_to_all x1, blocking collectives, body(): lax.all_to_all(copies, 'tp', 0, 0, tiled=True, axis_index_groups=ring)  18.3 us
    all_to_all x1, blocking collectives, body(): lax.all_to_all(blocks, ('kv', 'tp'), 0, 0, tiled=True, axis_index_groups=...  17.7 us
    all_to_all x1, blocking collectives, body(): lax.all_to_all(tiles, ('kv', 'tp'), 0, 0, tiled=True, axis_index_groups=g...  17.7 us
    all_to_all x1, blocking collectives, body(): lax.all_to_all(tiles, 'tp', 0, 0, tiled=True, axis_index_groups=ring)  11.6 us
    ppermute x1, starting transfers between devices, body(): far = lax.ppermute(above, ('kv', 'tp'), y_ring(1, side, tp))  3.02 us
    ppermute x1, starting transfers between devices, body(): below = lax.ppermute(own, ('kv', 'tp'), y_ring(-1, side, tp))  2.19 us
    pallas_call x1, Pallas kernels, body(): pl.pallas_call(attention_kernel, out_shape=(pltpu.VMEM((tp, count, part),...  2.13 us
    pallas_call x1, Pallas kernels, body(): pl.pallas_call(near_kernel, out_shape=pltpu.VMEM((rows, width), F32), in_...  2.04 us
  transfers between devices with their start and end apart: 7, of which 1 were waited for; matrix products, arithmetic and copies ran while one was open for 0% of the time, Pallas kernels for 5%

profile of v7, /device:TPU:1, one launch (start us, length us, event | category | flops | bytes accessed | tf_op | source)
XLA Modules:
  0.0 81.9 jit_solution(6838268062591043227)
XLA Ops:
  1.3 1.3 %pack.1 = (bf16[3,44,4096]{2,1,0:T(8,128)(2,1)S(1)}, f32[1,128]{1,0:T(1,128)S(1)}, bf16[16,256]{1,0:T(8,128)(2,1)S(1)}) custom-call(f32[1]{0:T(128)S(6)} %copy.18.rate_ref, bf16[44,4096]{1,0:T(8,128)(2,1)} %bitcast.16, bf16[44,4096]{1,0:T(8,128)(2,1)} %bitcast.17, bf16[44,4096]{1,0:T(8,128)(2,1)} %bitcast.18, bf16[16,256]{1,0:T(8,128)(2,1)} %tokens_hbm.1), custom_call_target="tpu_custom_call" | custom-call | tf_op jit(solution)/shard_map/pack/pallas_call | solution.py:224
  2.6 2.2 %collective-permute-start.1 = (bf16[3,44,4096]{2,1,0:T(8,128)(2,1)S(1)}, bf16[3,44,4096]{2,1,0:T(8,128)(2,1)S(1)}, u32[]{:S(2)}, u32[]{:S(2)}) collective-permute-start(bf16[3,44,4096]{2,1,0:T(8,128)(2,1)S(1)} %get-tuple-element.23.refs_0_), channel_id=1, source_target_pairs={{0,192},{1,65},{2,194},{3,67},{4,196},{5,69},{6,198},{7,71},{8,200... | collective-permute-start | bytes 3244040 | tf_op jit(solution)/shard_map/ppermute | solution.py:238
  4.8 1.5 %collective-permute-start = (bf16[3,44,4096]{2,1,0:T(8,128)(2,1)S(1)}, bf16[3,44,4096]{2,1,0:T(8,128)(2,1)S(1)}, u32[]{:S(2)}, u32[]{:S(2)}) collective-permute-start(bf16[3,44,4096]{2,1,0:T(8,128)(2,1)S(1)} %get-tuple-element.23.refs_0_), channel_id=1, source_target_pairs={{0,64},{1,193},{2,66},{3,195},{4,68},{5,197},{6,70},{7,199},{8,72}... | collective-permute-start | bytes 3244040 | tf_op jit(solution)/shard_map/ppermute | solution.py:237
  6.3 0.0 copy-start.4
  6.3 0.0 copy-start.5
  6.3 0.0 copy-start.6
  6.3 0.0 copy-start.7
  6.3 0.0 copy-start.9
  6.4 18.3 %all_to_all.20.tiles_ref = bf16[16,16,256]{2,1,0:T(8,128)(2,1)S(1)} all-to-all(bf16[16,16,256]{2,1,0:T(8,128)(2,1)S(1)} %spread.1), channel_id=1, replica_groups={{0,1,2,3,4,5,6,7,8,9,10,11,12,13,14,15},{16,17,18,19,20,21,22,23,24,25,..., dimensions={0} | all-to-all | bytes 262144 | tf_op jit(solution)/shard_map/all_to_all | solution.py:250
  24.8 0.0 copy-start.8
  24.8 2.1 %attention.1 = (bf16[16,16,256]{2,1,0:T(8,128)(2,1)S(1)}, f32[16,128,128]{2,1,0:T(8,128)}) custom-call(bf16[16,16,256]{2,1,0:T(8,128)(2,1)S(1)} %all_to_all.20.tiles_ref, f32[1,4096]{1,0:T(1,128)S(1)} %bitcast.12, bf16[2,4096]{1,0:T(2,128)(2,1)S(1)} %bitcast.13, f32[1,128]{1,0:T(1,128)S(1)} %get-tuple-element.16.rate_ref, f32[1,128]{1,0:T(1,128)S(1)} %bitcast.15, ...), custom_call_target="tpu_custom_call" | custom-call | tf_op jit(solution)/shard_map/attention/pallas_call | solution.py:252
  26.9 11.6 %all_to_all.21.tiles_ref = bf16[16,16,256]{2,1,0:T(8,128)(2,1)S(1)} all-to-all(bf16[16,16,256]{2,1,0:T(8,128)(2,1)S(1)} %get-tuple-element.17), channel_id=1, replica_groups={{0,1,2,3,4,5,6,7,8,9,10,11,12,13,14,15},{16,17,18,19,20,21,22,23,24,25,..., dimensions={0} | all-to-all | bytes 262144 | tf_op jit(solution)/shard_map/all_to_all | solution.py:279
  38.5 0.0 collective-permute-done.refs_1_
  38.5 3.0 %collective-permute-start.2 = (bf16[3,44,4096]{2,1,0:T(8,128)(2,1)S(1)}, bf16[3,44,4096]{2,1,0:T(8,128)(2,1)S(1)}, u32[]{:S(2)}, u32[]{:S(2)}) collective-permute-start(bf16[3,44,4096]{2,1,0:T(8,128)(2,1)S(1)} %collective-permute-done.refs_1_), channel_id=1, source_target_pairs={{0,64},{1,193},{2,66},{3,195},{4,68},{5,197},{6,70},{7,199},{8,72}... | collective-permute-start | bytes 3244040 | tf_op jit(solution)/shard_map/ppermute | solution.py:294
  41.5 0.5 collective-permute-start.5
  42.0 0.0 collective-permute-start.4
  42.1 17.7 %all_to_all.22.tiles_ref = bf16[64,8,256]{2,1,0:T(8,128)(2,1)S(1)} all-to-all(bf16[64,8,256]{2,1,0:T(8,128)(2,1)S(1)} %get-tuple-element.20), channel_id=1, replica_groups={{0,1,2,3,4,5,6,7,8,9,10,11,12,13,14,15,16,17,18,19,20,21,22,23,24,25,26..., dimensions={0} | all-to-all | bytes 524288 | tf_op jit(solution)/shard_map/all_to_all | solution.py:299
  59.8 0.2 norm.1.xn_ref
  60.0 0.5 collective-permute-start.6
  60.5 2.0 %near.1.near_ref = f32[32,4096]{1,0:T(8,128)S(1)} custom-call(bf16[32,4096]{1,0:T(8,128)(2,1)S(1)} %norm.1.xn_ref, bf16[3,44,4096]{2,1,0:T(8,128)(2,1)S(1)} %get-tuple-element.23.refs_0_, bf16[3,44,4096]{2,1,0:T(8,128)(2,1)S(1)} %collective-permute-done.refs_1_, bf16[3,44,4096]{2,1,0:T(8,128)(2,1)S(1)} %collective-permute-done.1.refs_2_, ...), custom_call_target="tpu_custom_call" | custom-call | flops 8000000000 | bytes 8000000 | tf_op jit(solution)/shard_map/near/pallas_call | solution.py:313
  62.6 0.4 collective-permute-done.6.far_ref
  63.0 0.5 far.1
  63.6 17.7 %all_to_all.23.tiles_ref = bf16[64,8,256]{2,1,0:T(8,128)(2,1)S(1)} all-to-all(bf16[64,8,256]{2,1,0:T(8,128)(2,1)S(1)} %far.1), channel_id=1, replica_groups={{0,1,2,3,4,5,6,7,8,9,10,11,12,13,14,15,16,17,18,19,20,21,22,23,24,25,26..., dimensions={0} | all-to-all | bytes 524288 | tf_op jit(solution)/shard_map/all_to_all | solution.py:332
  81.3 0.6 last.1
  (22 shorter events, 0.1 us)
Async XLA Ops:
  2.6 35.9 %collective-permute-start.1 = (bf16[3,44,4096]{2,1,0:T(8,128)(2,1)S(1)}, bf16[3,44,4096]{2,1,0:T(8,128)(2,1)S(1)}, u32[]{:S(2)}, u32[]{:S(2)}) collective-permute-start(bf16[3,44,4096]{2,1,0:T(8,128)(2,1)S(1)} %get-tuple-element.23.refs_0_), channel_id=1, source_target_pairs={{0,192},{1,65},{2,194},{3,67},{4,196},{5,69},{6,198},{7,71},{8,200... | collective-permute-start | bytes 3244040 | tf_op jit(solution)/shard_map/ppermute | solution.py:238
  4.8 33.8 %collective-permute-start = (bf16[3,44,4096]{2,1,0:T(8,128)(2,1)S(1)}, bf16[3,44,4096]{2,1,0:T(8,128)(2,1)S(1)}, u32[]{:S(2)}, u32[]{:S(2)}) collective-permute-start(bf16[3,44,4096]{2,1,0:T(8,128)(2,1)S(1)} %get-tuple-element.23.refs_0_), channel_id=1, source_target_pairs={{0,64},{1,193},{2,66},{3,195},{4,68},{5,197},{6,70},{7,199},{8,72}... | collective-permute-start | bytes 3244040 | tf_op jit(solution)/shard_map/ppermute | solution.py:237
  6.3 18.4 %copy-start = (bf16[4096,128]{1,0:T(8,128)(2,1)S(1)}, bf16[4096,128]{1,0:T(8,128)(2,1)}, u32[]{:S(2)}) copy-start(bf16[4096,128]{1,0:T(8,128)(2,1)} %wq_ref.1) | copy-start | bytes 3145732
  6.3 18.4 %copy-start.1 = (bf16[4096,128]{1,0:T(8,128)(2,1)S(1)}, bf16[4096,128]{1,0:T(8,128)(2,1)}, u32[]{:S(2)}) copy-start(bf16[4096,128]{1,0:T(8,128)(2,1)} %wk_ref.1) | copy-start | bytes 3145732
  6.3 18.4 %copy-start.2 = (bf16[4096,128]{1,0:T(8,128)(2,1)S(1)}, bf16[4096,128]{1,0:T(8,128)(2,1)}, u32[]{:S(2)}) copy-start(bf16[4096,128]{1,0:T(8,128)(2,1)} %wv_ref.1) | copy-start | bytes 3145732
  6.3 18.4 %copy-start.3 = (bf16[4096,128]{1,0:T(8,128)(2,1)S(1)}, bf16[4096,128]{1,0:T(8,128)(2,1)}, u32[]{:S(2)}) copy-start(bf16[4096,128]{1,0:T(8,128)(2,1)} %wg_ref.1) | copy-start | bytes 3145732
  6.3 18.4 %copy-start.4 = (bf16[128,4096]{1,0:T(8,128)(2,1)S(1)}, bf16[128,4096]{1,0:T(8,128)(2,1)}, u32[]{:S(2)}) copy-start(bf16[128,4096]{1,0:T(8,128)(2,1)} %wo_ref.1) | copy-start | bytes 3145732
  6.3 18.4 %copy-start.5 = (f32[16,1,128,128]{3,2,1,0:T(8,128)S(1)}, f32[16,1,128,128]{3,2,1,0:T(8,128)}, u32[]{:S(2)}) copy-start(f32[16,1,128,128]{3,2,1,0:T(8,128)} %param.25) | copy-start | bytes 3145732
  6.3 18.4 %copy-start.6 = (f32[4096]{0:T(1024)S(1)}, f32[4096]{0:T(1024)}, u32[]{:S(2)}) copy-start(f32[4096]{0:T(1024)} %param.16) | copy-start | bytes 49156
  6.3 18.4 %copy-start.7 = (bf16[2,4096,1]{1,0,2:T(2,128)(2,1)S(1)}, bf16[2,4096,1]{1,0,2:T(2,128)(2,1)}, u32[]{:S(2)}) copy-start(bf16[2,4096,1]{1,0,2:T(2,128)(2,1)} %param.21) | copy-start | bytes 49156
  6.3 18.4 %copy-start.9 = (f32[128]{0:T(128)S(1)}, f32[128]{0:T(128)}, u32[]{:S(2)}) copy-start(f32[128]{0:T(128)} %param.23) | copy-start | bytes 1540
  24.8 35.1 %copy-start.8 = (f32[4096]{0:T(1024)S(1)}, f32[4096]{0:T(1024)}, u32[]{:S(2)}) copy-start(f32[4096]{0:T(1024)} %param.26) | copy-start | bytes 49156
  38.5 21.5 %collective-permute-start.2 = (bf16[3,44,4096]{2,1,0:T(8,128)(2,1)S(1)}, bf16[3,44,4096]{2,1,0:T(8,128)(2,1)S(1)}, u32[]{:S(2)}, u32[]{:S(2)}) collective-permute-start(bf16[3,44,4096]{2,1,0:T(8,128)(2,1)S(1)} %collective-permute-done.refs_1_), channel_id=1, source_target_pairs={{0,64},{1,193},{2,66},{3,195},{4,68},{5,197},{6,70},{7,199},{8,72}... | collective-permute-start | bytes 3244040 | tf_op jit(solution)/shard_map/ppermute | solution.py:294
  41.5 19.0 %collective-permute-start.3 = (bf16[3,44,4096]{2,1,0:T(8,128)(2,1)S(1)}, bf16[3,44,4096]{2,1,0:T(8,128)(2,1)S(1)}, u32[]{:S(2)}, u32[]{:S(2)}) collective-permute-start(bf16[3,44,4096]{2,1,0:T(8,128)(2,1)S(1)} %get-tuple-element.23.refs_0_), channel_id=1, source_target_pairs={{0,1},{1,0},{2,3},{3,2},{4,5},{5,4},{6,7},{7,6},{8,9},{9,8},{10,11... | collective-permute-start | bytes 3244040 | tf_op jit(solution)/shard_map/ppermute | solution.py:296
  41.5 19.0 %collective-permute-start.5 = (bf16[3,44,4096]{2,1,0:T(8,128)(2,1)S(1)}, bf16[3,44,4096]{2,1,0:T(8,128)(2,1)S(1)}, u32[]{:S(2)}, u32[]{:S(2)}) collective-permute-start(bf16[3,44,4096]{2,1,0:T(8,128)(2,1)S(1)} %collective-permute-done.1.refs_2_), channel_id=1, source_target_pairs={{0,1},{1,0},{2,3},{3,2},{4,5},{5,4},{6,7},{7,6},{8,9},{9,8},{10,11... | collective-permute-start | bytes 3244040 | tf_op jit(solution)/shard_map/ppermute | solution.py:298
  42.0 18.5 %collective-permute-start.4 = (bf16[3,44,4096]{2,1,0:T(8,128)(2,1)S(1)}, bf16[3,44,4096]{2,1,0:T(8,128)(2,1)S(1)}, u32[]{:S(2)}, u32[]{:S(2)}) collective-permute-start(bf16[3,44,4096]{2,1,0:T(8,128)(2,1)S(1)} %collective-permute-done.refs_1_), channel_id=1, source_target_pairs={{0,1},{1,0},{2,3},{3,2},{4,5},{5,4},{6,7},{7,6},{8,9},{9,8},{10,11... | collective-permute-start | bytes 3244040 | tf_op jit(solution)/shard_map/ppermute | solution.py:297
  60.0 3.0 %collective-permute-start.6 = (bf16[3,44,4096]{2,1,0:T(8,128)(2,1)S(1)}, bf16[3,44,4096]{2,1,0:T(8,128)(2,1)S(1)}, u32[]{:S(2)}, u32[]{:S(2)}) collective-permute-start(bf16[3,44,4096]{2,1,0:T(8,128)(2,1)S(1)} %collective-permute-done.2.refs_6_), channel_id=1, source_target_pairs={{0,1},{1,0},{2,3},{3,2},{4,5},{5,4},{6,7},{7,6},{8,9},{9,8},{10,11... | collective-permute-start | bytes 3244040 | tf_op jit(solution)/shard_map/ppermute | solution.py:312
